TPU v7x, 32 devices: a whole 2x2x4 slice. The times are simulated.
32 devices in a mesh: ep: 8 (over z, core), tp: 4 (over y, x).
Axes of the slice: x: 2, y: 2, z: 4, core: 2. Of those that a mesh axis runs over, the one named last changes fastest.
Arguments:
- tokens: bfloat16 [4096, 2048], P(('ep', 'tp')), may hold values from -6 to 6
- routes: int32 [4096, 2], P(('ep', 'tp')), may hold values from 0 to 7, all different within a row; in each aligned block of 128 rows (0 to 127, 128 to 255, ...) at most 48 rows name the same one
- route_weights: float32 [4096, 2], P(('ep', 'tp')), may hold values from 0.25 to 2
- norm_gain: float32 [2048], replicated, may hold values from 0.1 to 1.9
- expert_gate: bfloat16 [8, 2048, 512], P('ep'), may hold values from -0.125 to 0.125
- expert_up: bfloat16 [8, 2048, 512], P('ep'), may hold values from -0.125 to 0.125
- expert_down: bfloat16 [8, 512, 2048], P('ep', None, 'tp')
- shared_gate: bfloat16 [2048, 512], replicated, may hold values from -0.125 to 0.125
- shared_up: bfloat16 [2048, 512], replicated, may hold values from -0.125 to 0.125
- shared_down: bfloat16 [512, 2048], P(None, 'tp')
- out_gain: float32 [2048], P('tp'), may hold values from 0.1 to 1.9
Outputs:
- normalized_out: bfloat16 [4096, 2048], P('ep', 'tp')
Inputs may be any that keep to these rules, and one draw needn't show every extreme that they name: `routes`: each row names 2 different experts. Within the rows of one device (aligned blocks of 128 rows) no expert is named by more than 48 rows, a bound that some block reaches.
All inputs are finite; a program needn't handle non-finite values.
Results may differ from a plain program's by a relative error of at most 0.0073.
Values may be sent and summed in bfloat16 or wider, within the bound.
No kernel may reach another device: no remote copies, remote signals or barrier semaphores. Data moves between devices by JAX's collectives and lax.ppermute only.
A program may use at most 64 MiB of HBM per device.

v0:
```python
import functools

import jax
import jax.numpy as jnp
from jax import lax
from jax.experimental import pallas as pl
from jax.experimental.pallas import tpu as pltpu
from jax.sharding import PartitionSpec as P


VMEM = pl.BlockSpec(memory_space=pltpu.VMEM)
SMEM = pl.BlockSpec(memory_space=pltpu.SMEM)
HBM = pl.BlockSpec(memory_space=pltpu.HBM)
F32 = jnp.float32
BF16 = jnp.bfloat16


def dot(a, b):
    return jnp.dot(a, b, preferred_element_type=F32)


def call(kernel, outs, inputs, flops, scalars=0, far=(), scratch=()):
    moved = sum(a.size * a.dtype.itemsize for a in inputs)
    moved += sum(o.size * o.dtype.itemsize for o in outs)
    specs = [SMEM] * scalars + [VMEM] * (len(inputs) - scalars)
    for i in far:
        specs[i] = HBM
    return pl.pallas_call(
        kernel,
        out_shape=outs,
        in_specs=specs,
        out_specs=[VMEM] * len(outs),
        scratch_shapes=scratch,
        cost_estimate=pl.CostEstimate(flops=flops, bytes_accessed=moved, transcendentals=0),
        compiler_params=pltpu.CompilerParams(vmem_limit_bytes=40 * 1024 * 1024),
    )(*inputs)


def fetch(sources, targets, sems):
    copies = [
        pltpu.make_async_copy(source, target, sems.at[i])
        for i, (source, target) in enumerate(zip(sources, targets))
    ]
    for copy in copies:
        copy.start()
    return copies


def swiglu(rows, both):
    parts = dot(rows, both)
    inner = parts.shape[1] // 2
    gate_part, up_part = parts[:, :inner], parts[:, inner:]
    return (gate_part / (1.0 + jnp.exp(-gate_part)) * up_part).astype(BF16)


def prepare_kernel(experts, capacity, me, *refs):
    normed, pieces = refs[3], refs[4 : 4 + experts]
    tokens, gain, routes, sems = refs[4 + experts :]
    copies = fetch(refs[:3], (tokens, gain, routes), sems)
    copies[0].wait()
    values = tokens[...].astype(F32)
    inverse = lax.rsqrt(jnp.mean(values * values, axis=1, keepdims=True) + 1e-06)
    copies[1].wait()
    rows = (values * inverse * gain[...]).astype(BF16)
    normed[...] = rows
    copies[2].wait()
    count = values.shape[0]
    index = lax.broadcasted_iota(jnp.int32, (experts, count), 0)
    marks = [index == routes[j : j + 1, :] for j in range(routes.shape[0])]
    marked = functools.reduce(jnp.logical_or, marks)
    earlier = lax.broadcasted_iota(jnp.int32, (count, count), 0) < lax.broadcasted_iota(
        jnp.int32, (count, count), 1
    )
    before = dot(marked.astype(BF16), earlier.astype(BF16))
    places = []
    for j, mark in enumerate(marks):
        slot = jnp.sum(jnp.where(mark, before, 0.0), axis=0, keepdims=True)
        places.append((routes[j : j + 1, :] ^ me[0]) * capacity + slot.astype(jnp.int32))
    half = experts // 2
    for start in (half, 0):
        at = lax.broadcasted_iota(jnp.int32, (half * capacity, count), 0) + start * capacity
        chosen = functools.reduce(jnp.logical_or, [at == place for place in places])
        moved = dot(chosen.astype(F32).astype(BF16), rows).astype(BF16)
        for k in range(half):
            pieces[start + k][...] = moved[k * capacity : (k + 1) * capacity]


def table_kernel(capacity, groups, me, *refs):
    packed, outs = refs[: -len(groups)], refs[-len(groups) :]
    for m, ref in enumerate(packed):
        top_count = ref.shape[0] // 2
        count = ref.shape[1]
        columns = [
            jnp.broadcast_to(ref[r : r + 1, :], (count, count)).T for r in range(2 * top_count)
        ]
        lane = lax.broadcasted_iota(jnp.int32, (count, count), 1)
        chosen = [c.astype(jnp.int32) for c in columns[:top_count]]
        marks = [lane == c for c in chosen]
        marked = functools.reduce(jnp.logical_or, marks)
        earlier = lax.broadcasted_iota(jnp.int32, (count, count), 0) > lane
        before = dot(earlier.astype(F32).astype(BF16), marked.astype(F32).astype(BF16))
        places = []
        for c, mark in zip(chosen, marks):
            slot = jnp.sum(jnp.where(mark, before, 0.0), axis=1, keepdims=True)
            places.append((c[:, :1] ^ me[0]) * capacity + slot.astype(jnp.int32))
        for (start, size), out in zip(groups, outs):
            wide = size * capacity
            at = lax.broadcasted_iota(jnp.int32, (count, wide), 1) + start * capacity
            table = functools.reduce(
                jnp.add,
                [
                    jnp.where(at == place, weight[:, :1], 0.0)
                    for place, weight in zip(places, columns[top_count:])
                ],
            )
            for part in range(3):
                piece = table.astype(BF16)
                out[m, part * count : (part + 1) * count, :] = piece
                table = table - piece.astype(F32)


def stage_kernel(gate, upward, held, both, sems):
    inner = gate.shape[1]
    for copy in fetch((gate, upward), (both.at[:, :inner], both.at[:, inner:]), sems):
        copy.wait()


def shared_kernel(normed, gate, upward, hidden, both, sems):
    inner = gate.shape[1]
    for copy in fetch((gate, upward), (both.at[:, :inner], both.at[:, inner:]), sems):
        copy.wait()
    hidden[...] = swiglu(normed[...], both[...])


def hidden_kernel(*refs):
    rows = jnp.concatenate([r[...] for r in refs[:-2]], axis=0)
    refs[-1][...] = swiglu(rows, refs[-2][...])


def down_kernel(blocks, units, capacity, *refs):
    hidden = refs[:blocks]
    down = refs[blocks]
    outs = refs[blocks + 1 :]
    count = units * capacity
    rows = jnp.concatenate([h[...] for h in hidden], axis=0)
    result = dot(rows, down[...]).astype(BF16)
    for u in range(units):
        for m in range(blocks):
            first = m * count + u * capacity
            outs[u][m] = result[first : first + capacity]


def weighted(table, returned, m):
    rows = jnp.concatenate([r[m] for r in returned], axis=0)
    parts = dot(table[m], rows)
    count = parts.shape[0] // 3
    return parts[:count] + parts[count : 2 * count] + parts[2 * count :]


def base_kernel(blocks, *refs):
    hidden = refs[:blocks]
    down, table = refs[blocks : blocks + 2]
    returned, out = refs[blocks + 2 : -1], refs[-1]
    shared = dot(jnp.concatenate([h[...] for h in hidden], axis=0), down[...])
    count = out.shape[1]
    for m in range(blocks):
        out[m] = shared[m * count : (m + 1) * count] + weighted(table, returned, m)


def more_kernel(blocks, total, table, *refs):
    for m in range(blocks):
        refs[-1][m] = total[m] + weighted(table, refs[:-1], m)


def finish_kernel(blocks, total, table, *refs):
    returned = refs[:-2]
    moe, squares = refs[-2:]
    ones = jnp.ones((8, moe.shape[2]), F32)
    for m in range(blocks):
        rounded = (total[m] + weighted(table, returned, m)).astype(BF16)
        moe[m] = rounded
        wide = rounded.astype(F32)
        sums = lax.dot_general(
            ones,
            wide * wide,
            (((1,), (1,)), ((), ())),
            precision=lax.Precision.HIGHEST,
            preferred_element_type=F32,
        )
        squares[m : m + 1, :] = sums[:1]


def scale_kernel(blocks, width, me, moe, gain, *refs):
    squares, out = refs[:blocks], refs[-1]
    count = moe.shape[1]
    for m in range(blocks):
        total = squares[0][m : m + 1, :]
        for p in range(1, blocks):
            total = total + squares[p][m ^ p : (m ^ p) + 1, :]
        scale = lax.rsqrt(total / width + 1e-06)
        column = jnp.broadcast_to(scale, (count, count)).T[:, :1]
        first = pl.multiple_of((me[0] ^ m) * count, count)
        value = moe[m].astype(F32) * column * gain[...]
        out[pl.ds(first, count), :] = value.astype(BF16)


def swap(array, axis, k):
    size = lax.axis_size(axis)
    return lax.ppermute(array, axis, [(s, s ^ k) for s in range(size)])


def spread(array):
    return [array] + [swap(array, "tp", m) for m in range(1, lax.axis_size("tp"))]


def fast_device(
    tokens,
    routes,
    route_weights,
    norm_gain,
    expert_gate,
    expert_up,
    expert_down,
    shared_gate,
    shared_up,
    shared_down,
    out_gain,
):
    count, width = tokens.shape
    top_count = routes.shape[1]
    experts = lax.axis_size("ep")
    blocks = lax.axis_size("tp")
    inner = expert_gate.shape[2]
    local = expert_down.shape[2]
    capacity = 3 * count * top_count // (2 * experts)
    row = lax.axis_index("ep").astype(jnp.int32).reshape(1)
    column = lax.axis_index("tp").astype(jnp.int32).reshape(1)
    piece = jax.ShapeDtypeStruct((capacity, width), BF16)
    normed, *pieces = call(
        functools.partial(prepare_kernel, experts, capacity),
        [jax.ShapeDtypeStruct((count, width), BF16)] + [piece] * experts,
        [row, tokens, norm_gain[None, :], routes.T],
        2 * experts * capacity * count * width,
        scalars=1,
        far=(1, 2, 3),
        scratch=[
            pltpu.VMEM((count, width), BF16),
            pltpu.VMEM((1, width), F32),
            pltpu.VMEM((top_count, count), jnp.int32),
            pltpu.SemaphoreType.DMA((3,)),
        ],
    )
    half, quarter = experts // 2, experts // 4
    arrived = [pieces[0]] + [swap(pieces[k], "ep", k) for k in range(1, experts)]
    groups = {"N": (0, half), "A": (half, quarter), "B": (half + quarter, quarter)}

    packed = jnp.concatenate([routes.T.astype(F32), route_weights.T], axis=0)
    packed = spread(packed)
    both = jax.ShapeDtypeStruct((width, 2 * inner), BF16)
    (weights,) = call(
        stage_kernel,
        [both],
        [expert_gate[0], expert_up[0], normed],
        count * width,
        far=(0, 1, 2),
        scratch=[pltpu.SemaphoreType.DMA((2,))],
    )
    (shared,) = call(
        shared_kernel,
        [jax.ShapeDtypeStruct((count, inner), BF16)],
        [normed, shared_gate, shared_up],
        4 * count * width * inner,
        far=(1, 2),
        scratch=[pltpu.VMEM(both.shape, BF16), pltpu.SemaphoreType.DMA((2,))],
    )
    shared = spread(shared)
    tables = call(
        functools.partial(table_kernel, capacity, list(groups.values())),
        [
            jax.ShapeDtypeStruct((blocks, 3 * count, size * capacity), BF16)
            for _, size in groups.values()
        ],
        [row] + packed,
        blocks * count * count * count,
        scalars=1,
    )

    returned = {}
    for name, (first, size) in groups.items():
        rows = size * capacity
        (hidden,) = call(
            hidden_kernel,
            [jax.ShapeDtypeStruct((rows, inner), BF16)],
            arrived[first : first + size] + [weights],
            4 * rows * width * inner,
        )
        results = call(
            functools.partial(down_kernel, blocks, size, capacity),
            [jax.ShapeDtypeStruct((blocks, capacity, local), BF16)] * size,
            spread(hidden) + [expert_down[0]],
            2 * blocks * rows * inner * local,
        )
        returned[name] = [
            swap(results[u], "ep", first + u) if first + u else results[u]
            for u in range(size)
        ]

    sums = jax.ShapeDtypeStruct((blocks, count, local), F32)
    (total,) = call(
        functools.partial(base_kernel, blocks),
        [sums],
        shared + [shared_down, tables[0]] + returned["N"],
        2 * blocks * count * local * (inner + 3 * half * capacity),
    )
    (total,) = call(
        functools.partial(more_kernel, blocks),
        [sums],
        [total, tables[1]] + returned["A"],
        2 * blocks * count * local * 3 * quarter * capacity,
    )
    moe, squares = call(
        functools.partial(finish_kernel, blocks),
        [
            jax.ShapeDtypeStruct((blocks, count, local), BF16),
            jax.ShapeDtypeStruct((blocks, count), F32),
        ],
        [total, tables[2]] + returned["B"],
        2 * blocks * count * local * 3 * quarter * capacity,
    )
    (out,) = call(
        functools.partial(scale_kernel, blocks, width),
        [jax.ShapeDtypeStruct((blocks * count, local), BF16)],
        [column, moe, out_gain[None, :]] + spread(squares),
        4 * blocks * count * local,
        scalars=1,
    )
    return out


def swiglu_rows(rows, gate, upward):
    gate_part = jnp.dot(rows, gate, preferred_element_type=jnp.float32)
    up_part = jnp.dot(rows, upward, preferred_element_type=jnp.float32)
    return (jax.nn.silu(gate_part) * up_part).astype(jnp.bfloat16)


def plain_device(
    tokens,
    routes,
    route_weights,
    norm_gain,
    expert_gate,
    expert_up,
    expert_down,
    shared_gate,
    shared_up,
    shared_down,
    out_gain,
):
    count_tokens, width = tokens.shape
    top_count = routes.shape[1]
    experts = lax.axis_size("ep")
    capacity = max(2, 3 * count_tokens * top_count // (2 * experts))
    tokens_f32 = tokens.astype(jnp.float32)
    inverse = lax.rsqrt(jnp.mean(tokens_f32 * tokens_f32, axis=1, keepdims=True) + 1e-06)
    normed = (tokens_f32 * inverse * norm_gain[None, :]).astype(jnp.bfloat16)
    chosen = routes.reshape(-1)
    marks = (chosen[:, None] == jnp.arange(experts, dtype=jnp.int32)[None, :]).astype(jnp.int32)
    slots = jnp.sum(jnp.cumsum(marks, axis=0) * marks, axis=1) - 1
    places = chosen * capacity + slots
    owners = jnp.arange(chosen.shape[0], dtype=jnp.int32) // top_count
    table = jnp.zeros((experts * capacity,), jnp.int32).at[places].set(owners)
    filled = jnp.zeros((experts * capacity,), jnp.bool_).at[places].set(True)
    outbound = jnp.where(filled[:, None], normed[table], jnp.zeros((), jnp.bfloat16))
    outbound = outbound.reshape(experts, capacity, width)
    arrived = lax.all_to_all(outbound, "ep", split_axis=0, concat_axis=0, tiled=True).reshape(
        experts * capacity, width
    )
    hidden = swiglu_rows(arrived, expert_gate[0], expert_up[0])
    results = jnp.dot(
        hidden,
        lax.all_gather(expert_down[0], "tp", axis=1, tiled=True),
        preferred_element_type=jnp.float32,
    ).astype(jnp.bfloat16)
    returned = lax.all_to_all(
        results.reshape(experts, capacity, width), "ep", split_axis=0, concat_axis=0, tiled=True
    )
    returned = returned.reshape(experts * capacity, width)
    picked = returned[places].astype(jnp.float32).reshape(count_tokens, top_count, width)
    routed = jnp.sum(picked * route_weights[:, :, None], axis=1)
    shared_hidden = swiglu_rows(normed, shared_gate, shared_up)
    shared_out = jnp.dot(
        shared_hidden,
        lax.all_gather(shared_down, "tp", axis=1, tiled=True),
        preferred_element_type=jnp.float32,
    )
    moe = (shared_out + routed).astype(jnp.bfloat16)
    columns = lax.all_to_all(moe, "tp", split_axis=1, concat_axis=0, tiled=True)
    values = columns.astype(jnp.float32)
    own_rows = moe.astype(jnp.float32)
    totals = lax.all_gather(jnp.sum(own_rows * own_rows, axis=1), "tp", axis=0, tiled=True)
    scale = lax.rsqrt(totals / width + 1e-06)
    return (values * scale[:, None] * out_gain[None, :]).astype(jnp.bfloat16)


def per_device(tokens, routes, *rest):
    count, width = tokens.shape
    experts, blocks = lax.axis_size("ep"), lax.axis_size("tp")
    capacity = 3 * count * routes.shape[1] // (2 * experts)
    powers = experts & (experts - 1) == 0 and blocks & (blocks - 1) == 0
    aligned = capacity % 16 == 0 and width // blocks % 128 == 0 and count % 128 == 0
    fits = powers and aligned and experts >= 8
    return (fast_device if fits else plain_device)(tokens, routes, *rest)


def solution(mesh):
    in_specs = (
        P(("ep", "tp"), None),
        P(("ep", "tp"), None),
        P(("ep", "tp"), None),
        P(),
        P("ep", None, None),
        P("ep", None, None),
        P("ep", None, "tp"),
        P(),
        P(),
        P(None, "tp"),
        P("tp"),
    )
    out_specs = P("ep", "tp")
    return jax.shard_map(
        per_device, mesh=mesh, in_specs=in_specs, out_specs=out_specs, check_vma=False
    )
```

profile of v0, /device:TPU:16, one launch (start us, length us, event | category | flops | bytes accessed | tf_op | source)
XLA Modules:
  0.0 110.9 jit_solution(17184354721256008018)
XLA Ops:
  3.6 1.6 %collective-permute-start.7 = (bf16[48,2048]{1,0:T(8,128)(2,1)S(1)}, bf16[48,2048]{1,0:T(8,128)(2,1)S(1)}, u32[]{:S(2)}, u32[]{:S(2)}) collective-permute-start(bf16[48,2048]{1,0:T(8,128)(2,1)S(1)} %get-tuple-element.31), channel_id=1, source_target_pairs={{0,8},{4,12},{8,0},{12,4},{16,24},{20,28},{24,16},{28,20},{1,9},{5... | collective-permute-start | bytes 589832 | tf_op jit(solution)/shard_map/ppermute | solution.py:209
  9.7 2.4 %collective-permute-start.5 = (f32[4,128]{1,0:T(4,128)S(1)}, f32[4,128]{1,0:T(4,128)S(1)}, u32[]{:S(2)}, u32[]{:S(2)}) collective-permute-start(f32[4,128]{1,0:T(4,128)S(1)} %pad_maximum_fusion.refs_0_), channel_id=1, source_target_pairs={{0,3},{1,2},{2,1},{3,0},{4,7},{5,6},{6,5},{7,4},{8,11},{9,10},{10,... | collective-permute-start | bytes 6152 | tf_op jit(solution)/shard_map/ppermute | solution.py:209
  12.6 1.6 %collective-permute-done.5.refs_3_ = f32[4,128]{1,0:T(4,128)S(1)} collective-permute-done((f32[4,128]{1,0:T(4,128)S(1)}, f32[4,128]{1,0:T(4,128)S(1)}, u32[]{:S(2)}, u32[]{:S(2)}) %collective-permute-start.5) | collective-permute-done | bytes 2080 | tf_op jit(solution)/shard_map/ppermute | solution.py:209
  14.2 1.6 %copy-done.2 = bf16[2048,512]{1,0:T(8,128)(2,1)S(1)} copy-done((bf16[2048,512]{1,0:T(8,128)(2,1)S(1)}, bf16[2048,512]{1,0:T(8,128)(2,1)}, u32[]{:S(2)}) %copy-start.2) | copy-done | bytes 2097176
  15.8 1.6 %copy-done.3 = bf16[2048,512]{1,0:T(8,128)(2,1)S(1)} copy-done((bf16[2048,512]{1,0:T(8,128)(2,1)S(1)}, bf16[2048,512]{1,0:T(8,128)(2,1)}, u32[]{:S(2)}) %copy-start.3) | copy-done | bytes 2097176
  18.8 1.6 %collective-permute-start = (bf16[128,512]{1,0:T(8,128)(2,1)S(1)}, bf16[128,512]{1,0:T(8,128)(2,1)S(1)}, u32[]{:S(2)}, u32[]{:S(2)}) collective-permute-start(bf16[128,512]{1,0:T(8,128)(2,1)S(1)} %shard_map.110.refs_0_), channel_id=1, source_target_pairs={{0,1},{1,0},{2,3},{3,2},{4,5},{5,4},{6,7},{7,6},{8,9},{9,8},{10,11... | collective-permute-start | bytes 393224 | tf_op jit(solution)/shard_map/ppermute | solution.py:209
  21.1 2.0 %collective-permute-start.15 = (bf16[48,2048]{1,0:T(8,128)(2,1)S(1)}, bf16[48,2048]{1,0:T(8,128)(2,1)S(1)}, u32[]{:S(2)}, u32[]{:S(2)}) collective-permute-start(bf16[48,2048]{1,0:T(8,128)(2,1)S(1)} %get-tuple-element.38), channel_id=1, source_target_pairs={{0,16},{4,20},{8,24},{12,28},{16,0},{20,4},{24,8},{28,12},{1,17},{... | collective-permute-start | bytes 589832 | tf_op jit(solution)/shard_map/ppermute | solution.py:209
  23.1 1.6 %collective-permute-start.16 = (bf16[48,2048]{1,0:T(8,128)(2,1)S(1)}, bf16[48,2048]{1,0:T(8,128)(2,1)S(1)}, u32[]{:S(2)}, u32[]{:S(2)}) collective-permute-start(bf16[48,2048]{1,0:T(8,128)(2,1)S(1)} %get-tuple-element.39), channel_id=1, source_target_pairs={{0,20},{4,16},{8,28},{12,24},{16,4},{20,0},{24,12},{28,8},{1,21},{... | collective-permute-start | bytes 589832 | tf_op jit(solution)/shard_map/ppermute | solution.py:209
  25.6 1.6 %collective-permute-start.10 = (bf16[192,512]{1,0:T(8,128)(2,1)S(1)}, bf16[192,512]{1,0:T(8,128)(2,1)S(1)}, u32[]{:S(2)}, u32[]{:S(2)}) collective-permute-start(bf16[192,512]{1,0:T(8,128)(2,1)S(1)} %shard_map.113.refs_0_), channel_id=1, source_target_pairs={{0,2},{1,3},{2,0},{3,1},{4,6},{5,7},{6,4},{7,5},{8,10},{9,11},{10,... | collective-permute-start | bytes 589832 | tf_op jit(solution)/shard_map/ppermute | solution.py:209
  27.2 9.6 %collective-permute-done.22.refs_0_ = bf16[48,2048]{1,0:T(8,128)(2,1)S(1)} collective-permute-done((bf16[48,2048]{1,0:T(8,128)(2,1)S(1)}, bf16[48,2048]{1,0:T(8,128)(2,1)S(1)}, u32[]{:S(2)}, u32[]{:S(2)}) %collective-permute-start.22) | collective-permute-done | bytes 196640 | tf_op jit(solution)/shard_map/ppermute | solution.py:209
  36.8 2.1 %collective-permute-done.23.refs_1_ = bf16[48,2048]{1,0:T(8,128)(2,1)S(1)} collective-permute-done((bf16[48,2048]{1,0:T(8,128)(2,1)S(1)}, bf16[48,2048]{1,0:T(8,128)(2,1)S(1)}, u32[]{:S(2)}, u32[]{:S(2)}) %collective-permute-start.23) | collective-permute-done | bytes 196640 | tf_op jit(solution)/shard_map/ppermute | solution.py:209
  38.9 4.2 %collective-permute-done.15.refs_0_ = bf16[48,2048]{1,0:T(8,128)(2,1)S(1)} collective-permute-done((bf16[48,2048]{1,0:T(8,128)(2,1)S(1)}, bf16[48,2048]{1,0:T(8,128)(2,1)S(1)}, u32[]{:S(2)}, u32[]{:S(2)}) %collective-permute-start.15) | collective-permute-done | bytes 196640 | tf_op jit(solution)/shard_map/ppermute | solution.py:209
  43.1 2.5 %collective-permute-done.16.refs_1_ = bf16[48,2048]{1,0:T(8,128)(2,1)S(1)} collective-permute-done((bf16[48,2048]{1,0:T(8,128)(2,1)S(1)}, bf16[48,2048]{1,0:T(8,128)(2,1)S(1)}, u32[]{:S(2)}, u32[]{:S(2)}) %collective-permute-start.16) | collective-permute-done | bytes 196640 | tf_op jit(solution)/shard_map/ppermute | solution.py:209
  47.0 1.5 %collective-permute-start.24 = (bf16[96,512]{1,0:T(8,128)(2,1)S(1)}, bf16[96,512]{1,0:T(8,128)(2,1)S(1)}, u32[]{:S(2)}, u32[]{:S(2)}) collective-permute-start(bf16[96,512]{1,0:T(8,128)(2,1)S(1)} %shard_map.119.refs_0_), channel_id=1, source_target_pairs={{0,1},{1,0},{2,3},{3,2},{4,5},{5,4},{6,7},{7,6},{8,9},{9,8},{10,11... | collective-permute-start | bytes 294920 | tf_op jit(solution)/shard_map/ppermute | solution.py:209
  54.3 1.9 %collective-permute-start.19 = (bf16[96,512]{1,0:T(8,128)(2,1)S(1)}, bf16[96,512]{1,0:T(8,128)(2,1)S(1)}, u32[]{:S(2)}, u32[]{:S(2)}) collective-permute-start(bf16[96,512]{1,0:T(8,128)(2,1)S(1)} %shard_map.116.refs_0_), channel_id=1, source_target_pairs={{0,3},{1,2},{2,1},{3,0},{4,7},{5,6},{6,5},{7,4},{8,11},{9,10},{10,... | collective-permute-start | bytes 294920 | tf_op jit(solution)/shard_map/ppermute | solution.py:209
  57.3 1.6 %collective-permute-start.26 = (bf16[96,512]{1,0:T(8,128)(2,1)S(1)}, bf16[96,512]{1,0:T(8,128)(2,1)S(1)}, u32[]{:S(2)}, u32[]{:S(2)}) collective-permute-start(bf16[96,512]{1,0:T(8,128)(2,1)S(1)} %shard_map.119.refs_0_), channel_id=1, source_target_pairs={{0,3},{1,2},{2,1},{3,0},{4,7},{5,6},{6,5},{7,4},{8,11},{9,10},{10,... | collective-permute-start | bytes 294920 | tf_op jit(solution)/shard_map/ppermute | solution.py:209
  58.9 2.0 %collective-permute-done.19.refs_3_ = bf16[96,512]{1,0:T(8,128)(2,1)S(1)} collective-permute-done((bf16[96,512]{1,0:T(8,128)(2,1)S(1)}, bf16[96,512]{1,0:T(8,128)(2,1)S(1)}, u32[]{:S(2)}, u32[]{:S(2)}) %collective-permute-start.19) | collective-permute-done | bytes 98336 | tf_op jit(solution)/shard_map/ppermute | solution.py:209
  61.3 3.3 %collective-permute-done.25.refs_2_ = bf16[96,512]{1,0:T(8,128)(2,1)S(1)} collective-permute-done((bf16[96,512]{1,0:T(8,128)(2,1)S(1)}, bf16[96,512]{1,0:T(8,128)(2,1)S(1)}, u32[]{:S(2)}, u32[]{:S(2)}) %collective-permute-start.25) | collective-permute-done | bytes 98336 | tf_op jit(solution)/shard_map/ppermute | solution.py:209
  64.6 1.6 %collective-permute-start.20 = (bf16[4,48,512]{2,1,0:T(8,128)(2,1)S(1)}, bf16[4,48,512]{2,1,0:T(8,128)(2,1)S(1)}, u32[]{:S(2)}, u32[]{:S(2)}) collective-permute-start(bf16[4,48,512]{2,1,0:T(8,128)(2,1)S(1)} %get-tuple-element.40), channel_id=1, source_target_pairs={{0,16},{4,20},{8,24},{12,28},{16,0},{20,4},{24,8},{28,12},{1,17},{... | collective-permute-start | bytes 589832 | tf_op jit(solution)/shard_map/ppermute | solution.py:209
  71.5 16.6 %collective-permute-done.20.refs_0_ = bf16[4,48,512]{2,1,0:T(8,128)(2,1)S(1)} collective-permute-done((bf16[4,48,512]{2,1,0:T(8,128)(2,1)S(1)}, bf16[4,48,512]{2,1,0:T(8,128)(2,1)S(1)}, u32[]{:S(2)}, u32[]{:S(2)}) %collective-permute-start.20) | collective-permute-done | bytes 196640 | tf_op jit(solution)/shard_map/ppermute | solution.py:209
  88.1 4.2 %collective-permute-done.21.refs_1_ = bf16[4,48,512]{2,1,0:T(8,128)(2,1)S(1)} collective-permute-done((bf16[4,48,512]{2,1,0:T(8,128)(2,1)S(1)}, bf16[4,48,512]{2,1,0:T(8,128)(2,1)S(1)}, u32[]{:S(2)}, u32[]{:S(2)}) %collective-permute-start.21) | collective-permute-done | bytes 196640 | tf_op jit(solution)/shard_map/ppermute | solution.py:209
  92.9 4.8 %collective-permute-done.27.refs_0_ = bf16[4,48,512]{2,1,0:T(8,128)(2,1)S(1)} collective-permute-done((bf16[4,48,512]{2,1,0:T(8,128)(2,1)S(1)}, bf16[4,48,512]{2,1,0:T(8,128)(2,1)S(1)}, u32[]{:S(2)}, u32[]{:S(2)}) %collective-permute-start.27) | collective-permute-done | bytes 196640 | tf_op jit(solution)/shard_map/ppermute | solution.py:209
  97.7 4.0 %collective-permute-done.28.refs_1_ = bf16[4,48,512]{2,1,0:T(8,128)(2,1)S(1)} collective-permute-done((bf16[4,48,512]{2,1,0:T(8,128)(2,1)S(1)}, bf16[4,48,512]{2,1,0:T(8,128)(2,1)S(1)}, u32[]{:S(2)}, u32[]{:S(2)}) %collective-permute-start.28) | collective-permute-done | bytes 196640 | tf_op jit(solution)/shard_map/ppermute | solution.py:209
  107.6 2.2 %collective-permute-done.31.refs_3_ = f32[4,128]{1,0:T(4,128)S(1)} collective-permute-done((f32[4,128]{1,0:T(4,128)S(1)}, f32[4,128]{1,0:T(4,128)S(1)}, u32[]{:S(2)}, u32[]{:S(2)}) %collective-permute-start.31) | collective-permute-done | bytes 2080 | tf_op jit(solution)/shard_map/ppermute | solution.py:209
  (76 shorter events, 32.8 us)
Async XLA Ops:
  3.5 15.3 %collective-permute-start.6 = (bf16[48,2048]{1,0:T(8,128)(2,1)S(1)}, bf16[48,2048]{1,0:T(8,128)(2,1)S(1)}, u32[]{:S(2)}, u32[]{:S(2)}) collective-permute-start(bf16[48,2048]{1,0:T(8,128)(2,1)S(1)} %get-tuple-element.30), channel_id=1, source_target_pairs={{0,4},{4,0},{8,12},{12,8},{16,20},{20,16},{24,28},{28,24},{1,5},{5... | collective-permute-start | bytes 589832 | tf_op jit(solution)/shard_map/ppermute | solution.py:209
  3.6 17.5 %collective-permute-start.7 = (bf16[48,2048]{1,0:T(8,128)(2,1)S(1)}, bf16[48,2048]{1,0:T(8,128)(2,1)S(1)}, u32[]{:S(2)}, u32[]{:S(2)}) collective-permute-start(bf16[48,2048]{1,0:T(8,128)(2,1)S(1)} %get-tuple-element.31), channel_id=1, source_target_pairs={{0,8},{4,12},{8,0},{12,4},{16,24},{20,28},{24,16},{28,20},{1,9},{5... | collective-permute-start | bytes 589832 | tf_op jit(solution)/shard_map/ppermute | solution.py:209
  5.2 17.8 %collective-permute-start.8 = (bf16[48,2048]{1,0:T(8,128)(2,1)S(1)}, bf16[48,2048]{1,0:T(8,128)(2,1)S(1)}, u32[]{:S(2)}, u32[]{:S(2)}) collective-permute-start(bf16[48,2048]{1,0:T(8,128)(2,1)S(1)} %get-tuple-element.32), channel_id=1, source_target_pairs={{0,12},{4,8},{8,4},{12,0},{16,28},{20,24},{24,20},{28,16},{1,13},{... | collective-permute-start | bytes 589832 | tf_op jit(solution)/shard_map/ppermute | solution.py:209
  12.2 24.6 %collective-permute-start.22 = (bf16[48,2048]{1,0:T(8,128)(2,1)S(1)}, bf16[48,2048]{1,0:T(8,128)(2,1)S(1)}, u32[]{:S(2)}, u32[]{:S(2)}) collective-permute-start(bf16[48,2048]{1,0:T(8,128)(2,1)S(1)} %get-tuple-element.43), channel_id=1, source_target_pairs={{0,24},{4,28},{8,16},{12,20},{16,8},{20,12},{24,0},{28,4},{1,25},{... | collective-permute-start | bytes 589832 | tf_op jit(solution)/shard_map/ppermute | solution.py:209
  14.2 24.7 %collective-permute-start.23 = (bf16[48,2048]{1,0:T(8,128)(2,1)S(1)}, bf16[48,2048]{1,0:T(8,128)(2,1)S(1)}, u32[]{:S(2)}, u32[]{:S(2)}) collective-permute-start(bf16[48,2048]{1,0:T(8,128)(2,1)S(1)} %get-tuple-element.44), channel_id=1, source_target_pairs={{0,28},{4,24},{8,20},{12,16},{16,12},{20,8},{24,4},{28,0},{1,29},{... | collective-permute-start | bytes 589832 | tf_op jit(solution)/shard_map/ppermute | solution.py:209
  18.8 6.8 %collective-permute-start = (bf16[128,512]{1,0:T(8,128)(2,1)S(1)}, bf16[128,512]{1,0:T(8,128)(2,1)S(1)}, u32[]{:S(2)}, u32[]{:S(2)}) collective-permute-start(bf16[128,512]{1,0:T(8,128)(2,1)S(1)} %shard_map.110.refs_0_), channel_id=1, source_target_pairs={{0,1},{1,0},{2,3},{3,2},{4,5},{5,4},{6,7},{7,6},{8,9},{9,8},{10,11... | collective-permute-start | bytes 393224 | tf_op jit(solution)/shard_map/ppermute | solution.py:209
  21.1 22.0 %collective-permute-start.15 = (bf16[48,2048]{1,0:T(8,128)(2,1)S(1)}, bf16[48,2048]{1,0:T(8,128)(2,1)S(1)}, u32[]{:S(2)}, u32[]{:S(2)}) collective-permute-start(bf16[48,2048]{1,0:T(8,128)(2,1)S(1)} %get-tuple-element.38), channel_id=1, source_target_pairs={{0,16},{4,20},{8,24},{12,28},{16,0},{20,4},{24,8},{28,12},{1,17},{... | collective-permute-start | bytes 589832 | tf_op jit(solution)/shard_map/ppermute | solution.py:209
  23.1 22.6 %collective-permute-start.16 = (bf16[48,2048]{1,0:T(8,128)(2,1)S(1)}, bf16[48,2048]{1,0:T(8,128)(2,1)S(1)}, u32[]{:S(2)}, u32[]{:S(2)}) collective-permute-start(bf16[48,2048]{1,0:T(8,128)(2,1)S(1)} %get-tuple-element.39), channel_id=1, source_target_pairs={{0,20},{4,16},{8,28},{12,24},{16,4},{20,0},{24,12},{28,8},{1,21},{... | collective-permute-start | bytes 589832 | tf_op jit(solution)/shard_map/ppermute | solution.py:209
  25.6 21.4 %collective-permute-start.10 = (bf16[192,512]{1,0:T(8,128)(2,1)S(1)}, bf16[192,512]{1,0:T(8,128)(2,1)S(1)}, u32[]{:S(2)}, u32[]{:S(2)}) collective-permute-start(bf16[192,512]{1,0:T(8,128)(2,1)S(1)} %shard_map.113.refs_0_), channel_id=1, source_target_pairs={{0,2},{1,3},{2,0},{3,1},{4,6},{5,7},{6,4},{7,5},{8,10},{9,11},{10,... | collective-permute-start | bytes 589832 | tf_op jit(solution)/shard_map/ppermute | solution.py:209
  36.8 12.6 %collective-permute-start.11 = (bf16[192,512]{1,0:T(8,128)(2,1)S(1)}, bf16[192,512]{1,0:T(8,128)(2,1)S(1)}, u32[]{:S(2)}, u32[]{:S(2)}) collective-permute-start(bf16[192,512]{1,0:T(8,128)(2,1)S(1)} %shard_map.113.refs_0_), channel_id=1, source_target_pairs={{0,3},{1,2},{2,1},{3,0},{4,7},{5,6},{6,5},{7,4},{8,11},{9,10},{10,... | collective-permute-start | bytes 589832 | tf_op jit(solution)/shard_map/ppermute | solution.py:209
  38.9 11.1 %collective-permute-start.9 = (bf16[192,512]{1,0:T(8,128)(2,1)S(1)}, bf16[192,512]{1,0:T(8,128)(2,1)S(1)}, u32[]{:S(2)}, u32[]{:S(2)}) collective-permute-start(bf16[192,512]{1,0:T(8,128)(2,1)S(1)} %shard_map.113.refs_0_), channel_id=1, source_target_pairs={{0,1},{1,0},{2,3},{3,2},{4,5},{5,4},{6,7},{7,6},{8,9},{9,8},{10,11... | collective-permute-start | bytes 589832 | tf_op jit(solution)/shard_map/ppermute | solution.py:209
  43.1 8.9 %collective-permute-start.1 = (bf16[128,512]{1,0:T(8,128)(2,1)S(1)}, bf16[128,512]{1,0:T(8,128)(2,1)S(1)}, u32[]{:S(2)}, u32[]{:S(2)}) collective-permute-start(bf16[128,512]{1,0:T(8,128)(2,1)S(1)} %shard_map.110.refs_0_), channel_id=1, source_target_pairs={{0,2},{1,3},{2,0},{3,1},{4,6},{5,7},{6,4},{7,5},{8,10},{9,11},{10,... | collective-permute-start | bytes 393224 | tf_op jit(solution)/shard_map/ppermute | solution.py:209
  45.7 7.2 %collective-permute-start.2 = (bf16[128,512]{1,0:T(8,128)(2,1)S(1)}, bf16[128,512]{1,0:T(8,128)(2,1)S(1)}, u32[]{:S(2)}, u32[]{:S(2)}) collective-permute-start(bf16[128,512]{1,0:T(8,128)(2,1)S(1)} %shard_map.110.refs_0_), channel_id=1, source_target_pairs={{0,3},{1,2},{2,1},{3,0},{4,7},{5,6},{6,5},{7,4},{8,11},{9,10},{10,... | collective-permute-start | bytes 393224 | tf_op jit(solution)/shard_map/ppermute | solution.py:209
  47.0 7.3 %collective-permute-start.24 = (bf16[96,512]{1,0:T(8,128)(2,1)S(1)}, bf16[96,512]{1,0:T(8,128)(2,1)S(1)}, u32[]{:S(2)}, u32[]{:S(2)}) collective-permute-start(bf16[96,512]{1,0:T(8,128)(2,1)S(1)} %shard_map.119.refs_0_), channel_id=1, source_target_pairs={{0,1},{1,0},{2,3},{3,2},{4,5},{5,4},{6,7},{7,6},{8,9},{9,8},{10,11... | collective-permute-start | bytes 294920 | tf_op jit(solution)/shard_map/ppermute | solution.py:209
  50.0 7.3 %collective-permute-start.18 = (bf16[96,512]{1,0:T(8,128)(2,1)S(1)}, bf16[96,512]{1,0:T(8,128)(2,1)S(1)}, u32[]{:S(2)}, u32[]{:S(2)}) collective-permute-start(bf16[96,512]{1,0:T(8,128)(2,1)S(1)} %shard_map.116.refs_0_), channel_id=1, source_target_pairs={{0,2},{1,3},{2,0},{3,1},{4,6},{5,7},{6,4},{7,5},{8,10},{9,11},{10,... | collective-permute-start | bytes 294920 | tf_op jit(solution)/shard_map/ppermute | solution.py:209
  52.0 15.2 %collective-permute-start.12 = (bf16[4,48,512]{2,1,0:T(8,128)(2,1)S(1)}, bf16[4,48,512]{2,1,0:T(8,128)(2,1)S(1)}, u32[]{:S(2)}, u32[]{:S(2)}) collective-permute-start(bf16[4,48,512]{2,1,0:T(8,128)(2,1)S(1)} %get-tuple-element.34), channel_id=1, source_target_pairs={{0,4},{4,0},{8,12},{12,8},{16,20},{20,16},{24,28},{28,24},{1,5},{5... | collective-permute-start | bytes 589832 | tf_op jit(solution)/shard_map/ppermute | solution.py:209
  52.8 15.4 %collective-permute-start.13 = (bf16[4,48,512]{2,1,0:T(8,128)(2,1)S(1)}, bf16[4,48,512]{2,1,0:T(8,128)(2,1)S(1)}, u32[]{:S(2)}, u32[]{:S(2)}) collective-permute-start(bf16[4,48,512]{2,1,0:T(8,128)(2,1)S(1)} %get-tuple-element.35), channel_id=1, source_target_pairs={{0,8},{4,12},{8,0},{12,4},{16,24},{20,28},{24,16},{28,20},{1,9},{5... | collective-permute-start | bytes 589832 | tf_op jit(solution)/shard_map/ppermute | solution.py:209
  56.2 8.4 %collective-permute-start.25 = (bf16[96,512]{1,0:T(8,128)(2,1)S(1)}, bf16[96,512]{1,0:T(8,128)(2,1)S(1)}, u32[]{:S(2)}, u32[]{:S(2)}) collective-permute-start(bf16[96,512]{1,0:T(8,128)(2,1)S(1)} %shard_map.119.refs_0_), channel_id=1, source_target_pairs={{0,2},{1,3},{2,0},{3,1},{4,6},{5,7},{6,4},{7,5},{8,10},{9,11},{10,... | collective-permute-start | bytes 294920 | tf_op jit(solution)/shard_map/ppermute | solution.py:209
  57.3 8.9 %collective-permute-start.26 = (bf16[96,512]{1,0:T(8,128)(2,1)S(1)}, bf16[96,512]{1,0:T(8,128)(2,1)S(1)}, u32[]{:S(2)}, u32[]{:S(2)}) collective-permute-start(bf16[96,512]{1,0:T(8,128)(2,1)S(1)} %shard_map.119.refs_0_), channel_id=1, source_target_pairs={{0,3},{1,2},{2,1},{3,0},{4,7},{5,6},{6,5},{7,4},{8,11},{9,10},{10,... | collective-permute-start | bytes 294920 | tf_op jit(solution)/shard_map/ppermute | solution.py:209
  60.9 9.7 %collective-permute-start.14 = (bf16[4,48,512]{2,1,0:T(8,128)(2,1)S(1)}, bf16[4,48,512]{2,1,0:T(8,128)(2,1)S(1)}, u32[]{:S(2)}, u32[]{:S(2)}) collective-permute-start(bf16[4,48,512]{2,1,0:T(8,128)(2,1)S(1)} %get-tuple-element.36), channel_id=1, source_target_pairs={{0,12},{4,8},{8,4},{12,0},{16,28},{20,24},{24,20},{28,16},{1,13},{... | collective-permute-start | bytes 589832 | tf_op jit(solution)/shard_map/ppermute | solution.py:209
  64.6 23.5 %collective-permute-start.20 = (bf16[4,48,512]{2,1,0:T(8,128)(2,1)S(1)}, bf16[4,48,512]{2,1,0:T(8,128)(2,1)S(1)}, u32[]{:S(2)}, u32[]{:S(2)}) collective-permute-start(bf16[4,48,512]{2,1,0:T(8,128)(2,1)S(1)} %get-tuple-element.40), channel_id=1, source_target_pairs={{0,16},{4,20},{8,24},{12,28},{16,0},{20,4},{24,8},{28,12},{1,17},{... | collective-permute-start | bytes 589832 | tf_op jit(solution)/shard_map/ppermute | solution.py:209
  66.2 26.1 %collective-permute-start.21 = (bf16[4,48,512]{2,1,0:T(8,128)(2,1)S(1)}, bf16[4,48,512]{2,1,0:T(8,128)(2,1)S(1)}, u32[]{:S(2)}, u32[]{:S(2)}) collective-permute-start(bf16[4,48,512]{2,1,0:T(8,128)(2,1)S(1)} %get-tuple-element.41), channel_id=1, source_target_pairs={{0,20},{4,16},{8,28},{12,24},{16,4},{20,0},{24,12},{28,8},{1,21},{... | collective-permute-start | bytes 589832 | tf_op jit(solution)/shard_map/ppermute | solution.py:209
  67.3 30.4 %collective-permute-start.27 = (bf16[4,48,512]{2,1,0:T(8,128)(2,1)S(1)}, bf16[4,48,512]{2,1,0:T(8,128)(2,1)S(1)}, u32[]{:S(2)}, u32[]{:S(2)}) collective-permute-start(bf16[4,48,512]{2,1,0:T(8,128)(2,1)S(1)} %get-tuple-element.45), channel_id=1, source_target_pairs={{0,24},{4,28},{8,16},{12,20},{16,8},{20,12},{24,0},{28,4},{1,25},{... | collective-permute-start | bytes 589832 | tf_op jit(solution)/shard_map/ppermute | solution.py:209
  68.3 33.5 %collective-permute-start.28 = (bf16[4,48,512]{2,1,0:T(8,128)(2,1)S(1)}, bf16[4,48,512]{2,1,0:T(8,128)(2,1)S(1)}, u32[]{:S(2)}, u32[]{:S(2)}) collective-permute-start(bf16[4,48,512]{2,1,0:T(8,128)(2,1)S(1)} %get-tuple-element.46), channel_id=1, source_target_pairs={{0,28},{4,24},{8,20},{12,16},{16,12},{20,8},{24,4},{28,0},{1,29},{... | collective-permute-start | bytes 589832 | tf_op jit(solution)/shard_map/ppermute | solution.py:209
  (18 other events, 92.5 us)
where the time goes:
time: 111 us
  waiting for transfers between devices  59.5 us (54%)
  starting transfers between devices  32.8 us (30%)
  Pallas kernels  12.1 us (11%)
  local copies, waits for them, and re-layouts  5.62 us (5%)
    ppermute x32, waiting for transfers between devices, swap(): return lax.ppermute(array, axis, [(s, s ^ k) for s in range(size)])  59.5 us
    ppermute x32, starting transfers between devices, swap(): return lax.ppermute(array, axis, [(s, s ^ k) for s in range(size)])  32.8 us
    pallas_call x14, Pallas kernels, call(): pl.pallas_call(kernel, out_shape=outs, in_specs=specs, out_specs=[VMEM] *...  12.1 us
    unnamed x20, local copies, waits for them, and re-layouts  5.62 us
  transfers between devices with their start and end apart: 32, of which 16 were waited for; matrix products, arithmetic and copies ran while one was open for 1% of the time, Pallas kernels for 8%

commit v1 on v0

--- a/solution.py
+++ b/solution.py
@@ -12,6 +12,7 @@
 SMEM = pl.BlockSpec(memory_space=pltpu.SMEM)
 HBM = pl.BlockSpec(memory_space=pltpu.HBM)
 F32 = jnp.float32
+SPARE = 10800000
 BF16 = jnp.bfloat16
 
 
@@ -19,12 +20,13 @@
     return jnp.dot(a, b, preferred_element_type=F32)
 
 
-def call(kernel, outs, inputs, flops, scalars=0, far=(), scratch=()):
+def call(kernel, outs, inputs, flops, scalars=0, far=(), scratch=(), spare=None):
     moved = sum(a.size * a.dtype.itemsize for a in inputs)
     moved += sum(o.size * o.dtype.itemsize for o in outs)
     specs = [SMEM] * scalars + [VMEM] * (len(inputs) - scalars)
     for i in far:
         specs[i] = HBM
+    limit = 40 * 1024 * 1024 if spare is None else 67043328 - spare
     return pl.pallas_call(
         kernel,
         out_shape=outs,
@@ -32,7 +34,7 @@
         out_specs=[VMEM] * len(outs),
         scratch_shapes=scratch,
         cost_estimate=pl.CostEstimate(flops=flops, bytes_accessed=moved, transcendentals=0),
-        compiler_params=pltpu.CompilerParams(vmem_limit_bytes=40 * 1024 * 1024),
+        compiler_params=pltpu.CompilerParams(vmem_limit_bytes=limit),
     )(*inputs)
 
 
@@ -53,18 +55,18 @@
     return (gate_part / (1.0 + jnp.exp(-gate_part)) * up_part).astype(BF16)
 
 
+def normalize(values, gain):
+    values = values.astype(F32)
+    inverse = lax.rsqrt(jnp.mean(values * values, axis=1, keepdims=True) + 1e-06)
+    return (values * inverse * gain).astype(BF16)
+
+
 def prepare_kernel(experts, capacity, me, *refs):
-    normed, pieces = refs[3], refs[4 : 4 + experts]
-    tokens, gain, routes, sems = refs[4 + experts :]
-    copies = fetch(refs[:3], (tokens, gain, routes), sems)
-    copies[0].wait()
-    values = tokens[...].astype(F32)
-    inverse = lax.rsqrt(jnp.mean(values * values, axis=1, keepdims=True) + 1e-06)
+    pieces = refs[2 : 2 + experts]
+    tokens, routes, sems = refs[2 + experts :]
+    copies = fetch(refs[:2], (tokens, routes), sems)
     copies[1].wait()
-    rows = (values * inverse * gain[...]).astype(BF16)
-    normed[...] = rows
-    copies[2].wait()
-    count = values.shape[0]
+    count = tokens.shape[0]
     index = lax.broadcasted_iota(jnp.int32, (experts, count), 0)
     marks = [index == routes[j : j + 1, :] for j in range(routes.shape[0])]
     marked = functools.reduce(jnp.logical_or, marks)
@@ -76,6 +78,8 @@
     for j, mark in enumerate(marks):
         slot = jnp.sum(jnp.where(mark, before, 0.0), axis=0, keepdims=True)
         places.append((routes[j : j + 1, :] ^ me[0]) * capacity + slot.astype(jnp.int32))
+    copies[0].wait()
+    rows = tokens[...]
     half = experts // 2
     for start in (half, 0):
         at = lax.broadcasted_iota(jnp.int32, (half * capacity, count), 0) + start * capacity
@@ -125,16 +129,19 @@
         copy.wait()
 
 
-def shared_kernel(normed, gate, upward, hidden, both, sems):
+def shared_kernel(tokens, gain, gate, upward, hidden, both, sems):
     inner = gate.shape[1]
-    for copy in fetch((gate, upward), (both.at[:, :inner], both.at[:, inner:]), sems):
+    copies = fetch((gate, upward), (both.at[:, :inner], both.at[:, inner:]), sems)
+    rows = normalize(tokens[...], gain[...])
+    for copy in copies:
         copy.wait()
-    hidden[...] = swiglu(normed[...], both[...])
+    hidden[...] = swiglu(rows, both[...])
 
 
 def hidden_kernel(*refs):
-    rows = jnp.concatenate([r[...] for r in refs[:-2]], axis=0)
-    refs[-1][...] = swiglu(rows, refs[-2][...])
+    gain, both, out = refs[-3:]
+    rows = jnp.concatenate([r[...] for r in refs[:-3]], axis=0)
+    out[...] = swiglu(normalize(rows, gain[...]), both[...])
 
 
 def down_kernel(blocks, units, capacity, *refs):
@@ -172,17 +179,22 @@
         refs[-1][m] = total[m] + weighted(table, refs[:-1], m)
 
 
-def finish_kernel(blocks, total, table, *refs):
+def finish_kernel(blocks, lanes, total, table, *refs):
     returned = refs[:-2]
     moe, squares = refs[-2:]
-    ones = jnp.ones((8, moe.shape[2]), F32)
+    ones = jnp.ones((8, lanes), F32)
     for m in range(blocks):
         rounded = (total[m] + weighted(table, returned, m)).astype(BF16)
         moe[m] = rounded
         wide = rounded.astype(F32)
+        wide = wide * wide
+        folded = functools.reduce(
+            jnp.add,
+            [wide[:, at : at + lanes] for at in range(0, wide.shape[1], lanes)],
+        )
         sums = lax.dot_general(
             ones,
-            wide * wide,
+            folded,
             (((1,), (1,)), ((), ())),
             precision=lax.Precision.HIGHEST,
             preferred_element_type=F32,
@@ -236,19 +248,20 @@
     row = lax.axis_index("ep").astype(jnp.int32).reshape(1)
     column = lax.axis_index("tp").astype(jnp.int32).reshape(1)
     piece = jax.ShapeDtypeStruct((capacity, width), BF16)
-    normed, *pieces = call(
+    gain = norm_gain[None, :]
+    pieces = call(
         functools.partial(prepare_kernel, experts, capacity),
-        [jax.ShapeDtypeStruct((count, width), BF16)] + [piece] * experts,
-        [row, tokens, norm_gain[None, :], routes.T],
+        [piece] * experts,
+        [row, tokens, routes.T],
         2 * experts * capacity * count * width,
         scalars=1,
-        far=(1, 2, 3),
+        far=(1, 2),
         scratch=[
             pltpu.VMEM((count, width), BF16),
-            pltpu.VMEM((1, width), F32),
             pltpu.VMEM((top_count, count), jnp.int32),
-            pltpu.SemaphoreType.DMA((3,)),
+            pltpu.SemaphoreType.DMA((2,)),
         ],
+        spare=experts * capacity * width * 2 + SPARE,
     )
     half, quarter = experts // 2, experts // 4
     arrived = [pieces[0]] + [swap(pieces[k], "ep", k) for k in range(1, experts)]
@@ -260,7 +273,7 @@
     (weights,) = call(
         stage_kernel,
         [both],
-        [expert_gate[0], expert_up[0], normed],
+        [expert_gate[0], expert_up[0], pieces[0]],
         count * width,
         far=(0, 1, 2),
         scratch=[pltpu.SemaphoreType.DMA((2,))],
@@ -268,9 +281,9 @@
     (shared,) = call(
         shared_kernel,
         [jax.ShapeDtypeStruct((count, inner), BF16)],
-        [normed, shared_gate, shared_up],
+        [tokens, gain, shared_gate, shared_up],
         4 * count * width * inner,
-        far=(1, 2),
+        far=(2, 3),
         scratch=[pltpu.VMEM(both.shape, BF16), pltpu.SemaphoreType.DMA((2,))],
     )
     shared = spread(shared)
@@ -291,7 +304,7 @@
         (hidden,) = call(
             hidden_kernel,
             [jax.ShapeDtypeStruct((rows, inner), BF16)],
-            arrived[first : first + size] + [weights],
+            arrived[first : first + size] + [gain, weights],
             4 * rows * width * inner,
         )
         results = call(
@@ -319,7 +332,7 @@
         2 * blocks * count * local * 3 * quarter * capacity,
     )
     moe, squares = call(
-        functools.partial(finish_kernel, blocks),
+        functools.partial(finish_kernel, blocks, 128),
         [
             jax.ShapeDtypeStruct((blocks, count, local), BF16),
             jax.ShapeDtypeStruct((blocks, count), F32),

time: 111 us -> 110 us (level)
  the two profiles are of different devices: /device:TPU:16 before, /device:TPU:10 now
where the time goes in v1:
time: 110 us; the launch traced here: 109 us
  waiting for transfers between devices  56.6 us (51%)
  starting transfers between devices  33.3 us (30%)
  Pallas kernels  13 us (12%)
  local copies, waits for them, and re-layouts  5.62 us (5%)
    ppermute x32, waiting for transfers between devices, swap(): return lax.ppermute(array, axis, [(s, s ^ k) for s in range(size)])  56.6 us
    ppermute x32, starting transfers between devices, swap(): return lax.ppermute(array, axis, [(s, s ^ k) for s in range(size)])  33.3 us
    pallas_call x14, Pallas kernels, call(): pl.pallas_call(kernel, out_shape=outs, in_specs=specs, out_specs=[VMEM] *...  13 us
    unnamed x20, local copies, waits for them, and re-layouts  5.62 us
  transfers between devices with their start and end apart: 32, of which 15 were waited for; matrix products, arithmetic and copies ran while one was open for 1% of the time, Pallas kernels for 8%

profile of v1, /device:TPU:10, one launch (start us, length us, event | category | flops | bytes accessed | tf_op | source)
XLA Modules:
  0.0 109.4 jit_solution(968500799901653740)
XLA Ops:
  0.7 1.6 %shard_map.111 = (bf16[48,2048]{1,0:T(8,128)(2,1)S(1)}, bf16[48,2048]{1,0:T(8,128)(2,1)S(1)}, bf16[48,2048]{1,0:T(8,128)(2,1)S(1)}, bf16[48,2048]{1,0:T(8,128)(2...) custom-call(s32[1]{0:T(128)} %bitcast.2.me, ...), custom_call_target="tpu_custom_call" | custom-call | flops 201326592 | bytes 2098180 | tf_op jit(solution)/shard_map/pallas_call | solution.py:30
  10.0 1.6 %collective-permute-start.22 = (bf16[48,2048]{1,0:T(8,128)(2,1)S(1)}, bf16[48,2048]{1,0:T(8,128)(2,1)S(1)}, u32[]{:S(2)}, u32[]{:S(2)}) collective-permute-start(bf16[48,2048]{1,0:T(8,128)(2,1)S(1)} %get-tuple-element.41), channel_id=1, source_target_pairs={{0,24},{4,28},{8,16},{12,20},{16,8},{20,12},{24,0},{28,4},{1,25},{... | collective-permute-start | bytes 589832 | tf_op jit(solution)/shard_map/ppermute | solution.py:221
  13.0 1.6 %copy-done = bf16[2048,512]{1,0:T(8,128)(2,1)S(1)} copy-done((bf16[2048,512]{1,0:T(8,128)(2,1)S(1)}, bf16[2048,512]{1,0:T(8,128)(2,1)}, u32[]{:S(2)}) %copy-start) | copy-done | bytes 2097176
  14.6 1.6 %copy-done.1 = bf16[2048,512]{1,0:T(8,128)(2,1)S(1)} copy-done((bf16[2048,512]{1,0:T(8,128)(2,1)S(1)}, bf16[2048,512]{1,0:T(8,128)(2,1)}, u32[]{:S(2)}) %copy-start.1) | copy-done | bytes 2097176
  17.9 1.6 %shard_map.109.refs_0_ = bf16[128,512]{1,0:T(8,128)(2,1)S(1)} custom-call(bf16[128,2048]{1,0:T(8,128)(2,1)S(1)} %copy-done.5, f32[1,2048]{1,0:T(1,128)S(1)} %bitcast.15, bf16[2048,512]{1,0:T(8,128)(2,1)S(1)} %copy-done, bf16[2048,512]{1,0:T(8,128)(2,1)S(1)} %copy-done.1), custom_call_target="tpu_custom_call" | custom-call | flops 536870912 | bytes 4857856 | tf_op jit(solution)/shard_map/pallas_call | solution.py:30
  20.9 3.0 %collective-permute-start.15 = (bf16[48,2048]{1,0:T(8,128)(2,1)S(1)}, bf16[48,2048]{1,0:T(8,128)(2,1)S(1)}, u32[]{:S(2)}, u32[]{:S(2)}) collective-permute-start(bf16[48,2048]{1,0:T(8,128)(2,1)S(1)} %get-tuple-element.36), channel_id=1, source_target_pairs={{0,16},{4,20},{8,24},{12,28},{16,0},{20,4},{24,8},{28,12},{1,17},{... | collective-permute-start | bytes 589832 | tf_op jit(solution)/shard_map/ppermute | solution.py:221
  26.0 1.6 %collective-permute-start.10 = (bf16[192,512]{1,0:T(8,128)(2,1)S(1)}, bf16[192,512]{1,0:T(8,128)(2,1)S(1)}, u32[]{:S(2)}, u32[]{:S(2)}) collective-permute-start(bf16[192,512]{1,0:T(8,128)(2,1)S(1)} %shard_map.113.refs_0_), channel_id=1, source_target_pairs={{0,2},{1,3},{2,0},{3,1},{4,6},{5,7},{6,4},{7,5},{8,10},{9,11},{10,... | collective-permute-start | bytes 589832 | tf_op jit(solution)/shard_map/ppermute | solution.py:221
  27.6 6.0 %collective-permute-done.22.refs_0_ = bf16[48,2048]{1,0:T(8,128)(2,1)S(1)} collective-permute-done((bf16[48,2048]{1,0:T(8,128)(2,1)S(1)}, bf16[48,2048]{1,0:T(8,128)(2,1)S(1)}, u32[]{:S(2)}, u32[]{:S(2)}) %collective-permute-start.22) | collective-permute-done | bytes 196640 | tf_op jit(solution)/shard_map/ppermute | solution.py:221
  33.6 4.4 %collective-permute-done.23.refs_1_ = bf16[48,2048]{1,0:T(8,128)(2,1)S(1)} collective-permute-done((bf16[48,2048]{1,0:T(8,128)(2,1)S(1)}, bf16[48,2048]{1,0:T(8,128)(2,1)S(1)}, u32[]{:S(2)}, u32[]{:S(2)}) %collective-permute-start.23) | collective-permute-done | bytes 196640 | tf_op jit(solution)/shard_map/ppermute | solution.py:221
  39.4 2.7 %collective-permute-done.15.refs_0_ = bf16[48,2048]{1,0:T(8,128)(2,1)S(1)} collective-permute-done((bf16[48,2048]{1,0:T(8,128)(2,1)S(1)}, bf16[48,2048]{1,0:T(8,128)(2,1)S(1)}, u32[]{:S(2)}, u32[]{:S(2)}) %collective-permute-start.15) | collective-permute-done | bytes 196640 | tf_op jit(solution)/shard_map/ppermute | solution.py:221
  42.2 2.5 %collective-permute-done.16.refs_1_ = bf16[48,2048]{1,0:T(8,128)(2,1)S(1)} collective-permute-done((bf16[48,2048]{1,0:T(8,128)(2,1)S(1)}, bf16[48,2048]{1,0:T(8,128)(2,1)S(1)}, u32[]{:S(2)}, u32[]{:S(2)}) %collective-permute-start.16) | collective-permute-done | bytes 196640 | tf_op jit(solution)/shard_map/ppermute | solution.py:221
  53.3 1.8 %collective-permute-start.19 = (bf16[96,512]{1,0:T(8,128)(2,1)S(1)}, bf16[96,512]{1,0:T(8,128)(2,1)S(1)}, u32[]{:S(2)}, u32[]{:S(2)}) collective-permute-start(bf16[96,512]{1,0:T(8,128)(2,1)S(1)} %shard_map.116.refs_0_), channel_id=1, source_target_pairs={{0,3},{1,2},{2,1},{3,0},{4,7},{5,6},{6,5},{7,4},{8,11},{9,10},{10,... | collective-permute-start | bytes 294920 | tf_op jit(solution)/shard_map/ppermute | solution.py:221
  55.7 2.0 %collective-permute-start.26 = (bf16[96,512]{1,0:T(8,128)(2,1)S(1)}, bf16[96,512]{1,0:T(8,128)(2,1)S(1)}, u32[]{:S(2)}, u32[]{:S(2)}) collective-permute-start(bf16[96,512]{1,0:T(8,128)(2,1)S(1)} %shard_map.119.refs_0_), channel_id=1, source_target_pairs={{0,3},{1,2},{2,1},{3,0},{4,7},{5,6},{6,5},{7,4},{8,11},{9,10},{10,... | collective-permute-start | bytes 294920 | tf_op jit(solution)/shard_map/ppermute | solution.py:221
  59.3 3.7 %collective-permute-done.25.refs_2_ = bf16[96,512]{1,0:T(8,128)(2,1)S(1)} collective-permute-done((bf16[96,512]{1,0:T(8,128)(2,1)S(1)}, bf16[96,512]{1,0:T(8,128)(2,1)S(1)}, u32[]{:S(2)}, u32[]{:S(2)}) %collective-permute-start.25) | collective-permute-done | bytes 98336 | tf_op jit(solution)/shard_map/ppermute | solution.py:221
  63.0 2.2 %collective-permute-start.20 = (bf16[4,48,512]{2,1,0:T(8,128)(2,1)S(1)}, bf16[4,48,512]{2,1,0:T(8,128)(2,1)S(1)}, u32[]{:S(2)}, u32[]{:S(2)}) collective-permute-start(bf16[4,48,512]{2,1,0:T(8,128)(2,1)S(1)} %get-tuple-element.38), channel_id=1, source_target_pairs={{0,16},{4,20},{8,24},{12,28},{16,0},{20,4},{24,8},{28,12},{1,17},{... | collective-permute-start | bytes 589832 | tf_op jit(solution)/shard_map/ppermute | solution.py:221
  65.6 1.6 %collective-permute-start.27 = (bf16[4,48,512]{2,1,0:T(8,128)(2,1)S(1)}, bf16[4,48,512]{2,1,0:T(8,128)(2,1)S(1)}, u32[]{:S(2)}, u32[]{:S(2)}) collective-permute-start(bf16[4,48,512]{2,1,0:T(8,128)(2,1)S(1)} %get-tuple-element.43), channel_id=1, source_target_pairs={{0,24},{4,28},{8,16},{12,20},{16,8},{20,12},{24,0},{28,4},{1,25},{... | collective-permute-start | bytes 589832 | tf_op jit(solution)/shard_map/ppermute | solution.py:221
  69.8 16.9 %collective-permute-done.20.refs_0_ = bf16[4,48,512]{2,1,0:T(8,128)(2,1)S(1)} collective-permute-done((bf16[4,48,512]{2,1,0:T(8,128)(2,1)S(1)}, bf16[4,48,512]{2,1,0:T(8,128)(2,1)S(1)}, u32[]{:S(2)}, u32[]{:S(2)}) %collective-permute-start.20) | collective-permute-done | bytes 196640 | tf_op jit(solution)/shard_map/ppermute | solution.py:221
  86.7 4.2 %collective-permute-done.21.refs_1_ = bf16[4,48,512]{2,1,0:T(8,128)(2,1)S(1)} collective-permute-done((bf16[4,48,512]{2,1,0:T(8,128)(2,1)S(1)}, bf16[4,48,512]{2,1,0:T(8,128)(2,1)S(1)}, u32[]{:S(2)}, u32[]{:S(2)}) %collective-permute-start.21) | collective-permute-done | bytes 196640 | tf_op jit(solution)/shard_map/ppermute | solution.py:221
  91.5 5.0 %collective-permute-done.27.refs_0_ = bf16[4,48,512]{2,1,0:T(8,128)(2,1)S(1)} collective-permute-done((bf16[4,48,512]{2,1,0:T(8,128)(2,1)S(1)}, bf16[4,48,512]{2,1,0:T(8,128)(2,1)S(1)}, u32[]{:S(2)}, u32[]{:S(2)}) %collective-permute-start.27) | collective-permute-done | bytes 196640 | tf_op jit(solution)/shard_map/ppermute | solution.py:221
  96.4 2.6 %collective-permute-done.28.refs_1_ = bf16[4,48,512]{2,1,0:T(8,128)(2,1)S(1)} collective-permute-done((bf16[4,48,512]{2,1,0:T(8,128)(2,1)S(1)}, bf16[4,48,512]{2,1,0:T(8,128)(2,1)S(1)}, u32[]{:S(2)}, u32[]{:S(2)}) %collective-permute-start.28) | collective-permute-done | bytes 196640 | tf_op jit(solution)/shard_map/ppermute | solution.py:221
  100.3 1.8 %collective-permute-start.29 = (f32[4,128]{1,0:T(4,128)S(1)}, f32[4,128]{1,0:T(4,128)S(1)}, u32[]{:S(2)}, u32[]{:S(2)}) collective-permute-start(f32[4,128]{1,0:T(4,128)S(1)} %get-tuple-element.46.refs_0_), channel_id=1, source_target_pairs={{0,1},{1,0},{2,3},{3,2},{4,5},{5,4},{6,7},{7,6},{8,9},{9,8},{10,11... | collective-permute-start | bytes 6152 | tf_op jit(solution)/shard_map/ppermute | solution.py:221
  102.0 1.8 %collective-permute-start.30 = (f32[4,128]{1,0:T(4,128)S(1)}, f32[4,128]{1,0:T(4,128)S(1)}, u32[]{:S(2)}, u32[]{:S(2)}) collective-permute-start(f32[4,128]{1,0:T(4,128)S(1)} %get-tuple-element.46.refs_0_), channel_id=1, source_target_pairs={{0,2},{1,3},{2,0},{3,1},{4,6},{5,7},{6,4},{7,5},{8,10},{9,11},{10,... | collective-permute-start | bytes 6152 | tf_op jit(solution)/shard_map/ppermute | solution.py:221
  103.9 1.7 %collective-permute-done.30.refs_2_ = f32[4,128]{1,0:T(4,128)S(1)} collective-permute-done((f32[4,128]{1,0:T(4,128)S(1)}, f32[4,128]{1,0:T(4,128)S(1)}, u32[]{:S(2)}, u32[]{:S(2)}) %collective-permute-start.30) | collective-permute-done | bytes 2080 | tf_op jit(solution)/shard_map/ppermute | solution.py:221
  105.6 2.7 %collective-permute-done.31.refs_3_ = f32[4,128]{1,0:T(4,128)S(1)} collective-permute-done((f32[4,128]{1,0:T(4,128)S(1)}, f32[4,128]{1,0:T(4,128)S(1)}, u32[]{:S(2)}, u32[]{:S(2)}) %collective-permute-start.31) | collective-permute-done | bytes 2080 | tf_op jit(solution)/shard_map/ppermute | solution.py:221
  (76 shorter events, 33.1 us)
Async XLA Ops:
  2.3 17.3 %collective-permute-start.6 = (bf16[48,2048]{1,0:T(8,128)(2,1)S(1)}, bf16[48,2048]{1,0:T(8,128)(2,1)S(1)}, u32[]{:S(2)}, u32[]{:S(2)}) collective-permute-start(bf16[48,2048]{1,0:T(8,128)(2,1)S(1)} %get-tuple-element.28), channel_id=1, source_target_pairs={{0,4},{4,0},{8,12},{12,8},{16,20},{20,16},{24,28},{28,24},{1,5},{5... | collective-permute-start | bytes 589832 | tf_op jit(solution)/shard_map/ppermute | solution.py:221
  2.4 18.5 %collective-permute-start.7 = (bf16[48,2048]{1,0:T(8,128)(2,1)S(1)}, bf16[48,2048]{1,0:T(8,128)(2,1)S(1)}, u32[]{:S(2)}, u32[]{:S(2)}) collective-permute-start(bf16[48,2048]{1,0:T(8,128)(2,1)S(1)} %get-tuple-element.29), channel_id=1, source_target_pairs={{0,8},{4,12},{8,0},{12,4},{16,24},{20,28},{24,16},{28,20},{1,9},{5... | collective-permute-start | bytes 589832 | tf_op jit(solution)/shard_map/ppermute | solution.py:221
  2.9 21.0 %collective-permute-start.8 = (bf16[48,2048]{1,0:T(8,128)(2,1)S(1)}, bf16[48,2048]{1,0:T(8,128)(2,1)S(1)}, u32[]{:S(2)}, u32[]{:S(2)}) collective-permute-start(bf16[48,2048]{1,0:T(8,128)(2,1)S(1)} %get-tuple-element.30), channel_id=1, source_target_pairs={{0,12},{4,8},{8,4},{12,0},{16,28},{20,24},{24,20},{28,16},{1,13},{... | collective-permute-start | bytes 589832 | tf_op jit(solution)/shard_map/ppermute | solution.py:221
  10.0 23.6 %collective-permute-start.22 = (bf16[48,2048]{1,0:T(8,128)(2,1)S(1)}, bf16[48,2048]{1,0:T(8,128)(2,1)S(1)}, u32[]{:S(2)}, u32[]{:S(2)}) collective-permute-start(bf16[48,2048]{1,0:T(8,128)(2,1)S(1)} %get-tuple-element.41), channel_id=1, source_target_pairs={{0,24},{4,28},{8,16},{12,20},{16,8},{20,12},{24,0},{28,4},{1,25},{... | collective-permute-start | bytes 589832 | tf_op jit(solution)/shard_map/ppermute | solution.py:221
  13.0 24.9 %collective-permute-start.23 = (bf16[48,2048]{1,0:T(8,128)(2,1)S(1)}, bf16[48,2048]{1,0:T(8,128)(2,1)S(1)}, u32[]{:S(2)}, u32[]{:S(2)}) collective-permute-start(bf16[48,2048]{1,0:T(8,128)(2,1)S(1)} %get-tuple-element.42), channel_id=1, source_target_pairs={{0,28},{4,24},{8,20},{12,16},{16,12},{20,8},{24,4},{28,0},{1,29},{... | collective-permute-start | bytes 589832 | tf_op jit(solution)/shard_map/ppermute | solution.py:221
  19.6 6.4 %collective-permute-start = (bf16[128,512]{1,0:T(8,128)(2,1)S(1)}, bf16[128,512]{1,0:T(8,128)(2,1)S(1)}, u32[]{:S(2)}, u32[]{:S(2)}) collective-permute-start(bf16[128,512]{1,0:T(8,128)(2,1)S(1)} %shard_map.109.refs_0_), channel_id=1, source_target_pairs={{0,1},{1,0},{2,3},{3,2},{4,5},{5,4},{6,7},{7,6},{8,9},{9,8},{10,11... | collective-permute-start | bytes 393224 | tf_op jit(solution)/shard_map/ppermute | solution.py:221
  20.9 21.3 %collective-permute-start.15 = (bf16[48,2048]{1,0:T(8,128)(2,1)S(1)}, bf16[48,2048]{1,0:T(8,128)(2,1)S(1)}, u32[]{:S(2)}, u32[]{:S(2)}) collective-permute-start(bf16[48,2048]{1,0:T(8,128)(2,1)S(1)} %get-tuple-element.36), channel_id=1, source_target_pairs={{0,16},{4,20},{8,24},{12,28},{16,0},{20,4},{24,8},{28,12},{1,17},{... | collective-permute-start | bytes 589832 | tf_op jit(solution)/shard_map/ppermute | solution.py:221
  23.9 20.8 %collective-permute-start.16 = (bf16[48,2048]{1,0:T(8,128)(2,1)S(1)}, bf16[48,2048]{1,0:T(8,128)(2,1)S(1)}, u32[]{:S(2)}, u32[]{:S(2)}) collective-permute-start(bf16[48,2048]{1,0:T(8,128)(2,1)S(1)} %get-tuple-element.37), channel_id=1, source_target_pairs={{0,20},{4,16},{8,28},{12,24},{16,4},{20,0},{24,12},{28,8},{1,21},{... | collective-permute-start | bytes 589832 | tf_op jit(solution)/shard_map/ppermute | solution.py:221
  26.0 21.0 %collective-permute-start.10 = (bf16[192,512]{1,0:T(8,128)(2,1)S(1)}, bf16[192,512]{1,0:T(8,128)(2,1)S(1)}, u32[]{:S(2)}, u32[]{:S(2)}) collective-permute-start(bf16[192,512]{1,0:T(8,128)(2,1)S(1)} %shard_map.113.refs_0_), channel_id=1, source_target_pairs={{0,2},{1,3},{2,0},{3,1},{4,6},{5,7},{6,4},{7,5},{8,10},{9,11},{10,... | collective-permute-start | bytes 589832 | tf_op jit(solution)/shard_map/ppermute | solution.py:221
  33.6 15.0 %collective-permute-start.11 = (bf16[192,512]{1,0:T(8,128)(2,1)S(1)}, bf16[192,512]{1,0:T(8,128)(2,1)S(1)}, u32[]{:S(2)}, u32[]{:S(2)}) collective-permute-start(bf16[192,512]{1,0:T(8,128)(2,1)S(1)} %shard_map.113.refs_0_), channel_id=1, source_target_pairs={{0,3},{1,2},{2,1},{3,0},{4,7},{5,6},{6,5},{7,4},{8,11},{9,10},{10,... | collective-permute-start | bytes 589832 | tf_op jit(solution)/shard_map/ppermute | solution.py:221
  38.0 12.2 %collective-permute-start.9 = (bf16[192,512]{1,0:T(8,128)(2,1)S(1)}, bf16[192,512]{1,0:T(8,128)(2,1)S(1)}, u32[]{:S(2)}, u32[]{:S(2)}) collective-permute-start(bf16[192,512]{1,0:T(8,128)(2,1)S(1)} %shard_map.113.refs_0_), channel_id=1, source_target_pairs={{0,1},{1,0},{2,3},{3,2},{4,5},{5,4},{6,7},{7,6},{8,9},{9,8},{10,11... | collective-permute-start | bytes 589832 | tf_op jit(solution)/shard_map/ppermute | solution.py:221
  42.2 10.0 %collective-permute-start.1 = (bf16[128,512]{1,0:T(8,128)(2,1)S(1)}, bf16[128,512]{1,0:T(8,128)(2,1)S(1)}, u32[]{:S(2)}, u32[]{:S(2)}) collective-permute-start(bf16[128,512]{1,0:T(8,128)(2,1)S(1)} %shard_map.109.refs_0_), channel_id=1, source_target_pairs={{0,2},{1,3},{2,0},{3,1},{4,6},{5,7},{6,4},{7,5},{8,10},{9,11},{10,... | collective-permute-start | bytes 393224 | tf_op jit(solution)/shard_map/ppermute | solution.py:221
  44.6 7.6 %collective-permute-start.2 = (bf16[128,512]{1,0:T(8,128)(2,1)S(1)}, bf16[128,512]{1,0:T(8,128)(2,1)S(1)}, u32[]{:S(2)}, u32[]{:S(2)}) collective-permute-start(bf16[128,512]{1,0:T(8,128)(2,1)S(1)} %shard_map.109.refs_0_), channel_id=1, source_target_pairs={{0,3},{1,2},{2,1},{3,0},{4,7},{5,6},{6,5},{7,4},{8,11},{9,10},{10,... | collective-permute-start | bytes 393224 | tf_op jit(solution)/shard_map/ppermute | solution.py:221
  47.0 6.3 %collective-permute-start.24 = (bf16[96,512]{1,0:T(8,128)(2,1)S(1)}, bf16[96,512]{1,0:T(8,128)(2,1)S(1)}, u32[]{:S(2)}, u32[]{:S(2)}) collective-permute-start(bf16[96,512]{1,0:T(8,128)(2,1)S(1)} %shard_map.119.refs_0_), channel_id=1, source_target_pairs={{0,1},{1,0},{2,3},{3,2},{4,5},{5,4},{6,7},{7,6},{8,9},{9,8},{10,11... | collective-permute-start | bytes 294920 | tf_op jit(solution)/shard_map/ppermute | solution.py:221
  48.6 6.6 %collective-permute-start.17 = (bf16[96,512]{1,0:T(8,128)(2,1)S(1)}, bf16[96,512]{1,0:T(8,128)(2,1)S(1)}, u32[]{:S(2)}, u32[]{:S(2)}) collective-permute-start(bf16[96,512]{1,0:T(8,128)(2,1)S(1)} %shard_map.116.refs_0_), channel_id=1, source_target_pairs={{0,1},{1,0},{2,3},{3,2},{4,5},{5,4},{6,7},{7,6},{8,9},{9,8},{10,11... | collective-permute-start | bytes 294920 | tf_op jit(solution)/shard_map/ppermute | solution.py:221
  52.2 13.5 %collective-permute-start.12 = (bf16[4,48,512]{2,1,0:T(8,128)(2,1)S(1)}, bf16[4,48,512]{2,1,0:T(8,128)(2,1)S(1)}, u32[]{:S(2)}, u32[]{:S(2)}) collective-permute-start(bf16[4,48,512]{2,1,0:T(8,128)(2,1)S(1)} %get-tuple-element.32), channel_id=1, source_target_pairs={{0,4},{4,0},{8,12},{12,8},{16,20},{20,16},{24,28},{28,24},{1,5},{5... | collective-permute-start | bytes 589832 | tf_op jit(solution)/shard_map/ppermute | solution.py:221
  52.3 15.0 %collective-permute-start.13 = (bf16[4,48,512]{2,1,0:T(8,128)(2,1)S(1)}, bf16[4,48,512]{2,1,0:T(8,128)(2,1)S(1)}, u32[]{:S(2)}, u32[]{:S(2)}) collective-permute-start(bf16[4,48,512]{2,1,0:T(8,128)(2,1)S(1)} %get-tuple-element.33), channel_id=1, source_target_pairs={{0,8},{4,12},{8,0},{12,4},{16,24},{20,28},{24,16},{28,20},{1,9},{5... | collective-permute-start | bytes 589832 | tf_op jit(solution)/shard_map/ppermute | solution.py:221
  55.2 7.8 %collective-permute-start.25 = (bf16[96,512]{1,0:T(8,128)(2,1)S(1)}, bf16[96,512]{1,0:T(8,128)(2,1)S(1)}, u32[]{:S(2)}, u32[]{:S(2)}) collective-permute-start(bf16[96,512]{1,0:T(8,128)(2,1)S(1)} %shard_map.119.refs_0_), channel_id=1, source_target_pairs={{0,2},{1,3},{2,0},{3,1},{4,6},{5,7},{6,4},{7,5},{8,10},{9,11},{10,... | collective-permute-start | bytes 294920 | tf_op jit(solution)/shard_map/ppermute | solution.py:221
  55.7 9.5 %collective-permute-start.26 = (bf16[96,512]{1,0:T(8,128)(2,1)S(1)}, bf16[96,512]{1,0:T(8,128)(2,1)S(1)}, u32[]{:S(2)}, u32[]{:S(2)}) collective-permute-start(bf16[96,512]{1,0:T(8,128)(2,1)S(1)} %shard_map.119.refs_0_), channel_id=1, source_target_pairs={{0,3},{1,2},{2,1},{3,0},{4,7},{5,6},{6,5},{7,4},{8,11},{9,10},{10,... | collective-permute-start | bytes 294920 | tf_op jit(solution)/shard_map/ppermute | solution.py:221
  58.9 10.0 %collective-permute-start.14 = (bf16[4,48,512]{2,1,0:T(8,128)(2,1)S(1)}, bf16[4,48,512]{2,1,0:T(8,128)(2,1)S(1)}, u32[]{:S(2)}, u32[]{:S(2)}) collective-permute-start(bf16[4,48,512]{2,1,0:T(8,128)(2,1)S(1)} %get-tuple-element.34), channel_id=1, source_target_pairs={{0,12},{4,8},{8,4},{12,0},{16,28},{20,24},{24,20},{28,16},{1,13},{... | collective-permute-start | bytes 589832 | tf_op jit(solution)/shard_map/ppermute | solution.py:221
  63.0 23.7 %collective-permute-start.20 = (bf16[4,48,512]{2,1,0:T(8,128)(2,1)S(1)}, bf16[4,48,512]{2,1,0:T(8,128)(2,1)S(1)}, u32[]{:S(2)}, u32[]{:S(2)}) collective-permute-start(bf16[4,48,512]{2,1,0:T(8,128)(2,1)S(1)} %get-tuple-element.38), channel_id=1, source_target_pairs={{0,16},{4,20},{8,24},{12,28},{16,0},{20,4},{24,8},{28,12},{1,17},{... | collective-permute-start | bytes 589832 | tf_op jit(solution)/shard_map/ppermute | solution.py:221
  65.2 25.7 %collective-permute-start.21 = (bf16[4,48,512]{2,1,0:T(8,128)(2,1)S(1)}, bf16[4,48,512]{2,1,0:T(8,128)(2,1)S(1)}, u32[]{:S(2)}, u32[]{:S(2)}) collective-permute-start(bf16[4,48,512]{2,1,0:T(8,128)(2,1)S(1)} %get-tuple-element.39), channel_id=1, source_target_pairs={{0,20},{4,16},{8,28},{12,24},{16,4},{20,0},{24,12},{28,8},{1,21},{... | collective-permute-start | bytes 589832 | tf_op jit(solution)/shard_map/ppermute | solution.py:221
  65.6 30.8 %collective-permute-start.27 = (bf16[4,48,512]{2,1,0:T(8,128)(2,1)S(1)}, bf16[4,48,512]{2,1,0:T(8,128)(2,1)S(1)}, u32[]{:S(2)}, u32[]{:S(2)}) collective-permute-start(bf16[4,48,512]{2,1,0:T(8,128)(2,1)S(1)} %get-tuple-element.43), channel_id=1, source_target_pairs={{0,24},{4,28},{8,16},{12,20},{16,8},{20,12},{24,0},{28,4},{1,25},{... | collective-permute-start | bytes 589832 | tf_op jit(solution)/shard_map/ppermute | solution.py:221
  67.2 31.8 %collective-permute-start.28 = (bf16[4,48,512]{2,1,0:T(8,128)(2,1)S(1)}, bf16[4,48,512]{2,1,0:T(8,128)(2,1)S(1)}, u32[]{:S(2)}, u32[]{:S(2)}) collective-permute-start(bf16[4,48,512]{2,1,0:T(8,128)(2,1)S(1)} %get-tuple-element.44), channel_id=1, source_target_pairs={{0,28},{4,24},{8,20},{12,16},{16,12},{20,8},{24,4},{28,0},{1,29},{... | collective-permute-start | bytes 589832 | tf_op jit(solution)/shard_map/ppermute | solution.py:221
  (18 other events, 88.0 us)

commit v2 on v1

--- a/solution.py
+++ b/solution.py
@@ -61,32 +61,42 @@
     return (values * inverse * gain).astype(BF16)
 
 
+def compact(me, routes, rows, pieces, capacity, experts):
+    count = rows.shape[0]
+    index = lax.broadcasted_iota(jnp.int32, (experts, count), 0)
+    marks = [index == route for route in routes]
+    marked = functools.reduce(jnp.logical_or, marks)
+    earlier = lax.broadcasted_iota(jnp.int32, (count, count), 0) < lax.broadcasted_iota(
+        jnp.int32, (count, count), 1
+    )
+    before = dot(marked.astype(BF16), earlier.astype(BF16))
+    places = []
+    for route, mark in zip(routes, marks):
+        slot = jnp.sum(jnp.where(mark, before, 0.0), axis=0, keepdims=True)
+        places.append((route ^ me) * capacity + slot.astype(jnp.int32))
+    values = rows[...]
+    half = experts // 2
+    for start in range(len(pieces) - half, -1, -half):
+        at = lax.broadcasted_iota(jnp.int32, (half * capacity, count), 0) + start * capacity
+        chosen = functools.reduce(jnp.logical_or, [at == place for place in places])
+        moved = dot(chosen.astype(F32).astype(BF16), values).astype(BF16)
+        for k in range(half):
+            pieces[start + k][...] = moved[k * capacity : (k + 1) * capacity]
+
+
 def prepare_kernel(experts, capacity, me, *refs):
     pieces = refs[2 : 2 + experts]
     tokens, routes, sems = refs[2 + experts :]
     copies = fetch(refs[:2], (tokens, routes), sems)
-    copies[1].wait()
-    count = tokens.shape[0]
-    index = lax.broadcasted_iota(jnp.int32, (experts, count), 0)
-    marks = [index == routes[j : j + 1, :] for j in range(routes.shape[0])]
-    marked = functools.reduce(jnp.logical_or, marks)
-    earlier = lax.broadcasted_iota(jnp.int32, (count, count), 0) < lax.broadcasted_iota(
-        jnp.int32, (count, count), 1
-    )
-    before = dot(marked.astype(BF16), earlier.astype(BF16))
-    places = []
-    for j, mark in enumerate(marks):
-        slot = jnp.sum(jnp.where(mark, before, 0.0), axis=0, keepdims=True)
-        places.append((routes[j : j + 1, :] ^ me[0]) * capacity + slot.astype(jnp.int32))
-    copies[0].wait()
-    rows = tokens[...]
-    half = experts // 2
-    for start in (half, 0):
-        at = lax.broadcasted_iota(jnp.int32, (half * capacity, count), 0) + start * capacity
-        chosen = functools.reduce(jnp.logical_or, [at == place for place in places])
-        moved = dot(chosen.astype(F32).astype(BF16), rows).astype(BF16)
-        for k in range(half):
-            pieces[start + k][...] = moved[k * capacity : (k + 1) * capacity]
+    for copy in copies:
+        copy.wait()
+    chosen = [routes[j : j + 1, :] for j in range(routes.shape[0])]
+    compact(me[0], chosen, tokens, pieces, capacity, experts)
+
+
+def relay_kernel(experts, capacity, me, packed, tokens, *pieces):
+    chosen = [packed[j : j + 1, :].astype(jnp.int32) for j in range(packed.shape[0] // 2)]
+    compact(me[0], chosen, tokens, pieces, capacity, experts)
 
 
 def table_kernel(capacity, groups, me, *refs):
@@ -138,9 +148,16 @@
     hidden[...] = swiglu(rows, both[...])
 
 
-def hidden_kernel(*refs):
+def joined(refs, ways, at=Ellipsis):
+    units = []
+    for u in range(0, len(refs), ways):
+        units.append(functools.reduce(jnp.add, [r[at] for r in refs[u : u + ways]]))
+    return jnp.concatenate(units, axis=0)
+
+
+def hidden_kernel(ways, *refs):
     gain, both, out = refs[-3:]
-    rows = jnp.concatenate([r[...] for r in refs[:-3]], axis=0)
+    rows = joined(refs[:-3], ways)
     out[...] = swiglu(normalize(rows, gain[...]), both[...])
 
 
@@ -157,9 +174,8 @@
             outs[u][m] = result[first : first + capacity]
 
 
-def weighted(table, returned, m):
-    rows = jnp.concatenate([r[m] for r in returned], axis=0)
-    parts = dot(table[m], rows)
+def weighted(table, returned, ways, m):
+    parts = dot(table[m], joined(returned, ways, m))
     count = parts.shape[0] // 3
     return parts[:count] + parts[count : 2 * count] + parts[2 * count :]
 
@@ -171,12 +187,12 @@
     shared = dot(jnp.concatenate([h[...] for h in hidden], axis=0), down[...])
     count = out.shape[1]
     for m in range(blocks):
-        out[m] = shared[m * count : (m + 1) * count] + weighted(table, returned, m)
+        out[m] = shared[m * count : (m + 1) * count] + weighted(table, returned, 1, m)
 
 
 def more_kernel(blocks, total, table, *refs):
     for m in range(blocks):
-        refs[-1][m] = total[m] + weighted(table, refs[:-1], m)
+        refs[-1][m] = total[m] + weighted(table, refs[:-1], 2, m)
 
 
 def finish_kernel(blocks, lanes, total, table, *refs):
@@ -184,7 +200,7 @@
     moe, squares = refs[-2:]
     ones = jnp.ones((8, lanes), F32)
     for m in range(blocks):
-        rounded = (total[m] + weighted(table, returned, m)).astype(BF16)
+        rounded = (total[m] + weighted(table, returned, 2, m)).astype(BF16)
         moe[m] = rounded
         wide = rounded.astype(F32)
         wide = wide * wide
@@ -216,9 +232,14 @@
         out[pl.ds(first, count), :] = value.astype(BF16)
 
 
-def swap(array, axis, k):
+def swap(array, axis, k, only=None):
     size = lax.axis_size(axis)
-    return lax.ppermute(array, axis, [(s, s ^ k) for s in range(size)])
+    sources = [s for s in range(size) if only is None or is_inner(s, size) == only]
+    return lax.ppermute(array, axis, [(s, s ^ k) for s in sources])
+
+
+def is_inner(place, size):
+    return size // 4 <= place < size - size // 4
 
 
 def spread(array):
@@ -264,10 +285,27 @@
         spare=experts * capacity * width * 2 + SPARE,
     )
     half, quarter = experts // 2, experts // 4
-    arrived = [pieces[0]] + [swap(pieces[k], "ep", k) for k in range(1, experts)]
+    first, last = range(half, half + quarter), range(half + quarter, experts)
+    packed = jnp.concatenate([routes.T.astype(F32), route_weights.T], axis=0)
+    dense = swap(tokens, "ep", half, only=False)
+    dense_routes = swap(packed, "ep", half, only=False)
+    near = [pieces[0]] + [swap(pieces[k], "ep", k) for k in range(1, half)]
+    direct = {k: swap(pieces[k], "ep", k, only=True) for k in range(half, experts)}
+    relayed = call(
+        functools.partial(relay_kernel, experts, capacity),
+        [piece] * half,
+        [row, dense_routes, dense],
+        2 * half * capacity * count * width,
+        scalars=1,
+    )
+    passed = [relayed[0]]
+    passed += [swap(relayed[k], "ep", k, only=True) for k in range(1, half)]
+    arrived = {
+        "N": near,
+        "A": [direct[k] for u in range(quarter) for k in (last[u], first[u])],
+        "B": [passed[k] for u in range(quarter) for k in (u, quarter + u)],
+    }
     groups = {"N": (0, half), "A": (half, quarter), "B": (half + quarter, quarter)}
-
-    packed = jnp.concatenate([routes.T.astype(F32), route_weights.T], axis=0)
     packed = spread(packed)
     both = jax.ShapeDtypeStruct((width, 2 * inner), BF16)
     (weights,) = call(
@@ -298,25 +336,29 @@
         scalars=1,
     )
 
-    returned = {}
-    for name, (first, size) in groups.items():
+    results = {}
+    for name, (_, size) in groups.items():
         rows = size * capacity
         (hidden,) = call(
-            hidden_kernel,
+            functools.partial(hidden_kernel, len(arrived[name]) // size),
             [jax.ShapeDtypeStruct((rows, inner), BF16)],
-            arrived[first : first + size] + [gain, weights],
+            arrived[name] + [gain, weights],
             4 * rows * width * inner,
         )
-        results = call(
+        results[name] = call(
             functools.partial(down_kernel, blocks, size, capacity),
             [jax.ShapeDtypeStruct((blocks, capacity, local), BF16)] * size,
             spread(hidden) + [expert_down[0]],
             2 * blocks * rows * inner * local,
         )
-        returned[name] = [
-            swap(results[u], "ep", first + u) if first + u else results[u]
-            for u in range(size)
-        ]
+    returned = {"N": [results["N"][0]], "A": [], "B": []}
+    for k in range(1, half):
+        returned["N"].append(swap(results["N"][k], "ep", k))
+    for u in range(quarter):
+        for name, k in (("A", first[u]), ("B", last[u])):
+            for phase in "AB":
+                only = (phase == "A") == (name == "B")
+                returned[name].append(swap(results[phase][u], "ep", k, only=only))
 
     sums = jax.ShapeDtypeStruct((blocks, count, local), F32)
     (total,) = call(

time: 110 us -> 126 us (1.15)
  the two profiles are of different devices: /device:TPU:10 before, /device:TPU:0 now
where the time goes in v2:
time: 126 us
  starting transfers between devices  62.8 us (50%)
  waiting for transfers between devices  44.5 us (35%)
  Pallas kernels  13.7 us (11%)
  local copies, waits for them, and re-layouts  3.88 us (3%)
    ppermute x41, starting transfers between devices, swap(): return lax.ppermute(array, axis, [(s, s ^ k) for s in sources])  62.8 us
    ppermute x41, waiting for transfers between devices, swap(): return lax.ppermute(array, axis, [(s, s ^ k) for s in sources])  44.5 us
    pallas_call x15, Pallas kernels, call(): pl.pallas_call(kernel, out_shape=outs, in_specs=specs, out_specs=[VMEM] *...  13.7 us
    unnamed x20, local copies, waits for them, and re-layouts  3.88 us
  transfers between devices with their start and end apart: 41, of which 17 were waited for; matrix products, arithmetic and copies ran while one was open for 1% of the time, Pallas kernels for 9%

profile of v2, /device:TPU:0, one launch (start us, length us, event | category | flops | bytes accessed | tf_op | source)
XLA Modules:
  0.0 125.9 jit_solution(9173039624865426307)
XLA Ops:
  0.0 6.0 %collective-permute-start.24 = (bf16[128,2048]{1,0:T(8,128)(2,1)}, bf16[128,2048]{1,0:T(8,128)(2,1)S(1)}, u32[]{:S(2)}, u32[]{:S(2)}) collective-permute-start(bf16[128,2048]{1,0:T(8,128)(2,1)} %refs_0_.1), channel_id=1, source_target_pairs={{0,16},{4,20},{24,8},{28,12},{1,17},{5,21},{25,9},{29,13},{2,18},{... | collective-permute-start | bytes 1572872 | tf_op jit(solution)/shard_map/ppermute | solution.py:238
  6.7 1.8 %shard_map.111 = (bf16[48,2048]{1,0:T(8,128)(2,1)S(1)}, bf16[48,2048]{1,0:T(8,128)(2,1)S(1)}, bf16[48,2048]{1,0:T(8,128)(2,1)S(1)}, bf16[48,2048]{1,0:T(8,128)(2...) custom-call(s32[1]{0:T(128)} %bitcast.2.me, ...), custom_call_target="tpu_custom_call" | custom-call | flops 201326592 | bytes 2098180 | tf_op jit(solution)/shard_map/pallas_call | solution.py:30
  11.1 5.4 %collective-permute-start.23 = (f32[4,128]{1,0:T(4,128)S(1)}, f32[4,128]{1,0:T(4,128)S(1)}, u32[]{:S(2)}, u32[]{:S(2)}) collective-permute-start(f32[4,128]{1,0:T(4,128)S(1)} %pad_maximum_fusion.refs_0_), channel_id=1, source_target_pairs={{0,16},{4,20},{24,8},{28,12},{1,17},{5,21},{25,9},{29,13},{2,18},{... | collective-permute-start | bytes 6152 | tf_op jit(solution)/shard_map/ppermute | solution.py:238
  23.1 4.6 %collective-permute-done.16.refs_1_ = bf16[48,2048]{1,0:T(8,128)(2,1)S(1)} collective-permute-done((bf16[48,2048]{1,0:T(8,128)(2,1)S(1)}, bf16[48,2048]{1,0:T(8,128)(2,1)S(1)}, u32[]{:S(2)}, u32[]{:S(2)}) %collective-permute-start.16) | collective-permute-done | bytes 196640 | tf_op jit(solution)/shard_map/ppermute | solution.py:238
  30.8 5.3 %collective-permute-done.18.refs_3_ = bf16[48,2048]{1,0:T(8,128)(2,1)S(1)} collective-permute-done((bf16[48,2048]{1,0:T(8,128)(2,1)S(1)}, bf16[48,2048]{1,0:T(8,128)(2,1)S(1)}, u32[]{:S(2)}, u32[]{:S(2)}) %collective-permute-start.18) | collective-permute-done | bytes 196640 | tf_op jit(solution)/shard_map/ppermute | solution.py:238
  38.0 1.6 %copy-done.3 = bf16[1,2048,512]{2,1,0:T(8,128)(2,1)S(1)} copy-done((bf16[1,2048,512]{2,1,0:T(8,128)(2,1)S(1)}, bf16[1,2048,512]{2,1,0:T(8,128)(2,1)}, u32[]{:S(2)}) %copy-start.3) | copy-done | bytes 2097176
  39.6 1.6 %copy-done.4 = bf16[1,2048,512]{2,1,0:T(8,128)(2,1)S(1)} copy-done((bf16[1,2048,512]{2,1,0:T(8,128)(2,1)S(1)}, bf16[1,2048,512]{2,1,0:T(8,128)(2,1)}, u32[]{:S(2)}) %copy-start.4) | copy-done | bytes 2097176
  42.8 2.5 %collective-permute-start.5 = (f32[4,128]{1,0:T(4,128)S(1)}, f32[4,128]{1,0:T(4,128)S(1)}, u32[]{:S(2)}, u32[]{:S(2)}) collective-permute-start(f32[4,128]{1,0:T(4,128)S(1)} %pad_maximum_fusion.refs_0_), channel_id=1, source_target_pairs={{0,3},{1,2},{2,1},{3,0},{4,7},{5,6},{6,5},{7,4},{8,11},{9,10},{10,... | collective-permute-start | bytes 6152 | tf_op jit(solution)/shard_map/ppermute | solution.py:238
  55.3 5.3 %collective-permute-done.20.refs_2_ = bf16[96,512]{1,0:T(8,128)(2,1)S(1)} collective-permute-done((bf16[96,512]{1,0:T(8,128)(2,1)S(1)}, bf16[96,512]{1,0:T(8,128)(2,1)S(1)}, u32[]{:S(2)}, u32[]{:S(2)}) %collective-permute-start.20) | collective-permute-done | bytes 98336 | tf_op jit(solution)/shard_map/ppermute | solution.py:238
  60.6 1.7 %collective-permute-start.28 = (bf16[96,512]{1,0:T(8,128)(2,1)S(1)}, bf16[96,512]{1,0:T(8,128)(2,1)S(1)}, u32[]{:S(2)}, u32[]{:S(2)}) collective-permute-start(bf16[96,512]{1,0:T(8,128)(2,1)S(1)} %shard_map.119.refs_0_), channel_id=1, source_target_pairs={{0,1},{1,0},{2,3},{3,2},{4,5},{5,4},{6,7},{7,6},{8,9},{9,8},{10,11... | collective-permute-start | bytes 294920 | tf_op jit(solution)/shard_map/ppermute | solution.py:238
  62.3 1.9 %collective-permute-done.21.refs_3_ = bf16[96,512]{1,0:T(8,128)(2,1)S(1)} collective-permute-done((bf16[96,512]{1,0:T(8,128)(2,1)S(1)}, bf16[96,512]{1,0:T(8,128)(2,1)S(1)}, u32[]{:S(2)}, u32[]{:S(2)}) %collective-permute-start.21) | collective-permute-done | bytes 98336 | tf_op jit(solution)/shard_map/ppermute | solution.py:238
  64.5 6.0 %collective-permute-start.22 = (bf16[4,48,512]{2,1,0:T(8,128)(2,1)S(1)}, bf16[4,48,512]{2,1,0:T(8,128)(2,1)S(1)}, u32[]{:S(2)}, u32[]{:S(2)}) collective-permute-start(bf16[4,48,512]{2,1,0:T(8,128)(2,1)S(1)} %get-tuple-element.44), channel_id=1, source_target_pairs={{0,16},{4,20},{24,8},{28,12},{1,17},{5,21},{25,9},{29,13},{2,18},{... | collective-permute-start | bytes 589832 | tf_op jit(solution)/shard_map/ppermute | solution.py:238
  70.5 1.6 %shard_map.109.refs_0_ = bf16[128,512]{1,0:T(8,128)(2,1)S(1)} custom-call(bf16[128,2048]{1,0:T(8,128)(2,1)S(1)} %copy-done.5, f32[1,2048]{1,0:T(1,128)S(1)} %bitcast.18, bf16[2048,512]{1,0:T(8,128)(2,1)S(1)} %copy-done, bf16[2048,512]{1,0:T(8,128)(2,1)S(1)} %copy-done.1), custom_call_target="tpu_custom_call" | custom-call | flops 536870912 | bytes 4857856 | tf_op jit(solution)/shard_map/pallas_call | solution.py:30
  72.4 2.0 %collective-permute-start.1 = (bf16[128,512]{1,0:T(8,128)(2,1)S(1)}, bf16[128,512]{1,0:T(8,128)(2,1)S(1)}, u32[]{:S(2)}, u32[]{:S(2)}) collective-permute-start(bf16[128,512]{1,0:T(8,128)(2,1)S(1)} %shard_map.109.refs_0_), channel_id=1, source_target_pairs={{0,2},{1,3},{2,0},{3,1},{4,6},{5,7},{6,4},{7,5},{8,10},{9,11},{10,... | collective-permute-start | bytes 393224 | tf_op jit(solution)/shard_map/ppermute | solution.py:238
  77.9 3.4 %collective-permute-done.30.refs_3_ = bf16[96,512]{1,0:T(8,128)(2,1)S(1)} collective-permute-done((bf16[96,512]{1,0:T(8,128)(2,1)S(1)}, bf16[96,512]{1,0:T(8,128)(2,1)S(1)}, u32[]{:S(2)}, u32[]{:S(2)}) %collective-permute-start.30) | collective-permute-done | bytes 98336 | tf_op jit(solution)/shard_map/ppermute | solution.py:238
  83.2 1.8 %collective-permute-start.14 = (bf16[4,48,512]{2,1,0:T(8,128)(2,1)S(1)}, bf16[4,48,512]{2,1,0:T(8,128)(2,1)S(1)}, u32[]{:S(2)}, u32[]{:S(2)}) collective-permute-start(bf16[4,48,512]{2,1,0:T(8,128)(2,1)S(1)} %get-tuple-element.38), channel_id=1, source_target_pairs={{0,12},{4,8},{8,4},{12,0},{16,28},{20,24},{24,20},{28,16},{1,13},{... | collective-permute-start | bytes 589832 | tf_op jit(solution)/shard_map/ppermute | solution.py:238
  86.2 1.7 %collective-permute-done.32.refs_2_ = bf16[4,48,512]{2,1,0:T(8,128)(2,1)S(1)} collective-permute-done((bf16[4,48,512]{2,1,0:T(8,128)(2,1)S(1)}, bf16[4,48,512]{2,1,0:T(8,128)(2,1)S(1)}, u32[]{:S(2)}, u32[]{:S(2)}) %collective-permute-start.32) | collective-permute-done | bytes 196640 | tf_op jit(solution)/shard_map/ppermute | solution.py:238
  89.9 9.1 %collective-permute-done.13.refs_8_ = bf16[4,48,512]{2,1,0:T(8,128)(2,1)S(1)} collective-permute-done((bf16[4,48,512]{2,1,0:T(8,128)(2,1)S(1)}, bf16[4,48,512]{2,1,0:T(8,128)(2,1)S(1)}, u32[]{:S(2)}, u32[]{:S(2)}) %collective-permute-start.13) | collective-permute-done | bytes 196640 | tf_op jit(solution)/shard_map/ppermute | solution.py:238
  99.6 2.8 %collective-permute-done.14.refs_9_ = bf16[4,48,512]{2,1,0:T(8,128)(2,1)S(1)} collective-permute-done((bf16[4,48,512]{2,1,0:T(8,128)(2,1)S(1)}, bf16[4,48,512]{2,1,0:T(8,128)(2,1)S(1)}, u32[]{:S(2)}, u32[]{:S(2)}) %collective-permute-start.14) | collective-permute-done | bytes 196640 | tf_op jit(solution)/shard_map/ppermute | solution.py:238
  102.5 3.2 %collective-permute-start.35 = (bf16[4,48,512]{2,1,0:T(8,128)(2,1)S(1)}, bf16[4,48,512]{2,1,0:T(8,128)(2,1)S(1)}, u32[]{:S(2)}, u32[]{:S(2)}) collective-permute-start(bf16[4,48,512]{2,1,0:T(8,128)(2,1)S(1)} %get-tuple-element.49), channel_id=1, source_target_pairs={{0,24},{4,28},{24,0},{28,4},{1,25},{5,29},{25,1},{29,5},{2,26},{6,... | collective-permute-start | bytes 589832 | tf_op jit(solution)/shard_map/ppermute | solution.py:238
  105.7 4.1 %collective-permute-start.37 = (bf16[4,48,512]{2,1,0:T(8,128)(2,1)S(1)}, bf16[4,48,512]{2,1,0:T(8,128)(2,1)S(1)}, u32[]{:S(2)}, u32[]{:S(2)}) collective-permute-start(bf16[4,48,512]{2,1,0:T(8,128)(2,1)S(1)} %get-tuple-element.51), channel_id=1, source_target_pairs={{0,28},{4,24},{24,4},{28,0},{1,29},{5,25},{25,5},{29,1},{2,30},{6,... | collective-permute-start | bytes 589832 | tf_op jit(solution)/shard_map/ppermute | solution.py:238
  113.9 3.0 %collective-permute-done.37.refs_3_ = bf16[4,48,512]{2,1,0:T(8,128)(2,1)S(1)} collective-permute-done((bf16[4,48,512]{2,1,0:T(8,128)(2,1)S(1)}, bf16[4,48,512]{2,1,0:T(8,128)(2,1)S(1)}, u32[]{:S(2)}, u32[]{:S(2)}) %collective-permute-start.37) | collective-permute-done | bytes 196640 | tf_op jit(solution)/shard_map/ppermute | solution.py:238
  118.2 1.8 %collective-permute-start.38 = (f32[4,128]{1,0:T(4,128)S(1)}, f32[4,128]{1,0:T(4,128)S(1)}, u32[]{:S(2)}, u32[]{:S(2)}) collective-permute-start(f32[4,128]{1,0:T(4,128)S(1)} %get-tuple-element.54.refs_0_), channel_id=1, source_target_pairs={{0,1},{1,0},{2,3},{3,2},{4,5},{5,4},{6,7},{7,6},{8,9},{9,8},{10,11... | collective-permute-start | bytes 6152 | tf_op jit(solution)/shard_map/ppermute | solution.py:238
  121.8 1.7 %collective-permute-done.39.refs_2_ = f32[4,128]{1,0:T(4,128)S(1)} collective-permute-done((f32[4,128]{1,0:T(4,128)S(1)}, f32[4,128]{1,0:T(4,128)S(1)}, u32[]{:S(2)}, u32[]{:S(2)}) %collective-permute-start.39) | collective-permute-done | bytes 2080 | tf_op jit(solution)/shard_map/ppermute | solution.py:238
  (95 shorter events, 45.7 us)
Async XLA Ops:
  0.0 27.7 %collective-permute-start.24 = (bf16[128,2048]{1,0:T(8,128)(2,1)}, bf16[128,2048]{1,0:T(8,128)(2,1)S(1)}, u32[]{:S(2)}, u32[]{:S(2)}) collective-permute-start(bf16[128,2048]{1,0:T(8,128)(2,1)} %refs_0_.1), channel_id=1, source_target_pairs={{0,16},{4,20},{24,8},{28,12},{1,17},{5,21},{25,9},{29,13},{2,18},{... | collective-permute-start | bytes 1572872 | tf_op jit(solution)/shard_map/ppermute | solution.py:238
  8.5 14.6 %collective-permute-start.15 = (bf16[48,2048]{1,0:T(8,128)(2,1)S(1)}, bf16[48,2048]{1,0:T(8,128)(2,1)S(1)}, u32[]{:S(2)}, u32[]{:S(2)}) collective-permute-start(bf16[48,2048]{1,0:T(8,128)(2,1)S(1)} %get-tuple-element.40), channel_id=1, source_target_pairs={{8,16},{12,20},{16,8},{20,12},{9,17},{13,21},{17,9},{21,13},{10,18... | collective-permute-start | bytes 589832 | tf_op jit(solution)/shard_map/ppermute | solution.py:238
  9.1 18.6 %collective-permute-start.16 = (bf16[48,2048]{1,0:T(8,128)(2,1)S(1)}, bf16[48,2048]{1,0:T(8,128)(2,1)S(1)}, u32[]{:S(2)}, u32[]{:S(2)}) collective-permute-start(bf16[48,2048]{1,0:T(8,128)(2,1)S(1)} %get-tuple-element.41), channel_id=1, source_target_pairs={{8,24},{12,28},{16,0},{20,4},{9,25},{13,29},{17,1},{21,5},{10,26},... | collective-permute-start | bytes 589832 | tf_op jit(solution)/shard_map/ppermute | solution.py:238
  21.7 14.3 %collective-permute-start.18 = (bf16[48,2048]{1,0:T(8,128)(2,1)S(1)}, bf16[48,2048]{1,0:T(8,128)(2,1)S(1)}, u32[]{:S(2)}, u32[]{:S(2)}) collective-permute-start(bf16[48,2048]{1,0:T(8,128)(2,1)S(1)} %get-tuple-element.43), channel_id=1, source_target_pairs={{8,28},{12,24},{16,4},{20,0},{9,29},{13,25},{17,5},{21,1},{10,30},... | collective-permute-start | bytes 589832 | tf_op jit(solution)/shard_map/ppermute | solution.py:238
  23.0 13.7 %collective-permute-start.6 = (bf16[48,2048]{1,0:T(8,128)(2,1)S(1)}, bf16[48,2048]{1,0:T(8,128)(2,1)S(1)}, u32[]{:S(2)}, u32[]{:S(2)}) collective-permute-start(bf16[48,2048]{1,0:T(8,128)(2,1)S(1)} %get-tuple-element.32), channel_id=1, source_target_pairs={{0,4},{4,0},{8,12},{12,8},{16,20},{20,16},{24,28},{28,24},{1,5},{5... | collective-permute-start | bytes 589832 | tf_op jit(solution)/shard_map/ppermute | solution.py:238
  27.7 15.1 %collective-permute-start.7 = (bf16[48,2048]{1,0:T(8,128)(2,1)S(1)}, bf16[48,2048]{1,0:T(8,128)(2,1)S(1)}, u32[]{:S(2)}, u32[]{:S(2)}) collective-permute-start(bf16[48,2048]{1,0:T(8,128)(2,1)S(1)} %get-tuple-element.33), channel_id=1, source_target_pairs={{0,8},{4,12},{8,0},{12,4},{16,24},{20,28},{24,16},{28,20},{1,9},{5... | collective-permute-start | bytes 589832 | tf_op jit(solution)/shard_map/ppermute | solution.py:238
  27.7 17.6 %collective-permute-start.8 = (bf16[48,2048]{1,0:T(8,128)(2,1)S(1)}, bf16[48,2048]{1,0:T(8,128)(2,1)S(1)}, u32[]{:S(2)}, u32[]{:S(2)}) collective-permute-start(bf16[48,2048]{1,0:T(8,128)(2,1)S(1)} %get-tuple-element.34), channel_id=1, source_target_pairs={{0,12},{4,8},{8,4},{12,0},{16,28},{20,24},{24,20},{28,16},{1,13},{... | collective-permute-start | bytes 589832 | tf_op jit(solution)/shard_map/ppermute | solution.py:238
  29.5 21.4 %collective-permute-start.25 = (bf16[48,2048]{1,0:T(8,128)(2,1)S(1)}, bf16[48,2048]{1,0:T(8,128)(2,1)S(1)}, u32[]{:S(2)}, u32[]{:S(2)}) collective-permute-start(bf16[48,2048]{1,0:T(8,128)(2,1)S(1)} %get-tuple-element.46), channel_id=1, source_target_pairs={{8,0},{12,4},{16,24},{20,28},{9,1},{13,5},{17,25},{21,29},{10,2},{... | collective-permute-start | bytes 589832 | tf_op jit(solution)/shard_map/ppermute | solution.py:238
  36.0 15.9 %collective-permute-start.26 = (bf16[48,2048]{1,0:T(8,128)(2,1)S(1)}, bf16[48,2048]{1,0:T(8,128)(2,1)S(1)}, u32[]{:S(2)}, u32[]{:S(2)}) collective-permute-start(bf16[48,2048]{1,0:T(8,128)(2,1)S(1)} %get-tuple-element.47), channel_id=1, source_target_pairs={{8,12},{12,8},{16,20},{20,16},{9,13},{13,9},{17,21},{21,17},{10,14... | collective-permute-start | bytes 589832 | tf_op jit(solution)/shard_map/ppermute | solution.py:238
  36.7 16.7 %collective-permute-start.27 = (bf16[48,2048]{1,0:T(8,128)(2,1)S(1)}, bf16[48,2048]{1,0:T(8,128)(2,1)S(1)}, u32[]{:S(2)}, u32[]{:S(2)}) collective-permute-start(bf16[48,2048]{1,0:T(8,128)(2,1)S(1)} %get-tuple-element.48), channel_id=1, source_target_pairs={{8,4},{12,0},{16,28},{20,24},{9,5},{13,1},{17,29},{21,25},{10,6},{... | collective-permute-start | bytes 589832 | tf_op jit(solution)/shard_map/ppermute | solution.py:238
  47.4 17.1 %collective-permute-start.10 = (bf16[192,512]{1,0:T(8,128)(2,1)S(1)}, bf16[192,512]{1,0:T(8,128)(2,1)S(1)}, u32[]{:S(2)}, u32[]{:S(2)}) collective-permute-start(bf16[192,512]{1,0:T(8,128)(2,1)S(1)} %shard_map.113.refs_0_), channel_id=1, source_target_pairs={{0,2},{1,3},{2,0},{3,1},{4,6},{5,7},{6,4},{7,5},{8,10},{9,11},{10,... | collective-permute-start | bytes 589832 | tf_op jit(solution)/shard_map/ppermute | solution.py:238
  50.0 22.2 %collective-permute-start.11 = (bf16[192,512]{1,0:T(8,128)(2,1)S(1)}, bf16[192,512]{1,0:T(8,128)(2,1)S(1)}, u32[]{:S(2)}, u32[]{:S(2)}) collective-permute-start(bf16[192,512]{1,0:T(8,128)(2,1)S(1)} %shard_map.113.refs_0_), channel_id=1, source_target_pairs={{0,3},{1,2},{2,1},{3,0},{4,7},{5,6},{6,5},{7,4},{8,11},{9,10},{10,... | collective-permute-start | bytes 589832 | tf_op jit(solution)/shard_map/ppermute | solution.py:238
  50.9 21.5 %collective-permute-start.9 = (bf16[192,512]{1,0:T(8,128)(2,1)S(1)}, bf16[192,512]{1,0:T(8,128)(2,1)S(1)}, u32[]{:S(2)}, u32[]{:S(2)}) collective-permute-start(bf16[192,512]{1,0:T(8,128)(2,1)S(1)} %shard_map.113.refs_0_), channel_id=1, source_target_pairs={{0,1},{1,0},{2,3},{3,2},{4,5},{5,4},{6,7},{7,6},{8,9},{9,8},{10,11... | collective-permute-start | bytes 589832 | tf_op jit(solution)/shard_map/ppermute | solution.py:238
  60.6 13.8 %collective-permute-start.28 = (bf16[96,512]{1,0:T(8,128)(2,1)S(1)}, bf16[96,512]{1,0:T(8,128)(2,1)S(1)}, u32[]{:S(2)}, u32[]{:S(2)}) collective-permute-start(bf16[96,512]{1,0:T(8,128)(2,1)S(1)} %shard_map.119.refs_0_), channel_id=1, source_target_pairs={{0,1},{1,0},{2,3},{3,2},{4,5},{5,4},{6,7},{7,6},{8,9},{9,8},{10,11... | collective-permute-start | bytes 294920 | tf_op jit(solution)/shard_map/ppermute | solution.py:238
  64.1 11.6 %collective-permute-start.29 = (bf16[96,512]{1,0:T(8,128)(2,1)S(1)}, bf16[96,512]{1,0:T(8,128)(2,1)S(1)}, u32[]{:S(2)}, u32[]{:S(2)}) collective-permute-start(bf16[96,512]{1,0:T(8,128)(2,1)S(1)} %shard_map.119.refs_0_), channel_id=1, source_target_pairs={{0,2},{1,3},{2,0},{3,1},{4,6},{5,7},{6,4},{7,5},{8,10},{9,11},{10,... | collective-permute-start | bytes 294920 | tf_op jit(solution)/shard_map/ppermute | solution.py:238
  64.5 20.4 %collective-permute-start.22 = (bf16[4,48,512]{2,1,0:T(8,128)(2,1)S(1)}, bf16[4,48,512]{2,1,0:T(8,128)(2,1)S(1)}, u32[]{:S(2)}, u32[]{:S(2)}) collective-permute-start(bf16[4,48,512]{2,1,0:T(8,128)(2,1)S(1)} %get-tuple-element.44), channel_id=1, source_target_pairs={{0,16},{4,20},{24,8},{28,12},{1,17},{5,21},{25,9},{29,13},{2,18},{... | collective-permute-start | bytes 589832 | tf_op jit(solution)/shard_map/ppermute | solution.py:238
  83.2 15.8 %collective-permute-start.13 = (bf16[4,48,512]{2,1,0:T(8,128)(2,1)S(1)}, bf16[4,48,512]{2,1,0:T(8,128)(2,1)S(1)}, u32[]{:S(2)}, u32[]{:S(2)}) collective-permute-start(bf16[4,48,512]{2,1,0:T(8,128)(2,1)S(1)} %get-tuple-element.37), channel_id=1, source_target_pairs={{0,8},{4,12},{8,0},{12,4},{16,24},{20,28},{24,16},{28,20},{1,9},{5... | collective-permute-start | bytes 589832 | tf_op jit(solution)/shard_map/ppermute | solution.py:238
  83.2 19.3 %collective-permute-start.14 = (bf16[4,48,512]{2,1,0:T(8,128)(2,1)S(1)}, bf16[4,48,512]{2,1,0:T(8,128)(2,1)S(1)}, u32[]{:S(2)}, u32[]{:S(2)}) collective-permute-start(bf16[4,48,512]{2,1,0:T(8,128)(2,1)S(1)} %get-tuple-element.38), channel_id=1, source_target_pairs={{0,12},{4,8},{8,4},{12,0},{16,28},{20,24},{24,20},{28,16},{1,13},{... | collective-permute-start | bytes 589832 | tf_op jit(solution)/shard_map/ppermute | solution.py:238
  84.9 20.8 %collective-permute-start.31 = (bf16[4,48,512]{2,1,0:T(8,128)(2,1)S(1)}, bf16[4,48,512]{2,1,0:T(8,128)(2,1)S(1)}, u32[]{:S(2)}, u32[]{:S(2)}) collective-permute-start(bf16[4,48,512]{2,1,0:T(8,128)(2,1)S(1)} %get-tuple-element.49), channel_id=1, source_target_pairs={{8,24},{12,28},{16,0},{20,4},{9,25},{13,29},{17,1},{21,5},{10,26},... | collective-permute-start | bytes 589832 | tf_op jit(solution)/shard_map/ppermute | solution.py:238
  87.9 24.0 %collective-permute-start.33 = (bf16[4,48,512]{2,1,0:T(8,128)(2,1)S(1)}, bf16[4,48,512]{2,1,0:T(8,128)(2,1)S(1)}, u32[]{:S(2)}, u32[]{:S(2)}) collective-permute-start(bf16[4,48,512]{2,1,0:T(8,128)(2,1)S(1)} %get-tuple-element.51), channel_id=1, source_target_pairs={{8,28},{12,24},{16,4},{20,0},{9,29},{13,25},{17,5},{21,1},{10,30},... | collective-permute-start | bytes 589832 | tf_op jit(solution)/shard_map/ppermute | solution.py:238
  89.2 23.2 %collective-permute-start.34 = (bf16[4,48,512]{2,1,0:T(8,128)(2,1)S(1)}, bf16[4,48,512]{2,1,0:T(8,128)(2,1)S(1)}, u32[]{:S(2)}, u32[]{:S(2)}) collective-permute-start(bf16[4,48,512]{2,1,0:T(8,128)(2,1)S(1)} %get-tuple-element.44), channel_id=1, source_target_pairs={{8,16},{12,20},{16,8},{20,12},{9,17},{13,21},{17,9},{21,13},{10,18... | collective-permute-start | bytes 589832 | tf_op jit(solution)/shard_map/ppermute | solution.py:238
  99.0 13.5 %collective-permute-start.36 = (bf16[4,48,512]{2,1,0:T(8,128)(2,1)S(1)}, bf16[4,48,512]{2,1,0:T(8,128)(2,1)S(1)}, u32[]{:S(2)}, u32[]{:S(2)}) collective-permute-start(bf16[4,48,512]{2,1,0:T(8,128)(2,1)S(1)} %get-tuple-element.50), channel_id=1, source_target_pairs={{8,20},{12,16},{16,12},{20,8},{9,21},{13,17},{17,13},{21,9},{10,22... | collective-permute-start | bytes 589832 | tf_op jit(solution)/shard_map/ppermute | solution.py:238
  102.5 11.5 %collective-permute-start.35 = (bf16[4,48,512]{2,1,0:T(8,128)(2,1)S(1)}, bf16[4,48,512]{2,1,0:T(8,128)(2,1)S(1)}, u32[]{:S(2)}, u32[]{:S(2)}) collective-permute-start(bf16[4,48,512]{2,1,0:T(8,128)(2,1)S(1)} %get-tuple-element.49), channel_id=1, source_target_pairs={{0,24},{4,28},{24,0},{28,4},{1,25},{5,29},{25,1},{29,5},{2,26},{6,... | collective-permute-start | bytes 589832 | tf_op jit(solution)/shard_map/ppermute | solution.py:238
  105.7 11.2 %collective-permute-start.37 = (bf16[4,48,512]{2,1,0:T(8,128)(2,1)S(1)}, bf16[4,48,512]{2,1,0:T(8,128)(2,1)S(1)}, u32[]{:S(2)}, u32[]{:S(2)}) collective-permute-start(bf16[4,48,512]{2,1,0:T(8,128)(2,1)S(1)} %get-tuple-element.51), channel_id=1, source_target_pairs={{0,28},{4,24},{24,4},{28,0},{1,29},{5,25},{25,5},{29,1},{2,30},{6,... | collective-permute-start | bytes 589832 | tf_op jit(solution)/shard_map/ppermute | solution.py:238
  (27 other events, 226.6 us)

commit v3 on v1

--- a/solution.py
+++ b/solution.py
@@ -20,7 +20,7 @@
     return jnp.dot(a, b, preferred_element_type=F32)
 
 
-def call(kernel, outs, inputs, flops, scalars=0, far=(), scratch=(), spare=None):
+def call(kernel, outs, inputs, flops, scalars=0, far=(), scratch=(), spare=None, far_out=False):
     moved = sum(a.size * a.dtype.itemsize for a in inputs)
     moved += sum(o.size * o.dtype.itemsize for o in outs)
     specs = [SMEM] * scalars + [VMEM] * (len(inputs) - scalars)
@@ -31,7 +31,7 @@
         kernel,
         out_shape=outs,
         in_specs=specs,
-        out_specs=[VMEM] * len(outs),
+        out_specs=[HBM if far_out else VMEM] * len(outs),
         scratch_shapes=scratch,
         cost_estimate=pl.CostEstimate(flops=flops, bytes_accessed=moved, transcendentals=0),
         compiler_params=pltpu.CompilerParams(vmem_limit_bytes=limit),
@@ -203,17 +203,22 @@
 
 
 def scale_kernel(blocks, width, me, moe, gain, *refs):
-    squares, out = refs[:blocks], refs[-1]
+    squares, out, ready, sems = refs[:blocks], *refs[blocks:]
     count = moe.shape[1]
+    copies = []
     for m in range(blocks):
         total = squares[0][m : m + 1, :]
         for p in range(1, blocks):
             total = total + squares[p][m ^ p : (m ^ p) + 1, :]
         scale = lax.rsqrt(total / width + 1e-06)
         column = jnp.broadcast_to(scale, (count, count)).T[:, :1]
+        ready[m] = (moe[m].astype(F32) * column * gain[...]).astype(BF16)
         first = pl.multiple_of((me[0] ^ m) * count, count)
-        value = moe[m].astype(F32) * column * gain[...]
-        out[pl.ds(first, count), :] = value.astype(BF16)
+        copy = pltpu.make_async_copy(ready.at[m], out.at[pl.ds(first, count), :], sems.at[m])
+        copy.start()
+        copies.append(copy)
+    for copy in copies:
+        copy.wait()
 
 
 def swap(array, axis, k):
@@ -265,7 +270,7 @@
     )
     half, quarter = experts // 2, experts // 4
     arrived = [pieces[0]] + [swap(pieces[k], "ep", k) for k in range(1, experts)]
-    groups = {"N": (0, half), "A": (half, quarter), "B": (half + quarter, quarter)}
+    groups = {"N": (0, half), "A": (half + quarter, quarter), "B": (half, quarter)}
 
     packed = jnp.concatenate([routes.T.astype(F32), route_weights.T], axis=0)
     packed = spread(packed)
@@ -346,6 +351,11 @@
         [column, moe, out_gain[None, :]] + spread(squares),
         4 * blocks * count * local,
         scalars=1,
+        scratch=[
+            pltpu.VMEM((blocks, count, local), BF16),
+            pltpu.SemaphoreType.DMA((blocks,)),
+        ],
+        far_out=True,
     )
     return out
 

time: 110 us -> 111 us (level)
  the two profiles are of different devices: /device:TPU:10 before, /device:TPU:0 now
where the time goes in v3:
time: 111 us
  starting transfers between devices  47.2 us (43%)
  waiting for transfers between devices  43.9 us (40%)
  Pallas kernels  13 us (12%)
  local copies, waits for them, and re-layouts  5.62 us (5%)
    ppermute x32, starting transfers between devices, swap(): return lax.ppermute(array, axis, [(s, s ^ k) for s in range(size)])  47.2 us
    ppermute x32, waiting for transfers between devices, swap(): return lax.ppermute(array, axis, [(s, s ^ k) for s in range(size)])  43.9 us
    pallas_call x14, Pallas kernels, call(): pl.pallas_call(kernel, out_shape=outs, in_specs=specs, out_specs=[HBM if...  13 us
    unnamed x20, local copies, waits for them, and re-layouts  5.62 us
  transfers between devices with their start and end apart: 32, of which 13 were waited for; matrix products, arithmetic and copies ran while one was open for 1% of the time, Pallas kernels for 8%

profile of v3, /device:TPU:0, one launch (start us, length us, event | category | flops | bytes accessed | tf_op | source)
XLA Modules:
  0.0 110.6 jit_solution(5030971009845925755)
XLA Ops:
  0.7 1.6 %shard_map.111 = (bf16[48,2048]{1,0:T(8,128)(2,1)S(1)}, bf16[48,2048]{1,0:T(8,128)(2,1)S(1)}, bf16[48,2048]{1,0:T(8,128)(2,1)S(1)}, bf16[48,2048]{1,0:T(8,128)(2...) custom-call(s32[1]{0:T(128)} %bitcast.2.me, ...), custom_call_target="tpu_custom_call" | custom-call | flops 201326592 | bytes 2098180 | tf_op jit(solution)/shard_map/pallas_call | solution.py:30
  2.9 2.6 %collective-permute-start.7 = (bf16[48,2048]{1,0:T(8,128)(2,1)S(1)}, bf16[48,2048]{1,0:T(8,128)(2,1)S(1)}, u32[]{:S(2)}, u32[]{:S(2)}) collective-permute-start(bf16[48,2048]{1,0:T(8,128)(2,1)S(1)} %get-tuple-element.29), channel_id=1, source_target_pairs={{0,8},{4,12},{8,0},{12,4},{16,24},{20,28},{24,16},{28,20},{1,9},{5... | collective-permute-start | bytes 589832 | tf_op jit(solution)/shard_map/ppermute | solution.py:226
  6.2 1.7 %collective-permute-start.3 = (f32[4,128]{1,0:T(4,128)S(1)}, f32[4,128]{1,0:T(4,128)S(1)}, u32[]{:S(2)}, u32[]{:S(2)}) collective-permute-start(f32[4,128]{1,0:T(4,128)S(1)} %pad_maximum_fusion.refs_0_), channel_id=1, source_target_pairs={{0,1},{1,0},{2,3},{3,2},{4,5},{5,4},{6,7},{7,6},{8,9},{9,8},{10,11... | collective-permute-start | bytes 6152 | tf_op jit(solution)/shard_map/ppermute | solution.py:226
  9.8 2.6 %collective-permute-start.5 = (f32[4,128]{1,0:T(4,128)S(1)}, f32[4,128]{1,0:T(4,128)S(1)}, u32[]{:S(2)}, u32[]{:S(2)}) collective-permute-start(f32[4,128]{1,0:T(4,128)S(1)} %pad_maximum_fusion.refs_0_), channel_id=1, source_target_pairs={{0,3},{1,2},{2,1},{3,0},{4,7},{5,6},{6,5},{7,4},{8,11},{9,10},{10,... | collective-permute-start | bytes 6152 | tf_op jit(solution)/shard_map/ppermute | solution.py:226
  12.4 2.6 %collective-permute-start.22 = (bf16[48,2048]{1,0:T(8,128)(2,1)S(1)}, bf16[48,2048]{1,0:T(8,128)(2,1)S(1)}, u32[]{:S(2)}, u32[]{:S(2)}) collective-permute-start(bf16[48,2048]{1,0:T(8,128)(2,1)S(1)} %get-tuple-element.41), channel_id=1, source_target_pairs={{0,16},{4,20},{8,24},{12,28},{16,0},{20,4},{24,8},{28,12},{1,17},{... | collective-permute-start | bytes 589832 | tf_op jit(solution)/shard_map/ppermute | solution.py:226
  15.0 1.6 %copy-done = bf16[2048,512]{1,0:T(8,128)(2,1)S(1)} copy-done((bf16[2048,512]{1,0:T(8,128)(2,1)S(1)}, bf16[2048,512]{1,0:T(8,128)(2,1)}, u32[]{:S(2)}) %copy-start) | copy-done | bytes 2097176
  16.6 1.6 %copy-done.1 = bf16[2048,512]{1,0:T(8,128)(2,1)S(1)} copy-done((bf16[2048,512]{1,0:T(8,128)(2,1)S(1)}, bf16[2048,512]{1,0:T(8,128)(2,1)}, u32[]{:S(2)}) %copy-start.1) | copy-done | bytes 2097176
  20.0 1.6 %shard_map.109.refs_0_ = bf16[128,512]{1,0:T(8,128)(2,1)S(1)} custom-call(bf16[128,2048]{1,0:T(8,128)(2,1)S(1)} %copy-done.5, f32[1,2048]{1,0:T(1,128)S(1)} %bitcast.15, bf16[2048,512]{1,0:T(8,128)(2,1)S(1)} %copy-done, bf16[2048,512]{1,0:T(8,128)(2,1)S(1)} %copy-done.1), custom_call_target="tpu_custom_call" | custom-call | flops 536870912 | bytes 4857856 | tf_op jit(solution)/shard_map/pallas_call | solution.py:30
  21.6 1.5 %collective-permute-start = (bf16[128,512]{1,0:T(8,128)(2,1)S(1)}, bf16[128,512]{1,0:T(8,128)(2,1)S(1)}, u32[]{:S(2)}, u32[]{:S(2)}) collective-permute-start(bf16[128,512]{1,0:T(8,128)(2,1)S(1)} %shard_map.109.refs_0_), channel_id=1, source_target_pairs={{0,1},{1,0},{2,3},{3,2},{4,5},{5,4},{6,7},{7,6},{8,9},{9,8},{10,11... | collective-permute-start | bytes 393224 | tf_op jit(solution)/shard_map/ppermute | solution.py:226
  23.9 3.1 %collective-permute-start.15 = (bf16[48,2048]{1,0:T(8,128)(2,1)S(1)}, bf16[48,2048]{1,0:T(8,128)(2,1)S(1)}, u32[]{:S(2)}, u32[]{:S(2)}) collective-permute-start(bf16[48,2048]{1,0:T(8,128)(2,1)S(1)} %get-tuple-element.36), channel_id=1, source_target_pairs={{0,24},{4,28},{8,16},{12,20},{16,8},{20,12},{24,0},{28,4},{1,25},{... | collective-permute-start | bytes 589832 | tf_op jit(solution)/shard_map/ppermute | solution.py:226
  27.0 2.0 %collective-permute-start.16 = (bf16[48,2048]{1,0:T(8,128)(2,1)S(1)}, bf16[48,2048]{1,0:T(8,128)(2,1)S(1)}, u32[]{:S(2)}, u32[]{:S(2)}) collective-permute-start(bf16[48,2048]{1,0:T(8,128)(2,1)S(1)} %get-tuple-element.37), channel_id=1, source_target_pairs={{0,28},{4,24},{8,20},{12,16},{16,12},{20,8},{24,4},{28,0},{1,29},{... | collective-permute-start | bytes 589832 | tf_op jit(solution)/shard_map/ppermute | solution.py:226
  30.1 1.6 %collective-permute-start.10 = (bf16[192,512]{1,0:T(8,128)(2,1)S(1)}, bf16[192,512]{1,0:T(8,128)(2,1)S(1)}, u32[]{:S(2)}, u32[]{:S(2)}) collective-permute-start(bf16[192,512]{1,0:T(8,128)(2,1)S(1)} %shard_map.113.refs_0_), channel_id=1, source_target_pairs={{0,2},{1,3},{2,0},{3,1},{4,6},{5,7},{6,4},{7,5},{8,10},{9,11},{10,... | collective-permute-start | bytes 589832 | tf_op jit(solution)/shard_map/ppermute | solution.py:226
  31.7 6.3 %collective-permute-done.22.refs_0_ = bf16[48,2048]{1,0:T(8,128)(2,1)S(1)} collective-permute-done((bf16[48,2048]{1,0:T(8,128)(2,1)S(1)}, bf16[48,2048]{1,0:T(8,128)(2,1)S(1)}, u32[]{:S(2)}, u32[]{:S(2)}) %collective-permute-start.22) | collective-permute-done | bytes 196640 | tf_op jit(solution)/shard_map/ppermute | solution.py:226
  46.2 3.8 %collective-permute-start.18 = (bf16[96,512]{1,0:T(8,128)(2,1)S(1)}, bf16[96,512]{1,0:T(8,128)(2,1)S(1)}, u32[]{:S(2)}, u32[]{:S(2)}) collective-permute-start(bf16[96,512]{1,0:T(8,128)(2,1)S(1)} %shard_map.116.refs_0_), channel_id=1, source_target_pairs={{0,2},{1,3},{2,0},{3,1},{4,6},{5,7},{6,4},{7,5},{8,10},{9,11},{10,... | collective-permute-start | bytes 294920 | tf_op jit(solution)/shard_map/ppermute | solution.py:226
  50.6 1.6 %collective-permute-done.2.refs_3_ = bf16[128,512]{1,0:T(8,128)(2,1)S(1)} collective-permute-done((bf16[128,512]{1,0:T(8,128)(2,1)S(1)}, bf16[128,512]{1,0:T(8,128)(2,1)S(1)}, u32[]{:S(2)}, u32[]{:S(2)}) %collective-permute-start.2) | collective-permute-done | bytes 131104 | tf_op jit(solution)/shard_map/ppermute | solution.py:226
  52.2 4.6 %collective-permute-start.13 = (bf16[4,48,512]{2,1,0:T(8,128)(2,1)S(1)}, bf16[4,48,512]{2,1,0:T(8,128)(2,1)S(1)}, u32[]{:S(2)}, u32[]{:S(2)}) collective-permute-start(bf16[4,48,512]{2,1,0:T(8,128)(2,1)S(1)} %get-tuple-element.33), channel_id=1, source_target_pairs={{0,8},{4,12},{8,0},{12,4},{16,24},{20,28},{24,16},{28,20},{1,9},{5... | collective-permute-start | bytes 589832 | tf_op jit(solution)/shard_map/ppermute | solution.py:226
  60.4 2.0 %collective-permute-done.19.refs_3_ = bf16[96,512]{1,0:T(8,128)(2,1)S(1)} collective-permute-done((bf16[96,512]{1,0:T(8,128)(2,1)S(1)}, bf16[96,512]{1,0:T(8,128)(2,1)S(1)}, u32[]{:S(2)}, u32[]{:S(2)}) %collective-permute-start.19) | collective-permute-done | bytes 98336 | tf_op jit(solution)/shard_map/ppermute | solution.py:226
  62.8 3.6 %collective-permute-done.25.refs_2_ = bf16[96,512]{1,0:T(8,128)(2,1)S(1)} collective-permute-done((bf16[96,512]{1,0:T(8,128)(2,1)S(1)}, bf16[96,512]{1,0:T(8,128)(2,1)S(1)}, u32[]{:S(2)}, u32[]{:S(2)}) %collective-permute-start.25) | collective-permute-done | bytes 98336 | tf_op jit(solution)/shard_map/ppermute | solution.py:226
  66.4 2.7 %collective-permute-start.20 = (bf16[4,48,512]{2,1,0:T(8,128)(2,1)S(1)}, bf16[4,48,512]{2,1,0:T(8,128)(2,1)S(1)}, u32[]{:S(2)}, u32[]{:S(2)}) collective-permute-start(bf16[4,48,512]{2,1,0:T(8,128)(2,1)S(1)} %get-tuple-element.38), channel_id=1, source_target_pairs={{0,24},{4,28},{8,16},{12,20},{16,8},{20,12},{24,0},{28,4},{1,25},{... | collective-permute-start | bytes 589832 | tf_op jit(solution)/shard_map/ppermute | solution.py:226
  70.6 2.4 %collective-permute-start.28 = (bf16[4,48,512]{2,1,0:T(8,128)(2,1)S(1)}, bf16[4,48,512]{2,1,0:T(8,128)(2,1)S(1)}, u32[]{:S(2)}, u32[]{:S(2)}) collective-permute-start(bf16[4,48,512]{2,1,0:T(8,128)(2,1)S(1)} %get-tuple-element.44), channel_id=1, source_target_pairs={{0,20},{4,16},{8,28},{12,24},{16,4},{20,0},{24,12},{28,8},{1,21},{... | collective-permute-start | bytes 589832 | tf_op jit(solution)/shard_map/ppermute | solution.py:226
  76.0 3.3 %collective-permute-done.21.refs_1_ = bf16[4,48,512]{2,1,0:T(8,128)(2,1)S(1)} collective-permute-done((bf16[4,48,512]{2,1,0:T(8,128)(2,1)S(1)}, bf16[4,48,512]{2,1,0:T(8,128)(2,1)S(1)}, u32[]{:S(2)}, u32[]{:S(2)}) %collective-permute-start.21) | collective-permute-done | bytes 196640 | tf_op jit(solution)/shard_map/ppermute | solution.py:226
  79.9 19.9 %collective-permute-done.27.refs_0_ = bf16[4,48,512]{2,1,0:T(8,128)(2,1)S(1)} collective-permute-done((bf16[4,48,512]{2,1,0:T(8,128)(2,1)S(1)}, bf16[4,48,512]{2,1,0:T(8,128)(2,1)S(1)}, u32[]{:S(2)}, u32[]{:S(2)}) %collective-permute-start.27) | collective-permute-done | bytes 196640 | tf_op jit(solution)/shard_map/ppermute | solution.py:226
  99.8 2.9 %collective-permute-done.28.refs_1_ = bf16[4,48,512]{2,1,0:T(8,128)(2,1)S(1)} collective-permute-done((bf16[4,48,512]{2,1,0:T(8,128)(2,1)S(1)}, bf16[4,48,512]{2,1,0:T(8,128)(2,1)S(1)}, u32[]{:S(2)}, u32[]{:S(2)}) %collective-permute-start.28) | collective-permute-done | bytes 196640 | tf_op jit(solution)/shard_map/ppermute | solution.py:226
  105.1 2.3 %collective-permute-start.31 = (f32[4,128]{1,0:T(4,128)S(1)}, f32[4,128]{1,0:T(4,128)S(1)}, u32[]{:S(2)}, u32[]{:S(2)}) collective-permute-start(f32[4,128]{1,0:T(4,128)S(1)} %get-tuple-element.46.refs_0_), channel_id=1, source_target_pairs={{0,3},{1,2},{2,1},{3,0},{4,7},{5,6},{6,5},{7,4},{8,11},{9,10},{10,... | collective-permute-start | bytes 6152 | tf_op jit(solution)/shard_map/ppermute | solution.py:226
  (76 shorter events, 30.9 us)
Async XLA Ops:
  2.3 19.3 %collective-permute-start.6 = (bf16[48,2048]{1,0:T(8,128)(2,1)S(1)}, bf16[48,2048]{1,0:T(8,128)(2,1)S(1)}, u32[]{:S(2)}, u32[]{:S(2)}) collective-permute-start(bf16[48,2048]{1,0:T(8,128)(2,1)S(1)} %get-tuple-element.28), channel_id=1, source_target_pairs={{0,4},{4,0},{8,12},{12,8},{16,20},{20,16},{24,28},{28,24},{1,5},{5... | collective-permute-start | bytes 589832 | tf_op jit(solution)/shard_map/ppermute | solution.py:226
  2.9 21.0 %collective-permute-start.7 = (bf16[48,2048]{1,0:T(8,128)(2,1)S(1)}, bf16[48,2048]{1,0:T(8,128)(2,1)S(1)}, u32[]{:S(2)}, u32[]{:S(2)}) collective-permute-start(bf16[48,2048]{1,0:T(8,128)(2,1)S(1)} %get-tuple-element.29), channel_id=1, source_target_pairs={{0,8},{4,12},{8,0},{12,4},{16,24},{20,28},{24,16},{28,20},{1,9},{5... | collective-permute-start | bytes 589832 | tf_op jit(solution)/shard_map/ppermute | solution.py:226
  5.5 21.5 %collective-permute-start.8 = (bf16[48,2048]{1,0:T(8,128)(2,1)S(1)}, bf16[48,2048]{1,0:T(8,128)(2,1)S(1)}, u32[]{:S(2)}, u32[]{:S(2)}) collective-permute-start(bf16[48,2048]{1,0:T(8,128)(2,1)S(1)} %get-tuple-element.30), channel_id=1, source_target_pairs={{0,12},{4,8},{8,4},{12,0},{16,28},{20,24},{24,20},{28,16},{1,13},{... | collective-permute-start | bytes 589832 | tf_op jit(solution)/shard_map/ppermute | solution.py:226
  12.4 25.5 %collective-permute-start.22 = (bf16[48,2048]{1,0:T(8,128)(2,1)S(1)}, bf16[48,2048]{1,0:T(8,128)(2,1)S(1)}, u32[]{:S(2)}, u32[]{:S(2)}) collective-permute-start(bf16[48,2048]{1,0:T(8,128)(2,1)S(1)} %get-tuple-element.41), channel_id=1, source_target_pairs={{0,16},{4,20},{8,24},{12,28},{16,0},{20,4},{24,8},{28,12},{1,17},{... | collective-permute-start | bytes 589832 | tf_op jit(solution)/shard_map/ppermute | solution.py:226
  15.0 23.7 %collective-permute-start.23 = (bf16[48,2048]{1,0:T(8,128)(2,1)S(1)}, bf16[48,2048]{1,0:T(8,128)(2,1)S(1)}, u32[]{:S(2)}, u32[]{:S(2)}) collective-permute-start(bf16[48,2048]{1,0:T(8,128)(2,1)S(1)} %get-tuple-element.42), channel_id=1, source_target_pairs={{0,20},{4,16},{8,28},{12,24},{16,4},{20,0},{24,12},{28,8},{1,21},{... | collective-permute-start | bytes 589832 | tf_op jit(solution)/shard_map/ppermute | solution.py:226
  21.6 8.5 %collective-permute-start = (bf16[128,512]{1,0:T(8,128)(2,1)S(1)}, bf16[128,512]{1,0:T(8,128)(2,1)S(1)}, u32[]{:S(2)}, u32[]{:S(2)}) collective-permute-start(bf16[128,512]{1,0:T(8,128)(2,1)S(1)} %shard_map.109.refs_0_), channel_id=1, source_target_pairs={{0,1},{1,0},{2,3},{3,2},{4,5},{5,4},{6,7},{7,6},{8,9},{9,8},{10,11... | collective-permute-start | bytes 393224 | tf_op jit(solution)/shard_map/ppermute | solution.py:226
  23.9 16.2 %collective-permute-start.15 = (bf16[48,2048]{1,0:T(8,128)(2,1)S(1)}, bf16[48,2048]{1,0:T(8,128)(2,1)S(1)}, u32[]{:S(2)}, u32[]{:S(2)}) collective-permute-start(bf16[48,2048]{1,0:T(8,128)(2,1)S(1)} %get-tuple-element.36), channel_id=1, source_target_pairs={{0,24},{4,28},{8,16},{12,20},{16,8},{20,12},{24,0},{28,4},{1,25},{... | collective-permute-start | bytes 589832 | tf_op jit(solution)/shard_map/ppermute | solution.py:226
  27.0 14.6 %collective-permute-start.16 = (bf16[48,2048]{1,0:T(8,128)(2,1)S(1)}, bf16[48,2048]{1,0:T(8,128)(2,1)S(1)}, u32[]{:S(2)}, u32[]{:S(2)}) collective-permute-start(bf16[48,2048]{1,0:T(8,128)(2,1)S(1)} %get-tuple-element.37), channel_id=1, source_target_pairs={{0,28},{4,24},{8,20},{12,16},{16,12},{20,8},{24,4},{28,0},{1,29},{... | collective-permute-start | bytes 589832 | tf_op jit(solution)/shard_map/ppermute | solution.py:226
  30.1 13.0 %collective-permute-start.10 = (bf16[192,512]{1,0:T(8,128)(2,1)S(1)}, bf16[192,512]{1,0:T(8,128)(2,1)S(1)}, u32[]{:S(2)}, u32[]{:S(2)}) collective-permute-start(bf16[192,512]{1,0:T(8,128)(2,1)S(1)} %shard_map.113.refs_0_), channel_id=1, source_target_pairs={{0,2},{1,3},{2,0},{3,1},{4,6},{5,7},{6,4},{7,5},{8,10},{9,11},{10,... | collective-permute-start | bytes 589832 | tf_op jit(solution)/shard_map/ppermute | solution.py:226
  38.0 7.5 %collective-permute-start.11 = (bf16[192,512]{1,0:T(8,128)(2,1)S(1)}, bf16[192,512]{1,0:T(8,128)(2,1)S(1)}, u32[]{:S(2)}, u32[]{:S(2)}) collective-permute-start(bf16[192,512]{1,0:T(8,128)(2,1)S(1)} %shard_map.113.refs_0_), channel_id=1, source_target_pairs={{0,3},{1,2},{2,1},{3,0},{4,7},{5,6},{6,5},{7,4},{8,11},{9,10},{10,... | collective-permute-start | bytes 589832 | tf_op jit(solution)/shard_map/ppermute | solution.py:226
  40.1 10.5 %collective-permute-start.1 = (bf16[128,512]{1,0:T(8,128)(2,1)S(1)}, bf16[128,512]{1,0:T(8,128)(2,1)S(1)}, u32[]{:S(2)}, u32[]{:S(2)}) collective-permute-start(bf16[128,512]{1,0:T(8,128)(2,1)S(1)} %shard_map.109.refs_0_), channel_id=1, source_target_pairs={{0,2},{1,3},{2,0},{3,1},{4,6},{5,7},{6,4},{7,5},{8,10},{9,11},{10,... | collective-permute-start | bytes 393224 | tf_op jit(solution)/shard_map/ppermute | solution.py:226
  41.6 10.6 %collective-permute-start.2 = (bf16[128,512]{1,0:T(8,128)(2,1)S(1)}, bf16[128,512]{1,0:T(8,128)(2,1)S(1)}, u32[]{:S(2)}, u32[]{:S(2)}) collective-permute-start(bf16[128,512]{1,0:T(8,128)(2,1)S(1)} %shard_map.109.refs_0_), channel_id=1, source_target_pairs={{0,3},{1,2},{2,1},{3,0},{4,7},{5,6},{6,5},{7,4},{8,11},{9,10},{10,... | collective-permute-start | bytes 393224 | tf_op jit(solution)/shard_map/ppermute | solution.py:226
  43.1 13.7 %collective-permute-start.24 = (bf16[96,512]{1,0:T(8,128)(2,1)S(1)}, bf16[96,512]{1,0:T(8,128)(2,1)S(1)}, u32[]{:S(2)}, u32[]{:S(2)}) collective-permute-start(bf16[96,512]{1,0:T(8,128)(2,1)S(1)} %shard_map.119.refs_0_), channel_id=1, source_target_pairs={{0,1},{1,0},{2,3},{3,2},{4,5},{5,4},{6,7},{7,6},{8,9},{9,8},{10,11... | collective-permute-start | bytes 294920 | tf_op jit(solution)/shard_map/ppermute | solution.py:226
  45.5 12.4 %collective-permute-start.17 = (bf16[96,512]{1,0:T(8,128)(2,1)S(1)}, bf16[96,512]{1,0:T(8,128)(2,1)S(1)}, u32[]{:S(2)}, u32[]{:S(2)}) collective-permute-start(bf16[96,512]{1,0:T(8,128)(2,1)S(1)} %shard_map.116.refs_0_), channel_id=1, source_target_pairs={{0,1},{1,0},{2,3},{3,2},{4,5},{5,4},{6,7},{7,6},{8,9},{9,8},{10,11... | collective-permute-start | bytes 294920 | tf_op jit(solution)/shard_map/ppermute | solution.py:226
  46.2 13.1 %collective-permute-start.18 = (bf16[96,512]{1,0:T(8,128)(2,1)S(1)}, bf16[96,512]{1,0:T(8,128)(2,1)S(1)}, u32[]{:S(2)}, u32[]{:S(2)}) collective-permute-start(bf16[96,512]{1,0:T(8,128)(2,1)S(1)} %shard_map.116.refs_0_), channel_id=1, source_target_pairs={{0,2},{1,3},{2,0},{3,1},{4,6},{5,7},{6,4},{7,5},{8,10},{9,11},{10,... | collective-permute-start | bytes 294920 | tf_op jit(solution)/shard_map/ppermute | solution.py:226
  50.6 19.2 %collective-permute-start.12 = (bf16[4,48,512]{2,1,0:T(8,128)(2,1)S(1)}, bf16[4,48,512]{2,1,0:T(8,128)(2,1)S(1)}, u32[]{:S(2)}, u32[]{:S(2)}) collective-permute-start(bf16[4,48,512]{2,1,0:T(8,128)(2,1)S(1)} %get-tuple-element.32), channel_id=1, source_target_pairs={{0,4},{4,0},{8,12},{12,8},{16,20},{20,16},{24,28},{28,24},{1,5},{5... | collective-permute-start | bytes 589832 | tf_op jit(solution)/shard_map/ppermute | solution.py:226
  52.2 18.3 %collective-permute-start.13 = (bf16[4,48,512]{2,1,0:T(8,128)(2,1)S(1)}, bf16[4,48,512]{2,1,0:T(8,128)(2,1)S(1)}, u32[]{:S(2)}, u32[]{:S(2)}) collective-permute-start(bf16[4,48,512]{2,1,0:T(8,128)(2,1)S(1)} %get-tuple-element.33), channel_id=1, source_target_pairs={{0,8},{4,12},{8,0},{12,4},{16,24},{20,28},{24,16},{28,20},{1,9},{5... | collective-permute-start | bytes 589832 | tf_op jit(solution)/shard_map/ppermute | solution.py:226
  57.9 8.5 %collective-permute-start.25 = (bf16[96,512]{1,0:T(8,128)(2,1)S(1)}, bf16[96,512]{1,0:T(8,128)(2,1)S(1)}, u32[]{:S(2)}, u32[]{:S(2)}) collective-permute-start(bf16[96,512]{1,0:T(8,128)(2,1)S(1)} %shard_map.119.refs_0_), channel_id=1, source_target_pairs={{0,2},{1,3},{2,0},{3,1},{4,6},{5,7},{6,4},{7,5},{8,10},{9,11},{10,... | collective-permute-start | bytes 294920 | tf_op jit(solution)/shard_map/ppermute | solution.py:226
  59.3 9.8 %collective-permute-start.26 = (bf16[96,512]{1,0:T(8,128)(2,1)S(1)}, bf16[96,512]{1,0:T(8,128)(2,1)S(1)}, u32[]{:S(2)}, u32[]{:S(2)}) collective-permute-start(bf16[96,512]{1,0:T(8,128)(2,1)S(1)} %shard_map.119.refs_0_), channel_id=1, source_target_pairs={{0,3},{1,2},{2,1},{3,0},{4,7},{5,6},{6,5},{7,4},{8,11},{9,10},{10,... | collective-permute-start | bytes 294920 | tf_op jit(solution)/shard_map/ppermute | solution.py:226
  62.4 11.8 %collective-permute-start.14 = (bf16[4,48,512]{2,1,0:T(8,128)(2,1)S(1)}, bf16[4,48,512]{2,1,0:T(8,128)(2,1)S(1)}, u32[]{:S(2)}, u32[]{:S(2)}) collective-permute-start(bf16[4,48,512]{2,1,0:T(8,128)(2,1)S(1)} %get-tuple-element.34), channel_id=1, source_target_pairs={{0,12},{4,8},{8,4},{12,0},{16,28},{20,24},{24,20},{28,16},{1,13},{... | collective-permute-start | bytes 589832 | tf_op jit(solution)/shard_map/ppermute | solution.py:226
  66.4 9.7 %collective-permute-start.20 = (bf16[4,48,512]{2,1,0:T(8,128)(2,1)S(1)}, bf16[4,48,512]{2,1,0:T(8,128)(2,1)S(1)}, u32[]{:S(2)}, u32[]{:S(2)}) collective-permute-start(bf16[4,48,512]{2,1,0:T(8,128)(2,1)S(1)} %get-tuple-element.38), channel_id=1, source_target_pairs={{0,24},{4,28},{8,16},{12,20},{16,8},{20,12},{24,0},{28,4},{1,25},{... | collective-permute-start | bytes 589832 | tf_op jit(solution)/shard_map/ppermute | solution.py:226
  69.1 10.2 %collective-permute-start.21 = (bf16[4,48,512]{2,1,0:T(8,128)(2,1)S(1)}, bf16[4,48,512]{2,1,0:T(8,128)(2,1)S(1)}, u32[]{:S(2)}, u32[]{:S(2)}) collective-permute-start(bf16[4,48,512]{2,1,0:T(8,128)(2,1)S(1)} %get-tuple-element.39), channel_id=1, source_target_pairs={{0,28},{4,24},{8,20},{12,16},{16,12},{20,8},{24,4},{28,0},{1,29},{... | collective-permute-start | bytes 589832 | tf_op jit(solution)/shard_map/ppermute | solution.py:226
  69.8 30.0 %collective-permute-start.27 = (bf16[4,48,512]{2,1,0:T(8,128)(2,1)S(1)}, bf16[4,48,512]{2,1,0:T(8,128)(2,1)S(1)}, u32[]{:S(2)}, u32[]{:S(2)}) collective-permute-start(bf16[4,48,512]{2,1,0:T(8,128)(2,1)S(1)} %get-tuple-element.43), channel_id=1, source_target_pairs={{0,16},{4,20},{8,24},{12,28},{16,0},{20,4},{24,8},{28,12},{1,17},{... | collective-permute-start | bytes 589832 | tf_op jit(solution)/shard_map/ppermute | solution.py:226
  70.6 32.1 %collective-permute-start.28 = (bf16[4,48,512]{2,1,0:T(8,128)(2,1)S(1)}, bf16[4,48,512]{2,1,0:T(8,128)(2,1)S(1)}, u32[]{:S(2)}, u32[]{:S(2)}) collective-permute-start(bf16[4,48,512]{2,1,0:T(8,128)(2,1)S(1)} %get-tuple-element.44), channel_id=1, source_target_pairs={{0,20},{4,16},{8,28},{12,24},{16,4},{20,0},{24,12},{28,8},{1,21},{... | collective-permute-start | bytes 589832 | tf_op jit(solution)/shard_map/ppermute | solution.py:226
  (18 other events, 115.9 us)

commit v4 on v3

--- a/solution.py
+++ b/solution.py
@@ -12,7 +12,6 @@
 SMEM = pl.BlockSpec(memory_space=pltpu.SMEM)
 HBM = pl.BlockSpec(memory_space=pltpu.HBM)
 F32 = jnp.float32
-SPARE = 10800000
 BF16 = jnp.bfloat16
 
 
@@ -20,13 +19,13 @@
     return jnp.dot(a, b, preferred_element_type=F32)
 
 
-def call(kernel, outs, inputs, flops, scalars=0, far=(), scratch=(), spare=None, far_out=False):
+def call(kernel, outs, inputs, flops, scalars=0, far=(), scratch=(), far_out=False):
     moved = sum(a.size * a.dtype.itemsize for a in inputs)
     moved += sum(o.size * o.dtype.itemsize for o in outs)
     specs = [SMEM] * scalars + [VMEM] * (len(inputs) - scalars)
     for i in far:
         specs[i] = HBM
-    limit = 40 * 1024 * 1024 if spare is None else 67043328 - spare
+        inputs[i] = pltpu.with_memory_space_constraint(inputs[i], pltpu.HBM)
     return pl.pallas_call(
         kernel,
         out_shape=outs,
@@ -34,7 +33,7 @@
         out_specs=[HBM if far_out else VMEM] * len(outs),
         scratch_shapes=scratch,
         cost_estimate=pl.CostEstimate(flops=flops, bytes_accessed=moved, transcendentals=0),
-        compiler_params=pltpu.CompilerParams(vmem_limit_bytes=limit),
+        compiler_params=pltpu.CompilerParams(vmem_limit_bytes=40 * 1024 * 1024),
     )(*inputs)
 
 
@@ -117,10 +116,12 @@
                     for place, weight in zip(places, columns[top_count:])
                 ],
             )
-            for part in range(3):
+            parts = []
+            for _ in range(3):
                 piece = table.astype(BF16)
-                out[m, part * count : (part + 1) * count, :] = piece
+                parts.append(piece)
                 table = table - piece.astype(F32)
+            out[m] = jnp.concatenate(parts, axis=1)
 
 
 def stage_kernel(gate, upward, held, both, sems):
@@ -159,9 +160,7 @@
 
 def weighted(table, returned, m):
     rows = jnp.concatenate([r[m] for r in returned], axis=0)
-    parts = dot(table[m], rows)
-    count = parts.shape[0] // 3
-    return parts[:count] + parts[count : 2 * count] + parts[2 * count :]
+    return dot(table[m], jnp.concatenate([rows] * 3, axis=0))
 
 
 def base_kernel(blocks, *refs):
@@ -266,11 +265,10 @@
             pltpu.VMEM((top_count, count), jnp.int32),
             pltpu.SemaphoreType.DMA((2,)),
         ],
-        spare=experts * capacity * width * 2 + SPARE,
     )
     half, quarter = experts // 2, experts // 4
     arrived = [pieces[0]] + [swap(pieces[k], "ep", k) for k in range(1, experts)]
-    groups = {"N": (0, half), "A": (half + quarter, quarter), "B": (half, quarter)}
+    groups = {"N": (0, half), "A": (half, quarter), "B": (half + quarter, quarter)}
 
     packed = jnp.concatenate([routes.T.astype(F32), route_weights.T], axis=0)
     packed = spread(packed)
@@ -295,7 +293,7 @@
     tables = call(
         functools.partial(table_kernel, capacity, list(groups.values())),
         [
-            jax.ShapeDtypeStruct((blocks, 3 * count, size * capacity), BF16)
+            jax.ShapeDtypeStruct((blocks, count, 3 * size * capacity), BF16)
             for _, size in groups.values()
         ],
         [row] + packed,

time: 111 us -> 110 us (level)
  the two profiles are of different devices: /device:TPU:0 before, /device:TPU:10 now
where the time goes in v4:
time: 110 us
  waiting for transfers between devices  56.5 us (51%)
  starting transfers between devices  32.9 us (30%)
  Pallas kernels  16.5 us (15%)
  local copies, waits for them, and re-layouts  2.43 us (2%)
  other arithmetic  1.37 us (1%)
    ppermute x32, waiting for transfers between devices, swap(): return lax.ppermute(array, axis, [(s, s ^ k) for s in range(size)])  56.5 us
    ppermute x32, starting transfers between devices, swap(): return lax.ppermute(array, axis, [(s, s ^ k) for s in range(size)])  32.9 us
    pallas_call x14, Pallas kernels, call(): pl.pallas_call(kernel, out_shape=outs, in_specs=specs, out_specs=[HBM if...  16.5 us
    unnamed x14, local copies, waits for them, and re-layouts  2.43 us
  transfers between devices with their start and end apart: 32, of which 15 were waited for; matrix products, arithmetic and copies ran while one was open for 1% of the time, Pallas kernels for 11%

profile of v4, /device:TPU:10, one launch (start us, length us, event | category | flops | bytes accessed | tf_op | source)
XLA Modules:
  0.0 109.9 jit_solution(10482459651469027082)
XLA Ops:
  0.0 1.6 %shard_map.111 = (bf16[48,2048]{1,0:T(8,128)(2,1)S(1)}, bf16[48,2048]{1,0:T(8,128)(2,1)S(1)}, bf16[48,2048]{1,0:T(8,128)(2,1)S(1)}, bf16[48,2048]{1,0:T(8,128)(2...) custom-call(s32[1]{0:T(128)} %bitcast.2.me, ...), custom_call_target="tpu_custom_call" | custom-call | flops 201326592 | bytes 2098180 | tf_op jit(solution)/shard_map/pallas_call | solution.py:29
  6.1 1.5 %collective-permute-start.4 = (f32[4,128]{1,0:T(4,128)S(1)}, f32[4,128]{1,0:T(4,128)S(1)}, u32[]{:S(2)}, u32[]{:S(2)}) collective-permute-start(f32[4,128]{1,0:T(4,128)S(1)} %pad_maximum_fusion.refs_0_), channel_id=1, source_target_pairs={{0,2},{1,3},{2,0},{3,1},{4,6},{5,7},{6,4},{7,5},{8,10},{9,11},{10,... | collective-permute-start | bytes 6152 | tf_op jit(solution)/shard_map/ppermute | solution.py:225
  7.6 1.5 %collective-permute-done.3.refs_1_ = f32[4,128]{1,0:T(4,128)S(1)} collective-permute-done((f32[4,128]{1,0:T(4,128)S(1)}, f32[4,128]{1,0:T(4,128)S(1)}, u32[]{:S(2)}, u32[]{:S(2)}) %collective-permute-start.3) | collective-permute-done | bytes 2080 | tf_op jit(solution)/shard_map/ppermute | solution.py:225
  10.6 1.6 %collective-permute-start.22 = (bf16[48,2048]{1,0:T(8,128)(2,1)S(1)}, bf16[48,2048]{1,0:T(8,128)(2,1)S(1)}, u32[]{:S(2)}, u32[]{:S(2)}) collective-permute-start(bf16[48,2048]{1,0:T(8,128)(2,1)S(1)} %get-tuple-element.41), channel_id=1, source_target_pairs={{0,24},{4,28},{8,16},{12,20},{16,8},{20,12},{24,0},{28,4},{1,25},{... | collective-permute-start | bytes 589832 | tf_op jit(solution)/shard_map/ppermute | solution.py:225
  15.4 3.0 %shard_map.109.refs_0_ = bf16[128,512]{1,0:T(8,128)(2,1)S(1)} custom-call(bf16[128,2048]{1,0:T(8,128)(2,1)S(1)} %copy-done.3, f32[1,2048]{1,0:T(1,128)S(1)} %bitcast.13, bf16[2048,512]{1,0:T(8,128)(2,1)} %gate.1, bf16[2048,512]{1,0:T(8,128)(2,1)} %upward.1), custom_call_target="tpu_custom_call" | custom-call | flops 536870912 | bytes 4857856 | tf_op jit(solution)/shard_map/pallas_call | solution.py:29
  19.0 2.3 %shard_map.112.refs_5_.refs_3_ = bf16[2048,1024]{1,0:T(8,128)(2,1)S(1)} custom-call(bf16[2048,512]{1,0:T(8,128)(2,1)} %bitcast.18, bf16[2048,512]{1,0:T(8,128)(2,1)} %bitcast.19, bf16[48,2048]{1,0:T(8,128)(2,1)} %copy-done.1), custom_call_target="tpu_custom_call" | custom-call | flops 262144 | bytes 8585216 | tf_op jit(solution)/shard_map/pallas_call | solution.py:29
  21.2 2.9 %collective-permute-start.15 = (bf16[48,2048]{1,0:T(8,128)(2,1)S(1)}, bf16[48,2048]{1,0:T(8,128)(2,1)S(1)}, u32[]{:S(2)}, u32[]{:S(2)}) collective-permute-start(bf16[48,2048]{1,0:T(8,128)(2,1)S(1)} %get-tuple-element.36), channel_id=1, source_target_pairs={{0,16},{4,20},{8,24},{12,28},{16,0},{20,4},{24,8},{28,12},{1,17},{... | collective-permute-start | bytes 589832 | tf_op jit(solution)/shard_map/ppermute | solution.py:225
  27.7 7.3 %collective-permute-done.22.refs_0_ = bf16[48,2048]{1,0:T(8,128)(2,1)S(1)} collective-permute-done((bf16[48,2048]{1,0:T(8,128)(2,1)S(1)}, bf16[48,2048]{1,0:T(8,128)(2,1)S(1)}, u32[]{:S(2)}, u32[]{:S(2)}) %collective-permute-start.22) | collective-permute-done | bytes 196640 | tf_op jit(solution)/shard_map/ppermute | solution.py:225
  35.1 3.5 %collective-permute-done.23.refs_1_ = bf16[48,2048]{1,0:T(8,128)(2,1)S(1)} collective-permute-done((bf16[48,2048]{1,0:T(8,128)(2,1)S(1)}, bf16[48,2048]{1,0:T(8,128)(2,1)S(1)}, u32[]{:S(2)}, u32[]{:S(2)}) %collective-permute-start.23) | collective-permute-done | bytes 196640 | tf_op jit(solution)/shard_map/ppermute | solution.py:225
  40.1 2.7 %collective-permute-done.15.refs_0_ = bf16[48,2048]{1,0:T(8,128)(2,1)S(1)} collective-permute-done((bf16[48,2048]{1,0:T(8,128)(2,1)S(1)}, bf16[48,2048]{1,0:T(8,128)(2,1)S(1)}, u32[]{:S(2)}, u32[]{:S(2)}) %collective-permute-start.15) | collective-permute-done | bytes 196640 | tf_op jit(solution)/shard_map/ppermute | solution.py:225
  43.3 1.9 %collective-permute-done.16.refs_1_ = bf16[48,2048]{1,0:T(8,128)(2,1)S(1)} collective-permute-done((bf16[48,2048]{1,0:T(8,128)(2,1)S(1)}, bf16[48,2048]{1,0:T(8,128)(2,1)S(1)}, u32[]{:S(2)}, u32[]{:S(2)}) %collective-permute-start.16) | collective-permute-done | bytes 196640 | tf_op jit(solution)/shard_map/ppermute | solution.py:225
  49.1 1.6 %collective-permute-start.17 = (bf16[96,512]{1,0:T(8,128)(2,1)S(1)}, bf16[96,512]{1,0:T(8,128)(2,1)S(1)}, u32[]{:S(2)}, u32[]{:S(2)}) collective-permute-start(bf16[96,512]{1,0:T(8,128)(2,1)S(1)} %shard_map.116.refs_0_), channel_id=1, source_target_pairs={{0,1},{1,0},{2,3},{3,2},{4,5},{5,4},{6,7},{7,6},{8,9},{9,8},{10,11... | collective-permute-start | bytes 294920 | tf_op jit(solution)/shard_map/ppermute | solution.py:225
  56.0 1.6 %collective-permute-start.26 = (bf16[96,512]{1,0:T(8,128)(2,1)S(1)}, bf16[96,512]{1,0:T(8,128)(2,1)S(1)}, u32[]{:S(2)}, u32[]{:S(2)}) collective-permute-start(bf16[96,512]{1,0:T(8,128)(2,1)S(1)} %shard_map.119.refs_0_), channel_id=1, source_target_pairs={{0,3},{1,2},{2,1},{3,0},{4,7},{5,6},{6,5},{7,4},{8,11},{9,10},{10,... | collective-permute-start | bytes 294920 | tf_op jit(solution)/shard_map/ppermute | solution.py:225
  57.6 2.4 %collective-permute-done.19.refs_3_ = bf16[96,512]{1,0:T(8,128)(2,1)S(1)} collective-permute-done((bf16[96,512]{1,0:T(8,128)(2,1)S(1)}, bf16[96,512]{1,0:T(8,128)(2,1)S(1)}, u32[]{:S(2)}, u32[]{:S(2)}) %collective-permute-start.19) | collective-permute-done | bytes 98336 | tf_op jit(solution)/shard_map/ppermute | solution.py:225
  60.5 3.3 %collective-permute-done.25.refs_2_ = bf16[96,512]{1,0:T(8,128)(2,1)S(1)} collective-permute-done((bf16[96,512]{1,0:T(8,128)(2,1)S(1)}, bf16[96,512]{1,0:T(8,128)(2,1)S(1)}, u32[]{:S(2)}, u32[]{:S(2)}) %collective-permute-start.25) | collective-permute-done | bytes 98336 | tf_op jit(solution)/shard_map/ppermute | solution.py:225
  63.8 2.1 %collective-permute-start.20 = (bf16[4,48,512]{2,1,0:T(8,128)(2,1)S(1)}, bf16[4,48,512]{2,1,0:T(8,128)(2,1)S(1)}, u32[]{:S(2)}, u32[]{:S(2)}) collective-permute-start(bf16[4,48,512]{2,1,0:T(8,128)(2,1)S(1)} %get-tuple-element.38), channel_id=1, source_target_pairs={{0,16},{4,20},{8,24},{12,28},{16,0},{20,4},{24,8},{28,12},{1,17},{... | collective-permute-start | bytes 589832 | tf_op jit(solution)/shard_map/ppermute | solution.py:225
  68.6 1.7 %shard_map.110 = (bf16[4,128,576]{2,1,0:T(8,128)(2,1)S(1)}, bf16[4,128,288]{2,1,0:T(8,128)(2,1)S(1)}, bf16[4,128,288]{2,1,0:T(8,128)(2,1)S(1)}) custom-call(s32[1]{0:T(128)} %bitcast.2.me, f32[4,128]{1,0:T(4,128)S(1)} %pad_maximum_fusion.refs_0_, f32[4,128]{1,0:T(4,128)S(1)} %collective-permute-done.3.refs_1_, f32[4,128]{1,0:T(4,128)S(1)} %collective-permute-done.4.refs_2_, ...), custom_call_target="tpu_custom_call" | custom-call | flops 8388608 | bytes 1187844 | tf_op jit(solution)/shard_map/pallas_call | solution.py:29
  71.2 16.0 %collective-permute-done.20.refs_0_ = bf16[4,48,512]{2,1,0:T(8,128)(2,1)S(1)} collective-permute-done((bf16[4,48,512]{2,1,0:T(8,128)(2,1)S(1)}, bf16[4,48,512]{2,1,0:T(8,128)(2,1)S(1)}, u32[]{:S(2)}, u32[]{:S(2)}) %collective-permute-start.20) | collective-permute-done | bytes 196640 | tf_op jit(solution)/shard_map/ppermute | solution.py:225
  87.2 4.2 %collective-permute-done.21.refs_1_ = bf16[4,48,512]{2,1,0:T(8,128)(2,1)S(1)} collective-permute-done((bf16[4,48,512]{2,1,0:T(8,128)(2,1)S(1)}, bf16[4,48,512]{2,1,0:T(8,128)(2,1)S(1)}, u32[]{:S(2)}, u32[]{:S(2)}) %collective-permute-start.21) | collective-permute-done | bytes 196640 | tf_op jit(solution)/shard_map/ppermute | solution.py:225
  91.9 5.2 %collective-permute-done.27.refs_0_ = bf16[4,48,512]{2,1,0:T(8,128)(2,1)S(1)} collective-permute-done((bf16[4,48,512]{2,1,0:T(8,128)(2,1)S(1)}, bf16[4,48,512]{2,1,0:T(8,128)(2,1)S(1)}, u32[]{:S(2)}, u32[]{:S(2)}) %collective-permute-start.27) | collective-permute-done | bytes 196640 | tf_op jit(solution)/shard_map/ppermute | solution.py:225
  97.1 2.8 %collective-permute-done.28.refs_1_ = bf16[4,48,512]{2,1,0:T(8,128)(2,1)S(1)} collective-permute-done((bf16[4,48,512]{2,1,0:T(8,128)(2,1)S(1)}, bf16[4,48,512]{2,1,0:T(8,128)(2,1)S(1)}, u32[]{:S(2)}, u32[]{:S(2)}) %collective-permute-start.28) | collective-permute-done | bytes 196640 | tf_op jit(solution)/shard_map/ppermute | solution.py:225
  101.2 1.7 %collective-permute-start.29 = (f32[4,128]{1,0:T(4,128)S(1)}, f32[4,128]{1,0:T(4,128)S(1)}, u32[]{:S(2)}, u32[]{:S(2)}) collective-permute-start(f32[4,128]{1,0:T(4,128)S(1)} %get-tuple-element.46.refs_0_), channel_id=1, source_target_pairs={{0,1},{1,0},{2,3},{3,2},{4,5},{5,4},{6,7},{7,6},{8,9},{9,8},{10,11... | collective-permute-start | bytes 6152 | tf_op jit(solution)/shard_map/ppermute | solution.py:225
  104.8 1.6 %collective-permute-done.30.refs_2_ = f32[4,128]{1,0:T(4,128)S(1)} collective-permute-done((f32[4,128]{1,0:T(4,128)S(1)}, f32[4,128]{1,0:T(4,128)S(1)}, u32[]{:S(2)}, u32[]{:S(2)}) %collective-permute-start.30) | collective-permute-done | bytes 2080 | tf_op jit(solution)/shard_map/ppermute | solution.py:225
  106.5 2.4 %collective-permute-done.31.refs_3_ = f32[4,128]{1,0:T(4,128)S(1)} collective-permute-done((f32[4,128]{1,0:T(4,128)S(1)}, f32[4,128]{1,0:T(4,128)S(1)}, u32[]{:S(2)}, u32[]{:S(2)}) %collective-permute-start.31) | collective-permute-done | bytes 2080 | tf_op jit(solution)/shard_map/ppermute | solution.py:225
  (70 shorter events, 33.2 us)
Async XLA Ops:
  2.3 16.0 %collective-permute-start.6 = (bf16[48,2048]{1,0:T(8,128)(2,1)S(1)}, bf16[48,2048]{1,0:T(8,128)(2,1)S(1)}, u32[]{:S(2)}, u32[]{:S(2)}) collective-permute-start(bf16[48,2048]{1,0:T(8,128)(2,1)S(1)} %get-tuple-element.28), channel_id=1, source_target_pairs={{0,4},{4,0},{8,12},{12,8},{16,20},{20,16},{24,28},{28,24},{1,5},{5... | collective-permute-start | bytes 589832 | tf_op jit(solution)/shard_map/ppermute | solution.py:225
  2.3 18.9 %collective-permute-start.7 = (bf16[48,2048]{1,0:T(8,128)(2,1)S(1)}, bf16[48,2048]{1,0:T(8,128)(2,1)S(1)}, u32[]{:S(2)}, u32[]{:S(2)}) collective-permute-start(bf16[48,2048]{1,0:T(8,128)(2,1)S(1)} %get-tuple-element.29), channel_id=1, source_target_pairs={{0,8},{4,12},{8,0},{12,4},{16,24},{20,28},{24,16},{28,20},{1,9},{5... | collective-permute-start | bytes 589832 | tf_op jit(solution)/shard_map/ppermute | solution.py:225
  2.8 21.4 %collective-permute-start.8 = (bf16[48,2048]{1,0:T(8,128)(2,1)S(1)}, bf16[48,2048]{1,0:T(8,128)(2,1)S(1)}, u32[]{:S(2)}, u32[]{:S(2)}) collective-permute-start(bf16[48,2048]{1,0:T(8,128)(2,1)S(1)} %get-tuple-element.30), channel_id=1, source_target_pairs={{0,12},{4,8},{8,4},{12,0},{16,28},{20,24},{24,20},{28,16},{1,13},{... | collective-permute-start | bytes 589832 | tf_op jit(solution)/shard_map/ppermute | solution.py:225
  10.6 24.4 %collective-permute-start.22 = (bf16[48,2048]{1,0:T(8,128)(2,1)S(1)}, bf16[48,2048]{1,0:T(8,128)(2,1)S(1)}, u32[]{:S(2)}, u32[]{:S(2)}) collective-permute-start(bf16[48,2048]{1,0:T(8,128)(2,1)S(1)} %get-tuple-element.41), channel_id=1, source_target_pairs={{0,24},{4,28},{8,16},{12,20},{16,8},{20,12},{24,0},{28,4},{1,25},{... | collective-permute-start | bytes 589832 | tf_op jit(solution)/shard_map/ppermute | solution.py:225
  13.6 24.9 %collective-permute-start.23 = (bf16[48,2048]{1,0:T(8,128)(2,1)S(1)}, bf16[48,2048]{1,0:T(8,128)(2,1)S(1)}, u32[]{:S(2)}, u32[]{:S(2)}) collective-permute-start(bf16[48,2048]{1,0:T(8,128)(2,1)S(1)} %get-tuple-element.42), channel_id=1, source_target_pairs={{0,28},{4,24},{8,20},{12,16},{16,12},{20,8},{24,4},{28,0},{1,29},{... | collective-permute-start | bytes 589832 | tf_op jit(solution)/shard_map/ppermute | solution.py:225
  18.4 8.0 %collective-permute-start = (bf16[128,512]{1,0:T(8,128)(2,1)S(1)}, bf16[128,512]{1,0:T(8,128)(2,1)S(1)}, u32[]{:S(2)}, u32[]{:S(2)}) collective-permute-start(bf16[128,512]{1,0:T(8,128)(2,1)S(1)} %shard_map.109.refs_0_), channel_id=1, source_target_pairs={{0,1},{1,0},{2,3},{3,2},{4,5},{5,4},{6,7},{7,6},{8,9},{9,8},{10,11... | collective-permute-start | bytes 393224 | tf_op jit(solution)/shard_map/ppermute | solution.py:225
  21.2 21.5 %collective-permute-start.15 = (bf16[48,2048]{1,0:T(8,128)(2,1)S(1)}, bf16[48,2048]{1,0:T(8,128)(2,1)S(1)}, u32[]{:S(2)}, u32[]{:S(2)}) collective-permute-start(bf16[48,2048]{1,0:T(8,128)(2,1)S(1)} %get-tuple-element.36), channel_id=1, source_target_pairs={{0,16},{4,20},{8,24},{12,28},{16,0},{20,4},{24,8},{28,12},{1,17},{... | collective-permute-start | bytes 589832 | tf_op jit(solution)/shard_map/ppermute | solution.py:225
  24.2 21.0 %collective-permute-start.16 = (bf16[48,2048]{1,0:T(8,128)(2,1)S(1)}, bf16[48,2048]{1,0:T(8,128)(2,1)S(1)}, u32[]{:S(2)}, u32[]{:S(2)}) collective-permute-start(bf16[48,2048]{1,0:T(8,128)(2,1)S(1)} %get-tuple-element.37), channel_id=1, source_target_pairs={{0,20},{4,16},{8,28},{12,24},{16,4},{20,0},{24,12},{28,8},{1,21},{... | collective-permute-start | bytes 589832 | tf_op jit(solution)/shard_map/ppermute | solution.py:225
  26.4 21.2 %collective-permute-start.10 = (bf16[192,512]{1,0:T(8,128)(2,1)S(1)}, bf16[192,512]{1,0:T(8,128)(2,1)S(1)}, u32[]{:S(2)}, u32[]{:S(2)}) collective-permute-start(bf16[192,512]{1,0:T(8,128)(2,1)S(1)} %shard_map.113.refs_0_), channel_id=1, source_target_pairs={{0,2},{1,3},{2,0},{3,1},{4,6},{5,7},{6,4},{7,5},{8,10},{9,11},{10,... | collective-permute-start | bytes 589832 | tf_op jit(solution)/shard_map/ppermute | solution.py:225
  35.1 14.0 %collective-permute-start.11 = (bf16[192,512]{1,0:T(8,128)(2,1)S(1)}, bf16[192,512]{1,0:T(8,128)(2,1)S(1)}, u32[]{:S(2)}, u32[]{:S(2)}) collective-permute-start(bf16[192,512]{1,0:T(8,128)(2,1)S(1)} %shard_map.113.refs_0_), channel_id=1, source_target_pairs={{0,3},{1,2},{2,1},{3,0},{4,7},{5,6},{6,5},{7,4},{8,11},{9,10},{10,... | collective-permute-start | bytes 589832 | tf_op jit(solution)/shard_map/ppermute | solution.py:225
  38.6 12.1 %collective-permute-start.9 = (bf16[192,512]{1,0:T(8,128)(2,1)S(1)}, bf16[192,512]{1,0:T(8,128)(2,1)S(1)}, u32[]{:S(2)}, u32[]{:S(2)}) collective-permute-start(bf16[192,512]{1,0:T(8,128)(2,1)S(1)} %shard_map.113.refs_0_), channel_id=1, source_target_pairs={{0,1},{1,0},{2,3},{3,2},{4,5},{5,4},{6,7},{7,6},{8,9},{9,8},{10,11... | collective-permute-start | bytes 589832 | tf_op jit(solution)/shard_map/ppermute | solution.py:225
  42.8 9.9 %collective-permute-start.1 = (bf16[128,512]{1,0:T(8,128)(2,1)S(1)}, bf16[128,512]{1,0:T(8,128)(2,1)S(1)}, u32[]{:S(2)}, u32[]{:S(2)}) collective-permute-start(bf16[128,512]{1,0:T(8,128)(2,1)S(1)} %shard_map.109.refs_0_), channel_id=1, source_target_pairs={{0,2},{1,3},{2,0},{3,1},{4,6},{5,7},{6,4},{7,5},{8,10},{9,11},{10,... | collective-permute-start | bytes 393224 | tf_op jit(solution)/shard_map/ppermute | solution.py:225
  45.2 7.6 %collective-permute-start.2 = (bf16[128,512]{1,0:T(8,128)(2,1)S(1)}, bf16[128,512]{1,0:T(8,128)(2,1)S(1)}, u32[]{:S(2)}, u32[]{:S(2)}) collective-permute-start(bf16[128,512]{1,0:T(8,128)(2,1)S(1)} %shard_map.109.refs_0_), channel_id=1, source_target_pairs={{0,3},{1,2},{2,1},{3,0},{4,7},{5,6},{6,5},{7,4},{8,11},{9,10},{10,... | collective-permute-start | bytes 393224 | tf_op jit(solution)/shard_map/ppermute | solution.py:225
  47.6 6.3 %collective-permute-start.24 = (bf16[96,512]{1,0:T(8,128)(2,1)S(1)}, bf16[96,512]{1,0:T(8,128)(2,1)S(1)}, u32[]{:S(2)}, u32[]{:S(2)}) collective-permute-start(bf16[96,512]{1,0:T(8,128)(2,1)S(1)} %shard_map.119.refs_0_), channel_id=1, source_target_pairs={{0,1},{1,0},{2,3},{3,2},{4,5},{5,4},{6,7},{7,6},{8,9},{9,8},{10,11... | collective-permute-start | bytes 294920 | tf_op jit(solution)/shard_map/ppermute | solution.py:225
  52.7 13.7 %collective-permute-start.12 = (bf16[4,48,512]{2,1,0:T(8,128)(2,1)S(1)}, bf16[4,48,512]{2,1,0:T(8,128)(2,1)S(1)}, u32[]{:S(2)}, u32[]{:S(2)}) collective-permute-start(bf16[4,48,512]{2,1,0:T(8,128)(2,1)S(1)} %get-tuple-element.32), channel_id=1, source_target_pairs={{0,4},{4,0},{8,12},{12,8},{16,20},{20,16},{24,28},{28,24},{1,5},{5... | collective-permute-start | bytes 589832 | tf_op jit(solution)/shard_map/ppermute | solution.py:225
  52.8 15.0 %collective-permute-start.13 = (bf16[4,48,512]{2,1,0:T(8,128)(2,1)S(1)}, bf16[4,48,512]{2,1,0:T(8,128)(2,1)S(1)}, u32[]{:S(2)}, u32[]{:S(2)}) collective-permute-start(bf16[4,48,512]{2,1,0:T(8,128)(2,1)S(1)} %get-tuple-element.33), channel_id=1, source_target_pairs={{0,8},{4,12},{8,0},{12,4},{16,24},{20,28},{24,16},{28,20},{1,9},{5... | collective-permute-start | bytes 589832 | tf_op jit(solution)/shard_map/ppermute | solution.py:225
  53.9 6.2 %collective-permute-start.19 = (bf16[96,512]{1,0:T(8,128)(2,1)S(1)}, bf16[96,512]{1,0:T(8,128)(2,1)S(1)}, u32[]{:S(2)}, u32[]{:S(2)}) collective-permute-start(bf16[96,512]{1,0:T(8,128)(2,1)S(1)} %shard_map.116.refs_0_), channel_id=1, source_target_pairs={{0,3},{1,2},{2,1},{3,0},{4,7},{5,6},{6,5},{7,4},{8,11},{9,10},{10,... | collective-permute-start | bytes 294920 | tf_op jit(solution)/shard_map/ppermute | solution.py:225
  55.1 8.6 %collective-permute-start.25 = (bf16[96,512]{1,0:T(8,128)(2,1)S(1)}, bf16[96,512]{1,0:T(8,128)(2,1)S(1)}, u32[]{:S(2)}, u32[]{:S(2)}) collective-permute-start(bf16[96,512]{1,0:T(8,128)(2,1)S(1)} %shard_map.119.refs_0_), channel_id=1, source_target_pairs={{0,2},{1,3},{2,0},{3,1},{4,6},{5,7},{6,4},{7,5},{8,10},{9,11},{10,... | collective-permute-start | bytes 294920 | tf_op jit(solution)/shard_map/ppermute | solution.py:225
  56.0 9.8 %collective-permute-start.26 = (bf16[96,512]{1,0:T(8,128)(2,1)S(1)}, bf16[96,512]{1,0:T(8,128)(2,1)S(1)}, u32[]{:S(2)}, u32[]{:S(2)}) collective-permute-start(bf16[96,512]{1,0:T(8,128)(2,1)S(1)} %shard_map.119.refs_0_), channel_id=1, source_target_pairs={{0,3},{1,2},{2,1},{3,0},{4,7},{5,6},{6,5},{7,4},{8,11},{9,10},{10,... | collective-permute-start | bytes 294920 | tf_op jit(solution)/shard_map/ppermute | solution.py:225
  60.1 10.3 %collective-permute-start.14 = (bf16[4,48,512]{2,1,0:T(8,128)(2,1)S(1)}, bf16[4,48,512]{2,1,0:T(8,128)(2,1)S(1)}, u32[]{:S(2)}, u32[]{:S(2)}) collective-permute-start(bf16[4,48,512]{2,1,0:T(8,128)(2,1)S(1)} %get-tuple-element.34), channel_id=1, source_target_pairs={{0,12},{4,8},{8,4},{12,0},{16,28},{20,24},{24,20},{28,16},{1,13},{... | collective-permute-start | bytes 589832 | tf_op jit(solution)/shard_map/ppermute | solution.py:225
  63.8 23.5 %collective-permute-start.20 = (bf16[4,48,512]{2,1,0:T(8,128)(2,1)S(1)}, bf16[4,48,512]{2,1,0:T(8,128)(2,1)S(1)}, u32[]{:S(2)}, u32[]{:S(2)}) collective-permute-start(bf16[4,48,512]{2,1,0:T(8,128)(2,1)S(1)} %get-tuple-element.38), channel_id=1, source_target_pairs={{0,16},{4,20},{8,24},{12,28},{16,0},{20,4},{24,8},{28,12},{1,17},{... | collective-permute-start | bytes 589832 | tf_op jit(solution)/shard_map/ppermute | solution.py:225
  65.8 25.6 %collective-permute-start.21 = (bf16[4,48,512]{2,1,0:T(8,128)(2,1)S(1)}, bf16[4,48,512]{2,1,0:T(8,128)(2,1)S(1)}, u32[]{:S(2)}, u32[]{:S(2)}) collective-permute-start(bf16[4,48,512]{2,1,0:T(8,128)(2,1)S(1)} %get-tuple-element.39), channel_id=1, source_target_pairs={{0,20},{4,16},{8,28},{12,24},{16,4},{20,0},{24,12},{28,8},{1,21},{... | collective-permute-start | bytes 589832 | tf_op jit(solution)/shard_map/ppermute | solution.py:225
  66.4 30.7 %collective-permute-start.27 = (bf16[4,48,512]{2,1,0:T(8,128)(2,1)S(1)}, bf16[4,48,512]{2,1,0:T(8,128)(2,1)S(1)}, u32[]{:S(2)}, u32[]{:S(2)}) collective-permute-start(bf16[4,48,512]{2,1,0:T(8,128)(2,1)S(1)} %get-tuple-element.43), channel_id=1, source_target_pairs={{0,24},{4,28},{8,16},{12,20},{16,8},{20,12},{24,0},{28,4},{1,25},{... | collective-permute-start | bytes 589832 | tf_op jit(solution)/shard_map/ppermute | solution.py:225
  67.8 32.1 %collective-permute-start.28 = (bf16[4,48,512]{2,1,0:T(8,128)(2,1)S(1)}, bf16[4,48,512]{2,1,0:T(8,128)(2,1)S(1)}, u32[]{:S(2)}, u32[]{:S(2)}) collective-permute-start(bf16[4,48,512]{2,1,0:T(8,128)(2,1)S(1)} %get-tuple-element.44), channel_id=1, source_target_pairs={{0,28},{4,24},{8,20},{12,16},{16,12},{20,8},{24,4},{28,0},{1,29},{... | collective-permute-start | bytes 589832 | tf_op jit(solution)/shard_map/ppermute | solution.py:225
  (15 other events, 87.6 us)

commit v5 on v4

--- a/solution.py
+++ b/solution.py
@@ -178,39 +178,34 @@
         refs[-1][m] = total[m] + weighted(table, refs[:-1], m)
 
 
-def finish_kernel(blocks, lanes, total, table, *refs):
+def finish_kernel(blocks, total, table, *refs):
     returned = refs[:-2]
     moe, squares = refs[-2:]
-    ones = jnp.ones((8, lanes), F32)
+    count = moe.shape[1]
+    lane = lax.broadcasted_iota(jnp.int32, (count, count), 1)
+    sums = jnp.zeros((count, count), F32)
     for m in range(blocks):
         rounded = (total[m] + weighted(table, returned, m)).astype(BF16)
         moe[m] = rounded
         wide = rounded.astype(F32)
-        wide = wide * wide
-        folded = functools.reduce(
-            jnp.add,
-            [wide[:, at : at + lanes] for at in range(0, wide.shape[1], lanes)],
-        )
-        sums = lax.dot_general(
-            ones,
-            folded,
-            (((1,), (1,)), ((), ())),
-            precision=lax.Precision.HIGHEST,
-            preferred_element_type=F32,
-        )
-        squares[m : m + 1, :] = sums[:1]
+        sums = jnp.where(lane == m, jnp.sum(wide * wide, axis=1, keepdims=True), sums)
+    squares[...] = sums.T[:blocks, :]
 
 
 def scale_kernel(blocks, width, me, moe, gain, *refs):
     squares, out, ready, sems = refs[:blocks], *refs[blocks:]
     count = moe.shape[1]
-    copies = []
+    totals = []
     for m in range(blocks):
         total = squares[0][m : m + 1, :]
         for p in range(1, blocks):
             total = total + squares[p][m ^ p : (m ^ p) + 1, :]
-        scale = lax.rsqrt(total / width + 1e-06)
-        column = jnp.broadcast_to(scale, (count, count)).T[:, :1]
+        totals.append(lax.rsqrt(total / width + 1e-06))
+    totals.append(jnp.zeros((count - blocks, count), F32))
+    columns = jnp.concatenate(totals, axis=0).T
+    copies = []
+    for m in range(blocks):
+        column = columns[:, m : m + 1]
         ready[m] = (moe[m].astype(F32) * column * gain[...]).astype(BF16)
         first = pl.multiple_of((me[0] ^ m) * count, count)
         copy = pltpu.make_async_copy(ready.at[m], out.at[pl.ds(first, count), :], sems.at[m])
@@ -278,7 +273,7 @@
         [both],
         [expert_gate[0], expert_up[0], pieces[0]],
         count * width,
-        far=(0, 1, 2),
+        far=(0, 1),
         scratch=[pltpu.SemaphoreType.DMA((2,))],
     )
     (shared,) = call(
@@ -335,7 +330,7 @@
         2 * blocks * count * local * 3 * quarter * capacity,
     )
     moe, squares = call(
-        functools.partial(finish_kernel, blocks, 128),
+        functools.partial(finish_kernel, blocks),
         [
             jax.ShapeDtypeStruct((blocks, count, local), BF16),
             jax.ShapeDtypeStruct((blocks, count), F32),

time: 110 us -> 109 us (level)
    unnamed x14 -> x10, local copies, waits for them, and re-layouts: 2.43 us -> 1.75 us
where the time goes in v5:
time: 109 us
  waiting for transfers between devices  56.9 us (52%)
  starting transfers between devices  32.9 us (30%)
  Pallas kernels  15.7 us (14%)
  local copies, waits for them, and re-layouts  1.75 us (2%)
  other arithmetic  1.37 us (1%)
    ppermute x32, waiting for transfers between devices, swap(): return lax.ppermute(array, axis, [(s, s ^ k) for s in range(size)])  56.9 us
    ppermute x32, starting transfers between devices, swap(): return lax.ppermute(array, axis, [(s, s ^ k) for s in range(size)])  32.9 us
    pallas_call x14, Pallas kernels, call(): pl.pallas_call(kernel, out_shape=outs, in_specs=specs, out_specs=[HBM if...  15.7 us
  transfers between devices with their start and end apart: 32, of which 15 were waited for; matrix products, arithmetic and copies ran while one was open for 1% of the time, Pallas kernels for 11%

profile of v5, /device:TPU:10, one launch (start us, length us, event | category | flops | bytes accessed | tf_op | source)
XLA Modules:
  0.0 108.9 jit_solution(11784440232075120143)
XLA Ops:
  0.0 1.6 %shard_map.111 = (bf16[48,2048]{1,0:T(8,128)(2,1)S(1)}, bf16[48,2048]{1,0:T(8,128)(2,1)S(1)}, bf16[48,2048]{1,0:T(8,128)(2,1)S(1)}, bf16[48,2048]{1,0:T(8,128)(2...) custom-call(s32[1]{0:T(128)} %bitcast.2.me, ...), custom_call_target="tpu_custom_call" | custom-call | flops 201326592 | bytes 2098180 | tf_op jit(solution)/shard_map/pallas_call | solution.py:29
  5.5 1.5 %collective-permute-start.4 = (f32[4,128]{1,0:T(4,128)S(1)}, f32[4,128]{1,0:T(4,128)S(1)}, u32[]{:S(2)}, u32[]{:S(2)}) collective-permute-start(f32[4,128]{1,0:T(4,128)S(1)} %pad_maximum_fusion.refs_0_), channel_id=1, source_target_pairs={{0,2},{1,3},{2,0},{3,1},{4,6},{5,7},{6,4},{7,5},{8,10},{9,11},{10,... | collective-permute-start | bytes 6152 | tf_op jit(solution)/shard_map/ppermute | solution.py:220
  7.0 1.5 %collective-permute-done.3.refs_1_ = f32[4,128]{1,0:T(4,128)S(1)} collective-permute-done((f32[4,128]{1,0:T(4,128)S(1)}, f32[4,128]{1,0:T(4,128)S(1)}, u32[]{:S(2)}, u32[]{:S(2)}) %collective-permute-start.3) | collective-permute-done | bytes 2080 | tf_op jit(solution)/shard_map/ppermute | solution.py:220
  8.5 1.5 %collective-permute-start.5 = (f32[4,128]{1,0:T(4,128)S(1)}, f32[4,128]{1,0:T(4,128)S(1)}, u32[]{:S(2)}, u32[]{:S(2)}) collective-permute-start(f32[4,128]{1,0:T(4,128)S(1)} %pad_maximum_fusion.refs_0_), channel_id=1, source_target_pairs={{0,3},{1,2},{2,1},{3,0},{4,7},{5,6},{6,5},{7,4},{8,11},{9,10},{10,... | collective-permute-start | bytes 6152 | tf_op jit(solution)/shard_map/ppermute | solution.py:220
  10.0 1.6 %collective-permute-start.22 = (bf16[48,2048]{1,0:T(8,128)(2,1)S(1)}, bf16[48,2048]{1,0:T(8,128)(2,1)S(1)}, u32[]{:S(2)}, u32[]{:S(2)}) collective-permute-start(bf16[48,2048]{1,0:T(8,128)(2,1)S(1)} %get-tuple-element.41), channel_id=1, source_target_pairs={{0,24},{4,28},{8,16},{12,20},{16,8},{20,12},{24,0},{28,4},{1,25},{... | collective-permute-start | bytes 589832 | tf_op jit(solution)/shard_map/ppermute | solution.py:220
  14.7 3.0 %shard_map.109.refs_0_ = bf16[128,512]{1,0:T(8,128)(2,1)S(1)} custom-call(bf16[128,2048]{1,0:T(8,128)(2,1)S(1)} %copy-done.1, f32[1,2048]{1,0:T(1,128)S(1)} %bitcast.13, bf16[2048,512]{1,0:T(8,128)(2,1)} %gate.1, bf16[2048,512]{1,0:T(8,128)(2,1)} %upward.1), custom_call_target="tpu_custom_call" | custom-call | flops 536870912 | bytes 4857856 | tf_op jit(solution)/shard_map/pallas_call | solution.py:29
  18.3 2.2 %shard_map.112.refs_5_.refs_3_ = bf16[2048,1024]{1,0:T(8,128)(2,1)S(1)} custom-call(bf16[2048,512]{1,0:T(8,128)(2,1)} %bitcast.18, bf16[2048,512]{1,0:T(8,128)(2,1)} %bitcast.19, bf16[48,2048]{1,0:T(8,128)(2,1)S(1)} %get-tuple-element.27.held.refs_0_), custom_call_target="tpu_custom_call" | custom-call | flops 262144 | bytes 8585216 | tf_op jit(solution)/shard_map/pallas_call | solution.py:29
  20.6 3.0 %collective-permute-start.15 = (bf16[48,2048]{1,0:T(8,128)(2,1)S(1)}, bf16[48,2048]{1,0:T(8,128)(2,1)S(1)}, u32[]{:S(2)}, u32[]{:S(2)}) collective-permute-start(bf16[48,2048]{1,0:T(8,128)(2,1)S(1)} %get-tuple-element.36), channel_id=1, source_target_pairs={{0,16},{4,20},{8,24},{12,28},{16,0},{20,4},{24,8},{28,12},{1,17},{... | collective-permute-start | bytes 589832 | tf_op jit(solution)/shard_map/ppermute | solution.py:220
  27.1 7.5 %collective-permute-done.22.refs_0_ = bf16[48,2048]{1,0:T(8,128)(2,1)S(1)} collective-permute-done((bf16[48,2048]{1,0:T(8,128)(2,1)S(1)}, bf16[48,2048]{1,0:T(8,128)(2,1)S(1)}, u32[]{:S(2)}, u32[]{:S(2)}) %collective-permute-start.22) | collective-permute-done | bytes 196640 | tf_op jit(solution)/shard_map/ppermute | solution.py:220
  34.6 3.4 %collective-permute-done.23.refs_1_ = bf16[48,2048]{1,0:T(8,128)(2,1)S(1)} collective-permute-done((bf16[48,2048]{1,0:T(8,128)(2,1)S(1)}, bf16[48,2048]{1,0:T(8,128)(2,1)S(1)}, u32[]{:S(2)}, u32[]{:S(2)}) %collective-permute-start.23) | collective-permute-done | bytes 196640 | tf_op jit(solution)/shard_map/ppermute | solution.py:220
  38.0 1.5 %collective-permute-start.9 = (bf16[192,512]{1,0:T(8,128)(2,1)S(1)}, bf16[192,512]{1,0:T(8,128)(2,1)S(1)}, u32[]{:S(2)}, u32[]{:S(2)}) collective-permute-start(bf16[192,512]{1,0:T(8,128)(2,1)S(1)} %shard_map.113.refs_0_), channel_id=1, source_target_pairs={{0,1},{1,0},{2,3},{3,2},{4,5},{5,4},{6,7},{7,6},{8,9},{9,8},{10,11... | collective-permute-start | bytes 589832 | tf_op jit(solution)/shard_map/ppermute | solution.py:220
  39.4 2.7 %collective-permute-done.15.refs_0_ = bf16[48,2048]{1,0:T(8,128)(2,1)S(1)} collective-permute-done((bf16[48,2048]{1,0:T(8,128)(2,1)S(1)}, bf16[48,2048]{1,0:T(8,128)(2,1)S(1)}, u32[]{:S(2)}, u32[]{:S(2)}) %collective-permute-start.15) | collective-permute-done | bytes 196640 | tf_op jit(solution)/shard_map/ppermute | solution.py:220
  42.7 1.9 %collective-permute-done.16.refs_1_ = bf16[48,2048]{1,0:T(8,128)(2,1)S(1)} collective-permute-done((bf16[48,2048]{1,0:T(8,128)(2,1)S(1)}, bf16[48,2048]{1,0:T(8,128)(2,1)S(1)}, u32[]{:S(2)}, u32[]{:S(2)}) %collective-permute-start.16) | collective-permute-done | bytes 196640 | tf_op jit(solution)/shard_map/ppermute | solution.py:220
  48.6 1.6 %collective-permute-start.17 = (bf16[96,512]{1,0:T(8,128)(2,1)S(1)}, bf16[96,512]{1,0:T(8,128)(2,1)S(1)}, u32[]{:S(2)}, u32[]{:S(2)}) collective-permute-start(bf16[96,512]{1,0:T(8,128)(2,1)S(1)} %shard_map.116.refs_0_), channel_id=1, source_target_pairs={{0,1},{1,0},{2,3},{3,2},{4,5},{5,4},{6,7},{7,6},{8,9},{9,8},{10,11... | collective-permute-start | bytes 294920 | tf_op jit(solution)/shard_map/ppermute | solution.py:220
  57.0 2.8 %collective-permute-done.19.refs_3_ = bf16[96,512]{1,0:T(8,128)(2,1)S(1)} collective-permute-done((bf16[96,512]{1,0:T(8,128)(2,1)S(1)}, bf16[96,512]{1,0:T(8,128)(2,1)S(1)}, u32[]{:S(2)}, u32[]{:S(2)}) %collective-permute-start.19) | collective-permute-done | bytes 98336 | tf_op jit(solution)/shard_map/ppermute | solution.py:220
  60.2 3.1 %collective-permute-done.25.refs_2_ = bf16[96,512]{1,0:T(8,128)(2,1)S(1)} collective-permute-done((bf16[96,512]{1,0:T(8,128)(2,1)S(1)}, bf16[96,512]{1,0:T(8,128)(2,1)S(1)}, u32[]{:S(2)}, u32[]{:S(2)}) %collective-permute-start.25) | collective-permute-done | bytes 98336 | tf_op jit(solution)/shard_map/ppermute | solution.py:220
  63.3 1.9 %collective-permute-start.20 = (bf16[4,48,512]{2,1,0:T(8,128)(2,1)S(1)}, bf16[4,48,512]{2,1,0:T(8,128)(2,1)S(1)}, u32[]{:S(2)}, u32[]{:S(2)}) collective-permute-start(bf16[4,48,512]{2,1,0:T(8,128)(2,1)S(1)} %get-tuple-element.38), channel_id=1, source_target_pairs={{0,16},{4,20},{8,24},{12,28},{16,0},{20,4},{24,8},{28,12},{1,17},{... | collective-permute-start | bytes 589832 | tf_op jit(solution)/shard_map/ppermute | solution.py:220
  68.1 1.7 %shard_map.110 = (bf16[4,128,576]{2,1,0:T(8,128)(2,1)S(1)}, bf16[4,128,288]{2,1,0:T(8,128)(2,1)S(1)}, bf16[4,128,288]{2,1,0:T(8,128)(2,1)S(1)}) custom-call(s32[1]{0:T(128)} %bitcast.2.me, f32[4,128]{1,0:T(4,128)S(1)} %pad_maximum_fusion.refs_0_, f32[4,128]{1,0:T(4,128)S(1)} %collective-permute-done.3.refs_1_, f32[4,128]{1,0:T(4,128)S(1)} %collective-permute-done.4.refs_2_, ...), custom_call_target="tpu_custom_call" | custom-call | flops 8388608 | bytes 1187844 | tf_op jit(solution)/shard_map/pallas_call | solution.py:29
  70.7 16.0 %collective-permute-done.20.refs_0_ = bf16[4,48,512]{2,1,0:T(8,128)(2,1)S(1)} collective-permute-done((bf16[4,48,512]{2,1,0:T(8,128)(2,1)S(1)}, bf16[4,48,512]{2,1,0:T(8,128)(2,1)S(1)}, u32[]{:S(2)}, u32[]{:S(2)}) %collective-permute-start.20) | collective-permute-done | bytes 196640 | tf_op jit(solution)/shard_map/ppermute | solution.py:220
  86.7 4.2 %collective-permute-done.21.refs_1_ = bf16[4,48,512]{2,1,0:T(8,128)(2,1)S(1)} collective-permute-done((bf16[4,48,512]{2,1,0:T(8,128)(2,1)S(1)}, bf16[4,48,512]{2,1,0:T(8,128)(2,1)S(1)}, u32[]{:S(2)}, u32[]{:S(2)}) %collective-permute-start.21) | collective-permute-done | bytes 196640 | tf_op jit(solution)/shard_map/ppermute | solution.py:220
  91.3 5.1 %collective-permute-done.27.refs_0_ = bf16[4,48,512]{2,1,0:T(8,128)(2,1)S(1)} collective-permute-done((bf16[4,48,512]{2,1,0:T(8,128)(2,1)S(1)}, bf16[4,48,512]{2,1,0:T(8,128)(2,1)S(1)}, u32[]{:S(2)}, u32[]{:S(2)}) %collective-permute-start.27) | collective-permute-done | bytes 196640 | tf_op jit(solution)/shard_map/ppermute | solution.py:220
  96.4 3.2 %collective-permute-done.28.refs_1_ = bf16[4,48,512]{2,1,0:T(8,128)(2,1)S(1)} collective-permute-done((bf16[4,48,512]{2,1,0:T(8,128)(2,1)S(1)}, bf16[4,48,512]{2,1,0:T(8,128)(2,1)S(1)}, u32[]{:S(2)}, u32[]{:S(2)}) %collective-permute-start.28) | collective-permute-done | bytes 196640 | tf_op jit(solution)/shard_map/ppermute | solution.py:220
  101.6 1.7 %collective-permute-start.30 = (f32[4,128]{1,0:T(4,128)S(1)}, f32[4,128]{1,0:T(4,128)S(1)}, u32[]{:S(2)}, u32[]{:S(2)}) collective-permute-start(f32[4,128]{1,0:T(4,128)S(1)} %get-tuple-element.46.refs_0_), channel_id=1, source_target_pairs={{0,2},{1,3},{2,0},{3,1},{4,6},{5,7},{6,4},{7,5},{8,10},{9,11},{10,... | collective-permute-start | bytes 6152 | tf_op jit(solution)/shard_map/ppermute | solution.py:220
  105.1 2.6 %collective-permute-done.31.refs_3_ = f32[4,128]{1,0:T(4,128)S(1)} collective-permute-done((f32[4,128]{1,0:T(4,128)S(1)}, f32[4,128]{1,0:T(4,128)S(1)}, u32[]{:S(2)}, u32[]{:S(2)}) %collective-permute-start.31) | collective-permute-done | bytes 2080 | tf_op jit(solution)/shard_map/ppermute | solution.py:220
  (66 shorter events, 31.8 us)
Async XLA Ops:
  1.6 16.1 %collective-permute-start.6 = (bf16[48,2048]{1,0:T(8,128)(2,1)S(1)}, bf16[48,2048]{1,0:T(8,128)(2,1)S(1)}, u32[]{:S(2)}, u32[]{:S(2)}) collective-permute-start(bf16[48,2048]{1,0:T(8,128)(2,1)S(1)} %get-tuple-element.28), channel_id=1, source_target_pairs={{0,4},{4,0},{8,12},{12,8},{16,20},{20,16},{24,28},{28,24},{1,5},{5... | collective-permute-start | bytes 589832 | tf_op jit(solution)/shard_map/ppermute | solution.py:220
  1.7 18.9 %collective-permute-start.7 = (bf16[48,2048]{1,0:T(8,128)(2,1)S(1)}, bf16[48,2048]{1,0:T(8,128)(2,1)S(1)}, u32[]{:S(2)}, u32[]{:S(2)}) collective-permute-start(bf16[48,2048]{1,0:T(8,128)(2,1)S(1)} %get-tuple-element.29), channel_id=1, source_target_pairs={{0,8},{4,12},{8,0},{12,4},{16,24},{20,28},{24,16},{28,20},{1,9},{5... | collective-permute-start | bytes 589832 | tf_op jit(solution)/shard_map/ppermute | solution.py:220
  2.2 21.4 %collective-permute-start.8 = (bf16[48,2048]{1,0:T(8,128)(2,1)S(1)}, bf16[48,2048]{1,0:T(8,128)(2,1)S(1)}, u32[]{:S(2)}, u32[]{:S(2)}) collective-permute-start(bf16[48,2048]{1,0:T(8,128)(2,1)S(1)} %get-tuple-element.30), channel_id=1, source_target_pairs={{0,12},{4,8},{8,4},{12,0},{16,28},{20,24},{24,20},{28,16},{1,13},{... | collective-permute-start | bytes 589832 | tf_op jit(solution)/shard_map/ppermute | solution.py:220
  10.0 24.6 %collective-permute-start.22 = (bf16[48,2048]{1,0:T(8,128)(2,1)S(1)}, bf16[48,2048]{1,0:T(8,128)(2,1)S(1)}, u32[]{:S(2)}, u32[]{:S(2)}) collective-permute-start(bf16[48,2048]{1,0:T(8,128)(2,1)S(1)} %get-tuple-element.41), channel_id=1, source_target_pairs={{0,24},{4,28},{8,16},{12,20},{16,8},{20,12},{24,0},{28,4},{1,25},{... | collective-permute-start | bytes 589832 | tf_op jit(solution)/shard_map/ppermute | solution.py:220
  13.0 24.9 %collective-permute-start.23 = (bf16[48,2048]{1,0:T(8,128)(2,1)S(1)}, bf16[48,2048]{1,0:T(8,128)(2,1)S(1)}, u32[]{:S(2)}, u32[]{:S(2)}) collective-permute-start(bf16[48,2048]{1,0:T(8,128)(2,1)S(1)} %get-tuple-element.42), channel_id=1, source_target_pairs={{0,28},{4,24},{8,20},{12,16},{16,12},{20,8},{24,4},{28,0},{1,29},{... | collective-permute-start | bytes 589832 | tf_op jit(solution)/shard_map/ppermute | solution.py:220
  17.7 8.0 %collective-permute-start = (bf16[128,512]{1,0:T(8,128)(2,1)S(1)}, bf16[128,512]{1,0:T(8,128)(2,1)S(1)}, u32[]{:S(2)}, u32[]{:S(2)}) collective-permute-start(bf16[128,512]{1,0:T(8,128)(2,1)S(1)} %shard_map.109.refs_0_), channel_id=1, source_target_pairs={{0,1},{1,0},{2,3},{3,2},{4,5},{5,4},{6,7},{7,6},{8,9},{9,8},{10,11... | collective-permute-start | bytes 393224 | tf_op jit(solution)/shard_map/ppermute | solution.py:220
  20.6 21.6 %collective-permute-start.15 = (bf16[48,2048]{1,0:T(8,128)(2,1)S(1)}, bf16[48,2048]{1,0:T(8,128)(2,1)S(1)}, u32[]{:S(2)}, u32[]{:S(2)}) collective-permute-start(bf16[48,2048]{1,0:T(8,128)(2,1)S(1)} %get-tuple-element.36), channel_id=1, source_target_pairs={{0,16},{4,20},{8,24},{12,28},{16,0},{20,4},{24,8},{28,12},{1,17},{... | collective-permute-start | bytes 589832 | tf_op jit(solution)/shard_map/ppermute | solution.py:220
  23.6 21.0 %collective-permute-start.16 = (bf16[48,2048]{1,0:T(8,128)(2,1)S(1)}, bf16[48,2048]{1,0:T(8,128)(2,1)S(1)}, u32[]{:S(2)}, u32[]{:S(2)}) collective-permute-start(bf16[48,2048]{1,0:T(8,128)(2,1)S(1)} %get-tuple-element.37), channel_id=1, source_target_pairs={{0,20},{4,16},{8,28},{12,24},{16,4},{20,0},{24,12},{28,8},{1,21},{... | collective-permute-start | bytes 589832 | tf_op jit(solution)/shard_map/ppermute | solution.py:220
  25.7 21.3 %collective-permute-start.10 = (bf16[192,512]{1,0:T(8,128)(2,1)S(1)}, bf16[192,512]{1,0:T(8,128)(2,1)S(1)}, u32[]{:S(2)}, u32[]{:S(2)}) collective-permute-start(bf16[192,512]{1,0:T(8,128)(2,1)S(1)} %shard_map.113.refs_0_), channel_id=1, source_target_pairs={{0,2},{1,3},{2,0},{3,1},{4,6},{5,7},{6,4},{7,5},{8,10},{9,11},{10,... | collective-permute-start | bytes 589832 | tf_op jit(solution)/shard_map/ppermute | solution.py:220
  34.6 14.0 %collective-permute-start.11 = (bf16[192,512]{1,0:T(8,128)(2,1)S(1)}, bf16[192,512]{1,0:T(8,128)(2,1)S(1)}, u32[]{:S(2)}, u32[]{:S(2)}) collective-permute-start(bf16[192,512]{1,0:T(8,128)(2,1)S(1)} %shard_map.113.refs_0_), channel_id=1, source_target_pairs={{0,3},{1,2},{2,1},{3,0},{4,7},{5,6},{6,5},{7,4},{8,11},{9,10},{10,... | collective-permute-start | bytes 589832 | tf_op jit(solution)/shard_map/ppermute | solution.py:220
  38.0 12.2 %collective-permute-start.9 = (bf16[192,512]{1,0:T(8,128)(2,1)S(1)}, bf16[192,512]{1,0:T(8,128)(2,1)S(1)}, u32[]{:S(2)}, u32[]{:S(2)}) collective-permute-start(bf16[192,512]{1,0:T(8,128)(2,1)S(1)} %shard_map.113.refs_0_), channel_id=1, source_target_pairs={{0,1},{1,0},{2,3},{3,2},{4,5},{5,4},{6,7},{7,6},{8,9},{9,8},{10,11... | collective-permute-start | bytes 589832 | tf_op jit(solution)/shard_map/ppermute | solution.py:220
  42.2 10.0 %collective-permute-start.1 = (bf16[128,512]{1,0:T(8,128)(2,1)S(1)}, bf16[128,512]{1,0:T(8,128)(2,1)S(1)}, u32[]{:S(2)}, u32[]{:S(2)}) collective-permute-start(bf16[128,512]{1,0:T(8,128)(2,1)S(1)} %shard_map.109.refs_0_), channel_id=1, source_target_pairs={{0,2},{1,3},{2,0},{3,1},{4,6},{5,7},{6,4},{7,5},{8,10},{9,11},{10,... | collective-permute-start | bytes 393224 | tf_op jit(solution)/shard_map/ppermute | solution.py:220
  44.6 7.6 %collective-permute-start.2 = (bf16[128,512]{1,0:T(8,128)(2,1)S(1)}, bf16[128,512]{1,0:T(8,128)(2,1)S(1)}, u32[]{:S(2)}, u32[]{:S(2)}) collective-permute-start(bf16[128,512]{1,0:T(8,128)(2,1)S(1)} %shard_map.109.refs_0_), channel_id=1, source_target_pairs={{0,3},{1,2},{2,1},{3,0},{4,7},{5,6},{6,5},{7,4},{8,11},{9,10},{10,... | collective-permute-start | bytes 393224 | tf_op jit(solution)/shard_map/ppermute | solution.py:220
  47.0 6.3 %collective-permute-start.24 = (bf16[96,512]{1,0:T(8,128)(2,1)S(1)}, bf16[96,512]{1,0:T(8,128)(2,1)S(1)}, u32[]{:S(2)}, u32[]{:S(2)}) collective-permute-start(bf16[96,512]{1,0:T(8,128)(2,1)S(1)} %shard_map.119.refs_0_), channel_id=1, source_target_pairs={{0,1},{1,0},{2,3},{3,2},{4,5},{5,4},{6,7},{7,6},{8,9},{9,8},{10,11... | collective-permute-start | bytes 294920 | tf_op jit(solution)/shard_map/ppermute | solution.py:220
  52.2 13.7 %collective-permute-start.12 = (bf16[4,48,512]{2,1,0:T(8,128)(2,1)S(1)}, bf16[4,48,512]{2,1,0:T(8,128)(2,1)S(1)}, u32[]{:S(2)}, u32[]{:S(2)}) collective-permute-start(bf16[4,48,512]{2,1,0:T(8,128)(2,1)S(1)} %get-tuple-element.32), channel_id=1, source_target_pairs={{0,4},{4,0},{8,12},{12,8},{16,20},{20,16},{24,28},{28,24},{1,5},{5... | collective-permute-start | bytes 589832 | tf_op jit(solution)/shard_map/ppermute | solution.py:220
  52.3 15.0 %collective-permute-start.13 = (bf16[4,48,512]{2,1,0:T(8,128)(2,1)S(1)}, bf16[4,48,512]{2,1,0:T(8,128)(2,1)S(1)}, u32[]{:S(2)}, u32[]{:S(2)}) collective-permute-start(bf16[4,48,512]{2,1,0:T(8,128)(2,1)S(1)} %get-tuple-element.33), channel_id=1, source_target_pairs={{0,8},{4,12},{8,0},{12,4},{16,24},{20,28},{24,16},{28,20},{1,9},{5... | collective-permute-start | bytes 589832 | tf_op jit(solution)/shard_map/ppermute | solution.py:220
  53.4 6.4 %collective-permute-start.19 = (bf16[96,512]{1,0:T(8,128)(2,1)S(1)}, bf16[96,512]{1,0:T(8,128)(2,1)S(1)}, u32[]{:S(2)}, u32[]{:S(2)}) collective-permute-start(bf16[96,512]{1,0:T(8,128)(2,1)S(1)} %shard_map.116.refs_0_), channel_id=1, source_target_pairs={{0,3},{1,2},{2,1},{3,0},{4,7},{5,6},{6,5},{7,4},{8,11},{9,10},{10,... | collective-permute-start | bytes 294920 | tf_op jit(solution)/shard_map/ppermute | solution.py:220
  54.5 8.8 %collective-permute-start.25 = (bf16[96,512]{1,0:T(8,128)(2,1)S(1)}, bf16[96,512]{1,0:T(8,128)(2,1)S(1)}, u32[]{:S(2)}, u32[]{:S(2)}) collective-permute-start(bf16[96,512]{1,0:T(8,128)(2,1)S(1)} %shard_map.119.refs_0_), channel_id=1, source_target_pairs={{0,2},{1,3},{2,0},{3,1},{4,6},{5,7},{6,4},{7,5},{8,10},{9,11},{10,... | collective-permute-start | bytes 294920 | tf_op jit(solution)/shard_map/ppermute | solution.py:220
  55.7 9.5 %collective-permute-start.26 = (bf16[96,512]{1,0:T(8,128)(2,1)S(1)}, bf16[96,512]{1,0:T(8,128)(2,1)S(1)}, u32[]{:S(2)}, u32[]{:S(2)}) collective-permute-start(bf16[96,512]{1,0:T(8,128)(2,1)S(1)} %shard_map.119.refs_0_), channel_id=1, source_target_pairs={{0,3},{1,2},{2,1},{3,0},{4,7},{5,6},{6,5},{7,4},{8,11},{9,10},{10,... | collective-permute-start | bytes 294920 | tf_op jit(solution)/shard_map/ppermute | solution.py:220
  59.8 10.1 %collective-permute-start.14 = (bf16[4,48,512]{2,1,0:T(8,128)(2,1)S(1)}, bf16[4,48,512]{2,1,0:T(8,128)(2,1)S(1)}, u32[]{:S(2)}, u32[]{:S(2)}) collective-permute-start(bf16[4,48,512]{2,1,0:T(8,128)(2,1)S(1)} %get-tuple-element.34), channel_id=1, source_target_pairs={{0,12},{4,8},{8,4},{12,0},{16,28},{20,24},{24,20},{28,16},{1,13},{... | collective-permute-start | bytes 589832 | tf_op jit(solution)/shard_map/ppermute | solution.py:220
  63.3 23.4 %collective-permute-start.20 = (bf16[4,48,512]{2,1,0:T(8,128)(2,1)S(1)}, bf16[4,48,512]{2,1,0:T(8,128)(2,1)S(1)}, u32[]{:S(2)}, u32[]{:S(2)}) collective-permute-start(bf16[4,48,512]{2,1,0:T(8,128)(2,1)S(1)} %get-tuple-element.38), channel_id=1, source_target_pairs={{0,16},{4,20},{8,24},{12,28},{16,0},{20,4},{24,8},{28,12},{1,17},{... | collective-permute-start | bytes 589832 | tf_op jit(solution)/shard_map/ppermute | solution.py:220
  65.2 25.7 %collective-permute-start.21 = (bf16[4,48,512]{2,1,0:T(8,128)(2,1)S(1)}, bf16[4,48,512]{2,1,0:T(8,128)(2,1)S(1)}, u32[]{:S(2)}, u32[]{:S(2)}) collective-permute-start(bf16[4,48,512]{2,1,0:T(8,128)(2,1)S(1)} %get-tuple-element.39), channel_id=1, source_target_pairs={{0,20},{4,16},{8,28},{12,24},{16,4},{20,0},{24,12},{28,8},{1,21},{... | collective-permute-start | bytes 589832 | tf_op jit(solution)/shard_map/ppermute | solution.py:220
  65.9 30.6 %collective-permute-start.27 = (bf16[4,48,512]{2,1,0:T(8,128)(2,1)S(1)}, bf16[4,48,512]{2,1,0:T(8,128)(2,1)S(1)}, u32[]{:S(2)}, u32[]{:S(2)}) collective-permute-start(bf16[4,48,512]{2,1,0:T(8,128)(2,1)S(1)} %get-tuple-element.43), channel_id=1, source_target_pairs={{0,24},{4,28},{8,16},{12,20},{16,8},{20,12},{24,0},{28,4},{1,25},{... | collective-permute-start | bytes 589832 | tf_op jit(solution)/shard_map/ppermute | solution.py:220
  67.2 32.4 %collective-permute-start.28 = (bf16[4,48,512]{2,1,0:T(8,128)(2,1)S(1)}, bf16[4,48,512]{2,1,0:T(8,128)(2,1)S(1)}, u32[]{:S(2)}, u32[]{:S(2)}) collective-permute-start(bf16[4,48,512]{2,1,0:T(8,128)(2,1)S(1)} %get-tuple-element.44), channel_id=1, source_target_pairs={{0,28},{4,24},{8,20},{12,16},{16,12},{20,8},{24,4},{28,0},{1,29},{... | collective-permute-start | bytes 589832 | tf_op jit(solution)/shard_map/ppermute | solution.py:220
  (13 other events, 80.4 us)

commit v6 on v5

--- a/solution.py
+++ b/solution.py
@@ -263,7 +263,7 @@
     )
     half, quarter = experts // 2, experts // 4
     arrived = [pieces[0]] + [swap(pieces[k], "ep", k) for k in range(1, experts)]
-    groups = {"N": (0, half), "A": (half, quarter), "B": (half + quarter, quarter)}
+    groups = {"N": (0, half), "A": (half + quarter, quarter), "B": (half, quarter)}
 
     packed = jnp.concatenate([routes.T.astype(F32), route_weights.T], axis=0)
     packed = spread(packed)
@@ -320,14 +320,14 @@
     (total,) = call(
         functools.partial(base_kernel, blocks),
         [sums],
-        shared + [shared_down, tables[0]] + returned["N"],
-        2 * blocks * count * local * (inner + 3 * half * capacity),
+        shared + [shared_down, tables[1]] + returned["A"],
+        2 * blocks * count * local * (inner + 3 * quarter * capacity),
     )
     (total,) = call(
         functools.partial(more_kernel, blocks),
         [sums],
-        [total, tables[1]] + returned["A"],
-        2 * blocks * count * local * 3 * quarter * capacity,
+        [total, tables[0]] + returned["N"],
+        2 * blocks * count * local * 3 * half * capacity,
     )
     moe, squares = call(
         functools.partial(finish_kernel, blocks),

time: 109 us -> 103 us (0.945)
  the two profiles are of different devices: /device:TPU:10 before, /device:TPU:0 now
where the time goes in v6:
time: 103 us
  starting transfers between devices  52.6 us (51%)
  waiting for transfers between devices  32.7 us (32%)
  Pallas kernels  15.8 us (15%)
  local copies, waits for them, and re-layouts  1.76 us (2%)
    ppermute x32, starting transfers between devices, swap(): return lax.ppermute(array, axis, [(s, s ^ k) for s in range(size)])  52.6 us
    ppermute x32, waiting for transfers between devices, swap(): return lax.ppermute(array, axis, [(s, s ^ k) for s in range(size)])  32.7 us
    pallas_call x14, Pallas kernels, call(): pl.pallas_call(kernel, out_shape=outs, in_specs=specs, out_specs=[HBM if...  15.8 us
  transfers between devices with their start and end apart: 32, of which 12 were waited for; matrix products, arithmetic and copies ran while one was open for 0% of the time, Pallas kernels for 12%

profile of v6, /device:TPU:0, one launch (start us, length us, event | category | flops | bytes accessed | tf_op | source)
XLA Modules:
  0.0 103.0 jit_solution(7810865929201678434)
XLA Ops:
  0.0 1.6 %shard_map.111 = (bf16[48,2048]{1,0:T(8,128)(2,1)S(1)}, bf16[48,2048]{1,0:T(8,128)(2,1)S(1)}, bf16[48,2048]{1,0:T(8,128)(2,1)S(1)}, bf16[48,2048]{1,0:T(8,128)(2...) custom-call(s32[1]{0:T(128)} %bitcast.2.me, ...), custom_call_target="tpu_custom_call" | custom-call | flops 201326592 | bytes 2098180 | tf_op jit(solution)/shard_map/pallas_call | solution.py:29
  2.2 4.7 %collective-permute-start.6 = (bf16[48,2048]{1,0:T(8,128)(2,1)S(1)}, bf16[48,2048]{1,0:T(8,128)(2,1)S(1)}, u32[]{:S(2)}, u32[]{:S(2)}) collective-permute-start(bf16[48,2048]{1,0:T(8,128)(2,1)S(1)} %get-tuple-element.27), channel_id=1, source_target_pairs={{0,24},{4,28},{8,16},{12,20},{16,8},{20,12},{24,0},{28,4},{1,25},{... | collective-permute-start | bytes 589832 | tf_op jit(solution)/shard_map/ppermute | solution.py:220
  8.6 3.0 %shard_map.109.refs_0_ = bf16[128,512]{1,0:T(8,128)(2,1)S(1)} custom-call(bf16[128,2048]{1,0:T(8,128)(2,1)S(1)} %copy-done.1, f32[1,2048]{1,0:T(1,128)S(1)} %bitcast.13, bf16[2048,512]{1,0:T(8,128)(2,1)} %gate.1, bf16[2048,512]{1,0:T(8,128)(2,1)} %upward.1), custom_call_target="tpu_custom_call" | custom-call | flops 536870912 | bytes 4857856 | tf_op jit(solution)/shard_map/pallas_call | solution.py:29
  13.8 3.5 %collective-permute-done.3.refs_1_ = f32[4,128]{1,0:T(4,128)S(1)} collective-permute-done((f32[4,128]{1,0:T(4,128)S(1)}, f32[4,128]{1,0:T(4,128)S(1)}, u32[]{:S(2)}, u32[]{:S(2)}) %collective-permute-start.3) | collective-permute-done | bytes 2080 | tf_op jit(solution)/shard_map/ppermute | solution.py:220
  17.3 1.7 %collective-permute-start.4 = (f32[4,128]{1,0:T(4,128)S(1)}, f32[4,128]{1,0:T(4,128)S(1)}, u32[]{:S(2)}, u32[]{:S(2)}) collective-permute-start(f32[4,128]{1,0:T(4,128)S(1)} %pad_maximum_fusion.refs_0_), channel_id=1, source_target_pairs={{0,2},{1,3},{2,0},{3,1},{4,6},{5,7},{6,4},{7,5},{8,10},{9,11},{10,... | collective-permute-start | bytes 6152 | tf_op jit(solution)/shard_map/ppermute | solution.py:220
  19.0 1.9 %collective-permute-done.4.refs_2_ = f32[4,128]{1,0:T(4,128)S(1)} collective-permute-done((f32[4,128]{1,0:T(4,128)S(1)}, f32[4,128]{1,0:T(4,128)S(1)}, u32[]{:S(2)}, u32[]{:S(2)}) %collective-permute-start.4) | collective-permute-done | bytes 2080 | tf_op jit(solution)/shard_map/ppermute | solution.py:220
  20.9 2.6 %collective-permute-start.5 = (f32[4,128]{1,0:T(4,128)S(1)}, f32[4,128]{1,0:T(4,128)S(1)}, u32[]{:S(2)}, u32[]{:S(2)}) collective-permute-start(f32[4,128]{1,0:T(4,128)S(1)} %pad_maximum_fusion.refs_0_), channel_id=1, source_target_pairs={{0,3},{1,2},{2,1},{3,0},{4,7},{5,6},{6,5},{7,4},{8,11},{9,10},{10,... | collective-permute-start | bytes 6152 | tf_op jit(solution)/shard_map/ppermute | solution.py:220
  23.5 1.9 %collective-permute-done.5.refs_3_ = f32[4,128]{1,0:T(4,128)S(1)} collective-permute-done((f32[4,128]{1,0:T(4,128)S(1)}, f32[4,128]{1,0:T(4,128)S(1)}, u32[]{:S(2)}, u32[]{:S(2)}) %collective-permute-start.5) | collective-permute-done | bytes 2080 | tf_op jit(solution)/shard_map/ppermute | solution.py:220
  25.4 1.7 %collective-permute-start.1 = (bf16[128,512]{1,0:T(8,128)(2,1)S(1)}, bf16[128,512]{1,0:T(8,128)(2,1)S(1)}, u32[]{:S(2)}, u32[]{:S(2)}) collective-permute-start(bf16[128,512]{1,0:T(8,128)(2,1)S(1)} %shard_map.109.refs_0_), channel_id=1, source_target_pairs={{0,2},{1,3},{2,0},{3,1},{4,6},{5,7},{6,4},{7,5},{8,10},{9,11},{10,... | collective-permute-start | bytes 393224 | tf_op jit(solution)/shard_map/ppermute | solution.py:220
  28.6 2.2 %shard_map.112.refs_3_.refs_5_ = bf16[2048,1024]{1,0:T(8,128)(2,1)S(1)} custom-call(bf16[2048,512]{1,0:T(8,128)(2,1)} %bitcast.18, bf16[2048,512]{1,0:T(8,128)(2,1)} %bitcast.19, bf16[48,2048]{1,0:T(8,128)(2,1)S(1)} %get-tuple-element.29.held.refs_0_), custom_call_target="tpu_custom_call" | custom-call | flops 262144 | bytes 8585216 | tf_op jit(solution)/shard_map/pallas_call | solution.py:29
  31.7 4.4 %collective-permute-start.10 = (bf16[96,512]{1,0:T(8,128)(2,1)S(1)}, bf16[96,512]{1,0:T(8,128)(2,1)S(1)}, u32[]{:S(2)}, u32[]{:S(2)}) collective-permute-start(bf16[96,512]{1,0:T(8,128)(2,1)S(1)} %shard_map.113.refs_0_), channel_id=1, source_target_pairs={{0,3},{1,2},{2,1},{3,0},{4,7},{5,6},{6,5},{7,4},{8,11},{9,10},{10,... | collective-permute-start | bytes 294920 | tf_op jit(solution)/shard_map/ppermute | solution.py:220
  36.7 4.8 %collective-permute-start.22 = (bf16[48,2048]{1,0:T(8,128)(2,1)S(1)}, bf16[48,2048]{1,0:T(8,128)(2,1)S(1)}, u32[]{:S(2)}, u32[]{:S(2)}) collective-permute-start(bf16[48,2048]{1,0:T(8,128)(2,1)S(1)} %get-tuple-element.41), channel_id=1, source_target_pairs={{0,16},{4,20},{8,24},{12,28},{16,0},{20,4},{24,8},{28,12},{1,17},{... | collective-permute-start | bytes 589832 | tf_op jit(solution)/shard_map/ppermute | solution.py:220
  46.6 7.8 %collective-permute-done.22.refs_0_ = bf16[48,2048]{1,0:T(8,128)(2,1)S(1)} collective-permute-done((bf16[48,2048]{1,0:T(8,128)(2,1)S(1)}, bf16[48,2048]{1,0:T(8,128)(2,1)S(1)}, u32[]{:S(2)}, u32[]{:S(2)}) %collective-permute-start.22) | collective-permute-done | bytes 196640 | tf_op jit(solution)/shard_map/ppermute | solution.py:220
  54.5 2.3 %collective-permute-start.11 = (bf16[4,48,512]{2,1,0:T(8,128)(2,1)S(1)}, bf16[4,48,512]{2,1,0:T(8,128)(2,1)S(1)}, u32[]{:S(2)}, u32[]{:S(2)}) collective-permute-start(bf16[4,48,512]{2,1,0:T(8,128)(2,1)S(1)} %get-tuple-element.30), channel_id=1, source_target_pairs={{0,24},{4,28},{8,16},{12,20},{16,8},{20,12},{24,0},{28,4},{1,25},{... | collective-permute-start | bytes 589832 | tf_op jit(solution)/shard_map/ppermute | solution.py:220
  56.8 3.8 %collective-permute-start.12 = (bf16[4,48,512]{2,1,0:T(8,128)(2,1)S(1)}, bf16[4,48,512]{2,1,0:T(8,128)(2,1)S(1)}, u32[]{:S(2)}, u32[]{:S(2)}) collective-permute-start(bf16[4,48,512]{2,1,0:T(8,128)(2,1)S(1)} %get-tuple-element.31), channel_id=1, source_target_pairs={{0,28},{4,24},{8,20},{12,16},{16,12},{20,8},{24,4},{28,0},{1,29},{... | collective-permute-start | bytes 589832 | tf_op jit(solution)/shard_map/ppermute | solution.py:220
  66.3 4.1 %collective-permute-start.19 = (bf16[4,48,512]{2,1,0:T(8,128)(2,1)S(1)}, bf16[4,48,512]{2,1,0:T(8,128)(2,1)S(1)}, u32[]{:S(2)}, u32[]{:S(2)}) collective-permute-start(bf16[4,48,512]{2,1,0:T(8,128)(2,1)S(1)} %get-tuple-element.37), channel_id=1, source_target_pairs={{0,4},{4,0},{8,12},{12,8},{16,20},{20,16},{24,28},{28,24},{1,5},{5... | collective-permute-start | bytes 589832 | tf_op jit(solution)/shard_map/ppermute | solution.py:220
  73.1 3.3 %collective-permute-start.27 = (bf16[4,48,512]{2,1,0:T(8,128)(2,1)S(1)}, bf16[4,48,512]{2,1,0:T(8,128)(2,1)S(1)}, u32[]{:S(2)}, u32[]{:S(2)}) collective-permute-start(bf16[4,48,512]{2,1,0:T(8,128)(2,1)S(1)} %get-tuple-element.43), channel_id=1, source_target_pairs={{0,16},{4,20},{8,24},{12,28},{16,0},{20,4},{24,8},{28,12},{1,17},{... | collective-permute-start | bytes 589832 | tf_op jit(solution)/shard_map/ppermute | solution.py:220
  76.4 2.2 %collective-permute-start.28 = (bf16[4,48,512]{2,1,0:T(8,128)(2,1)S(1)}, bf16[4,48,512]{2,1,0:T(8,128)(2,1)S(1)}, u32[]{:S(2)}, u32[]{:S(2)}) collective-permute-start(bf16[4,48,512]{2,1,0:T(8,128)(2,1)S(1)} %get-tuple-element.44), channel_id=1, source_target_pairs={{0,20},{4,16},{8,28},{12,24},{16,4},{20,0},{24,12},{28,8},{1,21},{... | collective-permute-start | bytes 589832 | tf_op jit(solution)/shard_map/ppermute | solution.py:220
  78.6 1.7 %shard_map.110 = (bf16[4,128,576]{2,1,0:T(8,128)(2,1)S(1)}, bf16[4,128,288]{2,1,0:T(8,128)(2,1)S(1)}, bf16[4,128,288]{2,1,0:T(8,128)(2,1)S(1)}) custom-call(s32[1]{0:T(128)} %bitcast.2.me, f32[4,128]{1,0:T(4,128)S(1)} %pad_maximum_fusion.refs_0_, f32[4,128]{1,0:T(4,128)S(1)} %collective-permute-done.3.refs_1_, f32[4,128]{1,0:T(4,128)S(1)} %collective-permute-done.4.refs_2_, ...), custom_call_target="tpu_custom_call" | custom-call | flops 8388608 | bytes 1187844 | tf_op jit(solution)/shard_map/pallas_call | solution.py:29
  81.1 1.9 %collective-permute-done.20.refs_2_ = bf16[4,48,512]{2,1,0:T(8,128)(2,1)S(1)} collective-permute-done((bf16[4,48,512]{2,1,0:T(8,128)(2,1)S(1)}, bf16[4,48,512]{2,1,0:T(8,128)(2,1)S(1)}, u32[]{:S(2)}, u32[]{:S(2)}) %collective-permute-start.20) | collective-permute-done | bytes 196640 | tf_op jit(solution)/shard_map/ppermute | solution.py:220
  83.0 5.1 %collective-permute-done.21.refs_3_ = bf16[4,48,512]{2,1,0:T(8,128)(2,1)S(1)} collective-permute-done((bf16[4,48,512]{2,1,0:T(8,128)(2,1)S(1)}, bf16[4,48,512]{2,1,0:T(8,128)(2,1)S(1)}, u32[]{:S(2)}, u32[]{:S(2)}) %collective-permute-start.21) | collective-permute-done | bytes 196640 | tf_op jit(solution)/shard_map/ppermute | solution.py:220
  88.7 5.7 %collective-permute-done.28.refs_1_ = bf16[4,48,512]{2,1,0:T(8,128)(2,1)S(1)} collective-permute-done((bf16[4,48,512]{2,1,0:T(8,128)(2,1)S(1)}, bf16[4,48,512]{2,1,0:T(8,128)(2,1)S(1)}, u32[]{:S(2)}, u32[]{:S(2)}) %collective-permute-start.28) | collective-permute-done | bytes 196640 | tf_op jit(solution)/shard_map/ppermute | solution.py:220
  95.4 2.0 %collective-permute-start.30 = (f32[4,128]{1,0:T(4,128)S(1)}, f32[4,128]{1,0:T(4,128)S(1)}, u32[]{:S(2)}, u32[]{:S(2)}) collective-permute-start(f32[4,128]{1,0:T(4,128)S(1)} %get-tuple-element.46.refs_0_), channel_id=1, source_target_pairs={{0,2},{1,3},{2,0},{3,1},{4,6},{5,7},{6,4},{7,5},{8,10},{9,11},{10,... | collective-permute-start | bytes 6152 | tf_op jit(solution)/shard_map/ppermute | solution.py:220
  99.0 2.9 %collective-permute-done.31.refs_3_ = f32[4,128]{1,0:T(4,128)S(1)} collective-permute-done((f32[4,128]{1,0:T(4,128)S(1)}, f32[4,128]{1,0:T(4,128)S(1)}, u32[]{:S(2)}, u32[]{:S(2)}) %collective-permute-start.31) | collective-permute-done | bytes 2080 | tf_op jit(solution)/shard_map/ppermute | solution.py:220
  (70 shorter events, 25.8 us)
Async XLA Ops:
  1.6 35.1 %collective-permute-start.13 = (bf16[48,2048]{1,0:T(8,128)(2,1)S(1)}, bf16[48,2048]{1,0:T(8,128)(2,1)S(1)}, u32[]{:S(2)}, u32[]{:S(2)}) collective-permute-start(bf16[48,2048]{1,0:T(8,128)(2,1)S(1)} %get-tuple-element.33), channel_id=1, source_target_pairs={{0,4},{4,0},{8,12},{12,8},{16,20},{20,16},{24,28},{28,24},{1,5},{5... | collective-permute-start | bytes 589832 | tf_op jit(solution)/shard_map/ppermute | solution.py:220
  2.2 23.2 %collective-permute-start.6 = (bf16[48,2048]{1,0:T(8,128)(2,1)S(1)}, bf16[48,2048]{1,0:T(8,128)(2,1)S(1)}, u32[]{:S(2)}, u32[]{:S(2)}) collective-permute-start(bf16[48,2048]{1,0:T(8,128)(2,1)S(1)} %get-tuple-element.27), channel_id=1, source_target_pairs={{0,24},{4,28},{8,16},{12,20},{16,8},{20,12},{24,0},{28,4},{1,25},{... | collective-permute-start | bytes 589832 | tf_op jit(solution)/shard_map/ppermute | solution.py:220
  6.9 20.3 %collective-permute-start.7 = (bf16[48,2048]{1,0:T(8,128)(2,1)S(1)}, bf16[48,2048]{1,0:T(8,128)(2,1)S(1)}, u32[]{:S(2)}, u32[]{:S(2)}) collective-permute-start(bf16[48,2048]{1,0:T(8,128)(2,1)S(1)} %get-tuple-element.28), channel_id=1, source_target_pairs={{0,28},{4,24},{8,20},{12,16},{16,12},{20,8},{24,4},{28,0},{1,29},{... | collective-permute-start | bytes 589832 | tf_op jit(solution)/shard_map/ppermute | solution.py:220
  11.7 13.7 %collective-permute-start = (bf16[128,512]{1,0:T(8,128)(2,1)S(1)}, bf16[128,512]{1,0:T(8,128)(2,1)S(1)}, u32[]{:S(2)}, u32[]{:S(2)}) collective-permute-start(bf16[128,512]{1,0:T(8,128)(2,1)S(1)} %shard_map.109.refs_0_), channel_id=1, source_target_pairs={{0,1},{1,0},{2,3},{3,2},{4,5},{5,4},{6,7},{7,6},{8,9},{9,8},{10,11... | collective-permute-start | bytes 393224 | tf_op jit(solution)/shard_map/ppermute | solution.py:220
  25.4 11.4 %collective-permute-start.14 = (bf16[48,2048]{1,0:T(8,128)(2,1)S(1)}, bf16[48,2048]{1,0:T(8,128)(2,1)S(1)}, u32[]{:S(2)}, u32[]{:S(2)}) collective-permute-start(bf16[48,2048]{1,0:T(8,128)(2,1)S(1)} %get-tuple-element.34), channel_id=1, source_target_pairs={{0,8},{4,12},{8,0},{12,4},{16,24},{20,28},{24,16},{28,20},{1,9},{5... | collective-permute-start | bytes 589832 | tf_op jit(solution)/shard_map/ppermute | solution.py:220
  25.4 16.1 %collective-permute-start.15 = (bf16[48,2048]{1,0:T(8,128)(2,1)S(1)}, bf16[48,2048]{1,0:T(8,128)(2,1)S(1)}, u32[]{:S(2)}, u32[]{:S(2)}) collective-permute-start(bf16[48,2048]{1,0:T(8,128)(2,1)S(1)} %get-tuple-element.35), channel_id=1, source_target_pairs={{0,12},{4,8},{8,4},{12,0},{16,28},{20,24},{24,20},{28,16},{1,13},{... | collective-permute-start | bytes 589832 | tf_op jit(solution)/shard_map/ppermute | solution.py:220
  27.1 9.0 %collective-permute-start.2 = (bf16[128,512]{1,0:T(8,128)(2,1)S(1)}, bf16[128,512]{1,0:T(8,128)(2,1)S(1)}, u32[]{:S(2)}, u32[]{:S(2)}) collective-permute-start(bf16[128,512]{1,0:T(8,128)(2,1)S(1)} %shard_map.109.refs_0_), channel_id=1, source_target_pairs={{0,3},{1,2},{2,1},{3,0},{4,7},{5,6},{6,5},{7,4},{8,11},{9,10},{10,... | collective-permute-start | bytes 393224 | tf_op jit(solution)/shard_map/ppermute | solution.py:220
  31.7 10.9 %collective-permute-start.10 = (bf16[96,512]{1,0:T(8,128)(2,1)S(1)}, bf16[96,512]{1,0:T(8,128)(2,1)S(1)}, u32[]{:S(2)}, u32[]{:S(2)}) collective-permute-start(bf16[96,512]{1,0:T(8,128)(2,1)S(1)} %shard_map.113.refs_0_), channel_id=1, source_target_pairs={{0,3},{1,2},{2,1},{3,0},{4,7},{5,6},{6,5},{7,4},{8,11},{9,10},{10,... | collective-permute-start | bytes 294920 | tf_op jit(solution)/shard_map/ppermute | solution.py:220
  36.2 8.1 %collective-permute-start.8 = (bf16[96,512]{1,0:T(8,128)(2,1)S(1)}, bf16[96,512]{1,0:T(8,128)(2,1)S(1)}, u32[]{:S(2)}, u32[]{:S(2)}) collective-permute-start(bf16[96,512]{1,0:T(8,128)(2,1)S(1)} %shard_map.113.refs_0_), channel_id=1, source_target_pairs={{0,1},{1,0},{2,3},{3,2},{4,5},{5,4},{6,7},{7,6},{8,9},{9,8},{10,11... | collective-permute-start | bytes 294920 | tf_op jit(solution)/shard_map/ppermute | solution.py:220
  36.7 9.1 %collective-permute-start.9 = (bf16[96,512]{1,0:T(8,128)(2,1)S(1)}, bf16[96,512]{1,0:T(8,128)(2,1)S(1)}, u32[]{:S(2)}, u32[]{:S(2)}) collective-permute-start(bf16[96,512]{1,0:T(8,128)(2,1)S(1)} %shard_map.113.refs_0_), channel_id=1, source_target_pairs={{0,2},{1,3},{2,0},{3,1},{4,6},{5,7},{6,4},{7,5},{8,10},{9,11},{10,... | collective-permute-start | bytes 294920 | tf_op jit(solution)/shard_map/ppermute | solution.py:220
  36.7 17.7 %collective-permute-start.22 = (bf16[48,2048]{1,0:T(8,128)(2,1)S(1)}, bf16[48,2048]{1,0:T(8,128)(2,1)S(1)}, u32[]{:S(2)}, u32[]{:S(2)}) collective-permute-start(bf16[48,2048]{1,0:T(8,128)(2,1)S(1)} %get-tuple-element.41), channel_id=1, source_target_pairs={{0,16},{4,20},{8,24},{12,28},{16,0},{20,4},{24,8},{28,12},{1,17},{... | collective-permute-start | bytes 589832 | tf_op jit(solution)/shard_map/ppermute | solution.py:220
  41.5 15.3 %collective-permute-start.23 = (bf16[48,2048]{1,0:T(8,128)(2,1)S(1)}, bf16[48,2048]{1,0:T(8,128)(2,1)S(1)}, u32[]{:S(2)}, u32[]{:S(2)}) collective-permute-start(bf16[48,2048]{1,0:T(8,128)(2,1)S(1)} %get-tuple-element.42), channel_id=1, source_target_pairs={{0,20},{4,16},{8,28},{12,24},{16,4},{20,0},{24,12},{28,8},{1,21},{... | collective-permute-start | bytes 589832 | tf_op jit(solution)/shard_map/ppermute | solution.py:220
  42.7 18.9 %collective-permute-start.16 = (bf16[192,512]{1,0:T(8,128)(2,1)S(1)}, bf16[192,512]{1,0:T(8,128)(2,1)S(1)}, u32[]{:S(2)}, u32[]{:S(2)}) collective-permute-start(bf16[192,512]{1,0:T(8,128)(2,1)S(1)} %shard_map.116.refs_0_), channel_id=1, source_target_pairs={{0,1},{1,0},{2,3},{3,2},{4,5},{5,4},{6,7},{7,6},{8,9},{9,8},{10,11... | collective-permute-start | bytes 589832 | tf_op jit(solution)/shard_map/ppermute | solution.py:220
  44.3 18.9 %collective-permute-start.17 = (bf16[192,512]{1,0:T(8,128)(2,1)S(1)}, bf16[192,512]{1,0:T(8,128)(2,1)S(1)}, u32[]{:S(2)}, u32[]{:S(2)}) collective-permute-start(bf16[192,512]{1,0:T(8,128)(2,1)S(1)} %shard_map.116.refs_0_), channel_id=1, source_target_pairs={{0,2},{1,3},{2,0},{3,1},{4,6},{5,7},{6,4},{7,5},{8,10},{9,11},{10,... | collective-permute-start | bytes 589832 | tf_op jit(solution)/shard_map/ppermute | solution.py:220
  45.8 19.0 %collective-permute-start.18 = (bf16[192,512]{1,0:T(8,128)(2,1)S(1)}, bf16[192,512]{1,0:T(8,128)(2,1)S(1)}, u32[]{:S(2)}, u32[]{:S(2)}) collective-permute-start(bf16[192,512]{1,0:T(8,128)(2,1)S(1)} %shard_map.116.refs_0_), channel_id=1, source_target_pairs={{0,3},{1,2},{2,1},{3,0},{4,7},{5,6},{6,5},{7,4},{8,11},{9,10},{10,... | collective-permute-start | bytes 589832 | tf_op jit(solution)/shard_map/ppermute | solution.py:220
  54.5 18.6 %collective-permute-start.11 = (bf16[4,48,512]{2,1,0:T(8,128)(2,1)S(1)}, bf16[4,48,512]{2,1,0:T(8,128)(2,1)S(1)}, u32[]{:S(2)}, u32[]{:S(2)}) collective-permute-start(bf16[4,48,512]{2,1,0:T(8,128)(2,1)S(1)} %get-tuple-element.30), channel_id=1, source_target_pairs={{0,24},{4,28},{8,16},{12,20},{16,8},{20,12},{24,0},{28,4},{1,25},{... | collective-permute-start | bytes 589832 | tf_op jit(solution)/shard_map/ppermute | solution.py:220
  56.8 19.6 %collective-permute-start.12 = (bf16[4,48,512]{2,1,0:T(8,128)(2,1)S(1)}, bf16[4,48,512]{2,1,0:T(8,128)(2,1)S(1)}, u32[]{:S(2)}, u32[]{:S(2)}) collective-permute-start(bf16[4,48,512]{2,1,0:T(8,128)(2,1)S(1)} %get-tuple-element.31), channel_id=1, source_target_pairs={{0,28},{4,24},{8,20},{12,16},{16,12},{20,8},{24,4},{28,0},{1,29},{... | collective-permute-start | bytes 589832 | tf_op jit(solution)/shard_map/ppermute | solution.py:220
  63.1 7.3 %collective-permute-start.25 = (bf16[96,512]{1,0:T(8,128)(2,1)S(1)}, bf16[96,512]{1,0:T(8,128)(2,1)S(1)}, u32[]{:S(2)}, u32[]{:S(2)}) collective-permute-start(bf16[96,512]{1,0:T(8,128)(2,1)S(1)} %shard_map.119.refs_0_), channel_id=1, source_target_pairs={{0,2},{1,3},{2,0},{3,1},{4,6},{5,7},{6,4},{7,5},{8,10},{9,11},{10,... | collective-permute-start | bytes 294920 | tf_op jit(solution)/shard_map/ppermute | solution.py:220
  64.8 6.4 %collective-permute-start.26 = (bf16[96,512]{1,0:T(8,128)(2,1)S(1)}, bf16[96,512]{1,0:T(8,128)(2,1)S(1)}, u32[]{:S(2)}, u32[]{:S(2)}) collective-permute-start(bf16[96,512]{1,0:T(8,128)(2,1)S(1)} %shard_map.119.refs_0_), channel_id=1, source_target_pairs={{0,3},{1,2},{2,1},{3,0},{4,7},{5,6},{6,5},{7,4},{8,11},{9,10},{10,... | collective-permute-start | bytes 294920 | tf_op jit(solution)/shard_map/ppermute | solution.py:220
  66.3 14.8 %collective-permute-start.19 = (bf16[4,48,512]{2,1,0:T(8,128)(2,1)S(1)}, bf16[4,48,512]{2,1,0:T(8,128)(2,1)S(1)}, u32[]{:S(2)}, u32[]{:S(2)}) collective-permute-start(bf16[4,48,512]{2,1,0:T(8,128)(2,1)S(1)} %get-tuple-element.37), channel_id=1, source_target_pairs={{0,4},{4,0},{8,12},{12,8},{16,20},{20,16},{24,28},{28,24},{1,5},{5... | collective-permute-start | bytes 589832 | tf_op jit(solution)/shard_map/ppermute | solution.py:220
  70.4 12.6 %collective-permute-start.20 = (bf16[4,48,512]{2,1,0:T(8,128)(2,1)S(1)}, bf16[4,48,512]{2,1,0:T(8,128)(2,1)S(1)}, u32[]{:S(2)}, u32[]{:S(2)}) collective-permute-start(bf16[4,48,512]{2,1,0:T(8,128)(2,1)S(1)} %get-tuple-element.38), channel_id=1, source_target_pairs={{0,8},{4,12},{8,0},{12,4},{16,24},{20,28},{24,16},{28,20},{1,9},{5... | collective-permute-start | bytes 589832 | tf_op jit(solution)/shard_map/ppermute | solution.py:220
  71.2 16.9 %collective-permute-start.21 = (bf16[4,48,512]{2,1,0:T(8,128)(2,1)S(1)}, bf16[4,48,512]{2,1,0:T(8,128)(2,1)S(1)}, u32[]{:S(2)}, u32[]{:S(2)}) collective-permute-start(bf16[4,48,512]{2,1,0:T(8,128)(2,1)S(1)} %get-tuple-element.39), channel_id=1, source_target_pairs={{0,12},{4,8},{8,4},{12,0},{16,28},{20,24},{24,20},{28,16},{1,13},{... | collective-permute-start | bytes 589832 | tf_op jit(solution)/shard_map/ppermute | solution.py:220
  73.1 15.6 %collective-permute-start.27 = (bf16[4,48,512]{2,1,0:T(8,128)(2,1)S(1)}, bf16[4,48,512]{2,1,0:T(8,128)(2,1)S(1)}, u32[]{:S(2)}, u32[]{:S(2)}) collective-permute-start(bf16[4,48,512]{2,1,0:T(8,128)(2,1)S(1)} %get-tuple-element.43), channel_id=1, source_target_pairs={{0,16},{4,20},{8,24},{12,28},{16,0},{20,4},{24,8},{28,12},{1,17},{... | collective-permute-start | bytes 589832 | tf_op jit(solution)/shard_map/ppermute | solution.py:220
  76.4 18.0 %collective-permute-start.28 = (bf16[4,48,512]{2,1,0:T(8,128)(2,1)S(1)}, bf16[4,48,512]{2,1,0:T(8,128)(2,1)S(1)}, u32[]{:S(2)}, u32[]{:S(2)}) collective-permute-start(bf16[4,48,512]{2,1,0:T(8,128)(2,1)S(1)} %get-tuple-element.44), channel_id=1, source_target_pairs={{0,20},{4,16},{8,28},{12,24},{16,4},{20,0},{24,12},{28,8},{1,21},{... | collective-permute-start | bytes 589832 | tf_op jit(solution)/shard_map/ppermute | solution.py:220
  (15 other events, 83.1 us)

commit v7 on v6

--- a/solution.py
+++ b/solution.py
@@ -12,6 +12,7 @@
 SMEM = pl.BlockSpec(memory_space=pltpu.SMEM)
 HBM = pl.BlockSpec(memory_space=pltpu.HBM)
 F32 = jnp.float32
+CHUNKS = 1
 BF16 = jnp.bfloat16
 
 
@@ -60,32 +61,53 @@
     return (values * inverse * gain).astype(BF16)
 
 
-def prepare_kernel(experts, capacity, me, *refs):
-    pieces = refs[2 : 2 + experts]
-    tokens, routes, sems = refs[2 + experts :]
-    copies = fetch(refs[:2], (tokens, routes), sems)
-    copies[1].wait()
-    count = tokens.shape[0]
+def places_of(me, routes, capacity, experts):
+    count = routes.shape[1]
     index = lax.broadcasted_iota(jnp.int32, (experts, count), 0)
-    marks = [index == routes[j : j + 1, :] for j in range(routes.shape[0])]
+    rows = [routes[j : j + 1, :] for j in range(routes.shape[0])]
+    marks = [index == row for row in rows]
     marked = functools.reduce(jnp.logical_or, marks)
     earlier = lax.broadcasted_iota(jnp.int32, (count, count), 0) < lax.broadcasted_iota(
         jnp.int32, (count, count), 1
     )
     before = dot(marked.astype(BF16), earlier.astype(BF16))
     places = []
-    for j, mark in enumerate(marks):
+    for row, mark in zip(rows, marks):
         slot = jnp.sum(jnp.where(mark, before, 0.0), axis=0, keepdims=True)
-        places.append((routes[j : j + 1, :] ^ me[0]) * capacity + slot.astype(jnp.int32))
+        places.append((row ^ me) * capacity + slot.astype(jnp.int32))
+    return places
+
+
+def picks(places, first, units, capacity):
+    shape = (units * capacity, places[0].shape[1])
+    at = lax.broadcasted_iota(jnp.int32, shape, 0) + first * capacity
+    chosen = functools.reduce(jnp.logical_or, [at == place for place in places])
+    return chosen.astype(F32).astype(BF16)
+
+
+def prepare_kernel(experts, capacity, first, chunks, me, tokens, routes, held, kept, *refs):
+    pieces, sems = refs[:-1], refs[-1]
+    step = tokens.shape[1] // chunks
+    spans = [pl.ds(c * step, step) for c in range(chunks)]
+    sources = [routes] + [tokens.at[:, span] for span in spans]
+    copies = fetch(sources, [kept] + [held.at[:, span] for span in spans], sems)
     copies[0].wait()
-    rows = tokens[...]
-    half = experts // 2
-    for start in (half, 0):
-        at = lax.broadcasted_iota(jnp.int32, (half * capacity, count), 0) + start * capacity
-        chosen = functools.reduce(jnp.logical_or, [at == place for place in places])
-        moved = dot(chosen.astype(F32).astype(BF16), rows).astype(BF16)
-        for k in range(half):
-            pieces[start + k][...] = moved[k * capacity : (k + 1) * capacity]
+    chosen = picks(places_of(me[0], kept, capacity, experts), first, len(pieces), capacity)
+    for copy, span in zip(copies[1:], spans):
+        copy.wait()
+        moved = dot(chosen, held[:, span]).astype(BF16)
+        for u, piece in enumerate(pieces):
+            piece[:, span] = moved[u * capacity : (u + 1) * capacity]
+
+
+def remain_kernel(experts, capacity, groups, me, held, kept, *pieces):
+    places = places_of(me[0], kept, capacity, experts)
+    done = 0
+    for first, units in groups:
+        moved = dot(picks(places, first, units, capacity), held[...]).astype(BF16)
+        for u in range(units):
+            pieces[done + u][...] = moved[u * capacity : (u + 1) * capacity]
+        done += units
 
 
 def table_kernel(capacity, groups, me, *refs):
@@ -248,20 +270,30 @@
     column = lax.axis_index("tp").astype(jnp.int32).reshape(1)
     piece = jax.ShapeDtypeStruct((capacity, width), BF16)
     gain = norm_gain[None, :]
-    pieces = call(
-        functools.partial(prepare_kernel, experts, capacity),
-        [piece] * experts,
+    half, quarter = experts // 2, experts // 4
+    held, kept, *pieces = call(
+        functools.partial(prepare_kernel, experts, capacity, half + quarter, CHUNKS),
+        [
+            jax.ShapeDtypeStruct((count, width), BF16),
+            jax.ShapeDtypeStruct((top_count, count), jnp.int32),
+        ]
+        + [piece] * quarter,
         [row, tokens, routes.T],
-        2 * experts * capacity * count * width,
+        2 * quarter * capacity * count * width,
         scalars=1,
         far=(1, 2),
-        scratch=[
-            pltpu.VMEM((count, width), BF16),
-            pltpu.VMEM((top_count, count), jnp.int32),
-            pltpu.SemaphoreType.DMA((2,)),
-        ],
-    )
-    half, quarter = experts // 2, experts // 4
+        scratch=[pltpu.SemaphoreType.DMA((1 + CHUNKS,))],
+    )
+    rest = call(
+        functools.partial(
+            remain_kernel, experts, capacity, [(0, half), (half, quarter)]
+        ),
+        [piece] * (experts - quarter),
+        [row, held, kept],
+        2 * (experts - quarter) * capacity * count * width,
+        scalars=1,
+    )
+    pieces = [*rest, *pieces]
     arrived = [pieces[0]] + [swap(pieces[k], "ep", k) for k in range(1, experts)]
     groups = {"N": (0, half), "A": (half + quarter, quarter), "B": (half, quarter)}
 

time: 103 us -> 104 us (level)
    pallas_call x14 -> x15, Pallas kernels: 15.8 us -> 16 us  [call(): pl.pallas_call(kernel, out_shape=outs, in_specs=specs, out_specs=[HBM if...]
where the time goes in v7:
time: 104 us; the launch traced here: 103 us
  starting transfers between devices  52.6 us (51%)
  waiting for transfers between devices  32.8 us (32%)
  Pallas kernels  16 us (15%)
  local copies, waits for them, and re-layouts  1.76 us (2%)
    ppermute x32, starting transfers between devices, swap(): return lax.ppermute(array, axis, [(s, s ^ k) for s in range(size)])  52.6 us
    ppermute x32, waiting for transfers between devices, swap(): return lax.ppermute(array, axis, [(s, s ^ k) for s in range(size)])  32.8 us
    pallas_call x15, Pallas kernels, call(): pl.pallas_call(kernel, out_shape=outs, in_specs=specs, out_specs=[HBM if...  16 us
  transfers between devices with their start and end apart: 32, of which 12 were waited for; matrix products, arithmetic and copies ran while one was open for 0% of the time, Pallas kernels for 12%

profile of v7, /device:TPU:0, one launch (start us, length us, event | category | flops | bytes accessed | tf_op | source)
XLA Modules:
  0.0 103.4 jit_solution(7735548428858249630)
XLA Ops:
  2.5 4.7 %collective-permute-start.6 = (bf16[48,2048]{1,0:T(8,128)(2,1)S(1)}, bf16[48,2048]{1,0:T(8,128)(2,1)S(1)}, u32[]{:S(2)}, u32[]{:S(2)}) collective-permute-start(bf16[48,2048]{1,0:T(8,128)(2,1)S(1)} %get-tuple-element.29), channel_id=1, source_target_pairs={{0,24},{4,28},{8,16},{12,20},{16,8},{20,12},{24,0},{28,4},{1,25},{... | collective-permute-start | bytes 589832 | tf_op jit(solution)/shard_map/ppermute | solution.py:242
  8.9 3.0 %shard_map.109.refs_0_ = bf16[128,512]{1,0:T(8,128)(2,1)S(1)} custom-call(bf16[128,2048]{1,0:T(8,128)(2,1)S(1)} %copy-done, f32[1,2048]{1,0:T(1,128)S(1)} %bitcast.13, bf16[2048,512]{1,0:T(8,128)(2,1)} %gate.1, bf16[2048,512]{1,0:T(8,128)(2,1)} %upward.1), custom_call_target="tpu_custom_call" | custom-call | flops 536870912 | bytes 4857856 | tf_op jit(solution)/shard_map/pallas_call | solution.py:30
  14.1 3.5 %collective-permute-done.3.refs_1_ = f32[4,128]{1,0:T(4,128)S(1)} collective-permute-done((f32[4,128]{1,0:T(4,128)S(1)}, f32[4,128]{1,0:T(4,128)S(1)}, u32[]{:S(2)}, u32[]{:S(2)}) %collective-permute-start.3) | collective-permute-done | bytes 2080 | tf_op jit(solution)/shard_map/ppermute | solution.py:242
  17.6 1.7 %collective-permute-start.4 = (f32[4,128]{1,0:T(4,128)S(1)}, f32[4,128]{1,0:T(4,128)S(1)}, u32[]{:S(2)}, u32[]{:S(2)}) collective-permute-start(f32[4,128]{1,0:T(4,128)S(1)} %pad_maximum_fusion.refs_0_), channel_id=1, source_target_pairs={{0,2},{1,3},{2,0},{3,1},{4,6},{5,7},{6,4},{7,5},{8,10},{9,11},{10,... | collective-permute-start | bytes 6152 | tf_op jit(solution)/shard_map/ppermute | solution.py:242
  19.3 1.9 %collective-permute-done.4.refs_2_ = f32[4,128]{1,0:T(4,128)S(1)} collective-permute-done((f32[4,128]{1,0:T(4,128)S(1)}, f32[4,128]{1,0:T(4,128)S(1)}, u32[]{:S(2)}, u32[]{:S(2)}) %collective-permute-start.4) | collective-permute-done | bytes 2080 | tf_op jit(solution)/shard_map/ppermute | solution.py:242
  21.2 2.6 %collective-permute-start.5 = (f32[4,128]{1,0:T(4,128)S(1)}, f32[4,128]{1,0:T(4,128)S(1)}, u32[]{:S(2)}, u32[]{:S(2)}) collective-permute-start(f32[4,128]{1,0:T(4,128)S(1)} %pad_maximum_fusion.refs_0_), channel_id=1, source_target_pairs={{0,3},{1,2},{2,1},{3,0},{4,7},{5,6},{6,5},{7,4},{8,11},{9,10},{10,... | collective-permute-start | bytes 6152 | tf_op jit(solution)/shard_map/ppermute | solution.py:242
  23.8 1.9 %collective-permute-done.5.refs_3_ = f32[4,128]{1,0:T(4,128)S(1)} collective-permute-done((f32[4,128]{1,0:T(4,128)S(1)}, f32[4,128]{1,0:T(4,128)S(1)}, u32[]{:S(2)}, u32[]{:S(2)}) %collective-permute-start.5) | collective-permute-done | bytes 2080 | tf_op jit(solution)/shard_map/ppermute | solution.py:242
  25.7 1.7 %collective-permute-start.1 = (bf16[128,512]{1,0:T(8,128)(2,1)S(1)}, bf16[128,512]{1,0:T(8,128)(2,1)S(1)}, u32[]{:S(2)}, u32[]{:S(2)}) collective-permute-start(bf16[128,512]{1,0:T(8,128)(2,1)S(1)} %shard_map.109.refs_0_), channel_id=1, source_target_pairs={{0,2},{1,3},{2,0},{3,1},{4,6},{5,7},{6,4},{7,5},{8,10},{9,11},{10,... | collective-permute-start | bytes 393224 | tf_op jit(solution)/shard_map/ppermute | solution.py:242
  28.9 2.2 %shard_map.113.refs_3_.refs_5_ = bf16[2048,1024]{1,0:T(8,128)(2,1)S(1)} custom-call(bf16[2048,512]{1,0:T(8,128)(2,1)} %bitcast.18, bf16[2048,512]{1,0:T(8,128)(2,1)} %bitcast.19, bf16[48,2048]{1,0:T(8,128)(2,1)S(1)} %get-tuple-element.33.held.refs_0_), custom_call_target="tpu_custom_call" | custom-call | flops 262144 | bytes 8585216 | tf_op jit(solution)/shard_map/pallas_call | solution.py:30
  32.0 4.4 %collective-permute-start.10 = (bf16[96,512]{1,0:T(8,128)(2,1)S(1)}, bf16[96,512]{1,0:T(8,128)(2,1)S(1)}, u32[]{:S(2)}, u32[]{:S(2)}) collective-permute-start(bf16[96,512]{1,0:T(8,128)(2,1)S(1)} %shard_map.114.refs_0_), channel_id=1, source_target_pairs={{0,3},{1,2},{2,1},{3,0},{4,7},{5,6},{6,5},{7,4},{8,11},{9,10},{10,... | collective-permute-start | bytes 294920 | tf_op jit(solution)/shard_map/ppermute | solution.py:242
  37.0 4.8 %collective-permute-start.22 = (bf16[48,2048]{1,0:T(8,128)(2,1)S(1)}, bf16[48,2048]{1,0:T(8,128)(2,1)S(1)}, u32[]{:S(2)}, u32[]{:S(2)}) collective-permute-start(bf16[48,2048]{1,0:T(8,128)(2,1)S(1)} %get-tuple-element.45), channel_id=1, source_target_pairs={{0,16},{4,20},{8,24},{12,28},{16,0},{20,4},{24,8},{28,12},{1,17},{... | collective-permute-start | bytes 589832 | tf_op jit(solution)/shard_map/ppermute | solution.py:242
  46.9 7.8 %collective-permute-done.22.refs_0_ = bf16[48,2048]{1,0:T(8,128)(2,1)S(1)} collective-permute-done((bf16[48,2048]{1,0:T(8,128)(2,1)S(1)}, bf16[48,2048]{1,0:T(8,128)(2,1)S(1)}, u32[]{:S(2)}, u32[]{:S(2)}) %collective-permute-start.22) | collective-permute-done | bytes 196640 | tf_op jit(solution)/shard_map/ppermute | solution.py:242
  54.8 2.3 %collective-permute-start.11 = (bf16[4,48,512]{2,1,0:T(8,128)(2,1)S(1)}, bf16[4,48,512]{2,1,0:T(8,128)(2,1)S(1)}, u32[]{:S(2)}, u32[]{:S(2)}) collective-permute-start(bf16[4,48,512]{2,1,0:T(8,128)(2,1)S(1)} %get-tuple-element.34), channel_id=1, source_target_pairs={{0,24},{4,28},{8,16},{12,20},{16,8},{20,12},{24,0},{28,4},{1,25},{... | collective-permute-start | bytes 589832 | tf_op jit(solution)/shard_map/ppermute | solution.py:242
  57.1 3.8 %collective-permute-start.12 = (bf16[4,48,512]{2,1,0:T(8,128)(2,1)S(1)}, bf16[4,48,512]{2,1,0:T(8,128)(2,1)S(1)}, u32[]{:S(2)}, u32[]{:S(2)}) collective-permute-start(bf16[4,48,512]{2,1,0:T(8,128)(2,1)S(1)} %get-tuple-element.35), channel_id=1, source_target_pairs={{0,28},{4,24},{8,20},{12,16},{16,12},{20,8},{24,4},{28,0},{1,29},{... | collective-permute-start | bytes 589832 | tf_op jit(solution)/shard_map/ppermute | solution.py:242
  63.4 1.6 %collective-permute-start.25 = (bf16[96,512]{1,0:T(8,128)(2,1)S(1)}, bf16[96,512]{1,0:T(8,128)(2,1)S(1)}, u32[]{:S(2)}, u32[]{:S(2)}) collective-permute-start(bf16[96,512]{1,0:T(8,128)(2,1)S(1)} %shard_map.120.refs_0_), channel_id=1, source_target_pairs={{0,2},{1,3},{2,0},{3,1},{4,6},{5,7},{6,4},{7,5},{8,10},{9,11},{10,... | collective-permute-start | bytes 294920 | tf_op jit(solution)/shard_map/ppermute | solution.py:242
  66.6 4.1 %collective-permute-start.19 = (bf16[4,48,512]{2,1,0:T(8,128)(2,1)S(1)}, bf16[4,48,512]{2,1,0:T(8,128)(2,1)S(1)}, u32[]{:S(2)}, u32[]{:S(2)}) collective-permute-start(bf16[4,48,512]{2,1,0:T(8,128)(2,1)S(1)} %get-tuple-element.41), channel_id=1, source_target_pairs={{0,4},{4,0},{8,12},{12,8},{16,20},{20,16},{24,28},{28,24},{1,5},{5... | collective-permute-start | bytes 589832 | tf_op jit(solution)/shard_map/ppermute | solution.py:242
  73.4 3.3 %collective-permute-start.27 = (bf16[4,48,512]{2,1,0:T(8,128)(2,1)S(1)}, bf16[4,48,512]{2,1,0:T(8,128)(2,1)S(1)}, u32[]{:S(2)}, u32[]{:S(2)}) collective-permute-start(bf16[4,48,512]{2,1,0:T(8,128)(2,1)S(1)} %get-tuple-element.47), channel_id=1, source_target_pairs={{0,16},{4,20},{8,24},{12,28},{16,0},{20,4},{24,8},{28,12},{1,17},{... | collective-permute-start | bytes 589832 | tf_op jit(solution)/shard_map/ppermute | solution.py:242
  76.7 2.2 %collective-permute-start.28 = (bf16[4,48,512]{2,1,0:T(8,128)(2,1)S(1)}, bf16[4,48,512]{2,1,0:T(8,128)(2,1)S(1)}, u32[]{:S(2)}, u32[]{:S(2)}) collective-permute-start(bf16[4,48,512]{2,1,0:T(8,128)(2,1)S(1)} %get-tuple-element.48), channel_id=1, source_target_pairs={{0,20},{4,16},{8,28},{12,24},{16,4},{20,0},{24,12},{28,8},{1,21},{... | collective-permute-start | bytes 589832 | tf_op jit(solution)/shard_map/ppermute | solution.py:242
  78.9 1.7 %shard_map.110 = (bf16[4,128,576]{2,1,0:T(8,128)(2,1)S(1)}, bf16[4,128,288]{2,1,0:T(8,128)(2,1)S(1)}, bf16[4,128,288]{2,1,0:T(8,128)(2,1)S(1)}) custom-call(s32[1]{0:T(128)} %bitcast.2.me, f32[4,128]{1,0:T(4,128)S(1)} %pad_maximum_fusion.refs_0_, f32[4,128]{1,0:T(4,128)S(1)} %collective-permute-done.3.refs_1_, f32[4,128]{1,0:T(4,128)S(1)} %collective-permute-done.4.refs_2_, ...), custom_call_target="tpu_custom_call" | custom-call | flops 8388608 | bytes 1187844 | tf_op jit(solution)/shard_map/pallas_call | solution.py:30
  81.4 1.9 %collective-permute-done.20.refs_2_ = bf16[4,48,512]{2,1,0:T(8,128)(2,1)S(1)} collective-permute-done((bf16[4,48,512]{2,1,0:T(8,128)(2,1)S(1)}, bf16[4,48,512]{2,1,0:T(8,128)(2,1)S(1)}, u32[]{:S(2)}, u32[]{:S(2)}) %collective-permute-start.20) | collective-permute-done | bytes 196640 | tf_op jit(solution)/shard_map/ppermute | solution.py:242
  83.3 5.1 %collective-permute-done.21.refs_3_ = bf16[4,48,512]{2,1,0:T(8,128)(2,1)S(1)} collective-permute-done((bf16[4,48,512]{2,1,0:T(8,128)(2,1)S(1)}, bf16[4,48,512]{2,1,0:T(8,128)(2,1)S(1)}, u32[]{:S(2)}, u32[]{:S(2)}) %collective-permute-start.21) | collective-permute-done | bytes 196640 | tf_op jit(solution)/shard_map/ppermute | solution.py:242
  89.0 5.7 %collective-permute-done.28.refs_1_ = bf16[4,48,512]{2,1,0:T(8,128)(2,1)S(1)} collective-permute-done((bf16[4,48,512]{2,1,0:T(8,128)(2,1)S(1)}, bf16[4,48,512]{2,1,0:T(8,128)(2,1)S(1)}, u32[]{:S(2)}, u32[]{:S(2)}) %collective-permute-start.28) | collective-permute-done | bytes 196640 | tf_op jit(solution)/shard_map/ppermute | solution.py:242
  95.7 2.1 %collective-permute-start.30 = (f32[4,128]{1,0:T(4,128)S(1)}, f32[4,128]{1,0:T(4,128)S(1)}, u32[]{:S(2)}, u32[]{:S(2)}) collective-permute-start(f32[4,128]{1,0:T(4,128)S(1)} %get-tuple-element.50.refs_0_), channel_id=1, source_target_pairs={{0,2},{1,3},{2,0},{3,1},{4,6},{5,7},{6,4},{7,5},{8,10},{9,11},{10,... | collective-permute-start | bytes 6152 | tf_op jit(solution)/shard_map/ppermute | solution.py:242
  99.4 2.9 %collective-permute-done.31.refs_3_ = f32[4,128]{1,0:T(4,128)S(1)} collective-permute-done((f32[4,128]{1,0:T(4,128)S(1)}, f32[4,128]{1,0:T(4,128)S(1)}, u32[]{:S(2)}, u32[]{:S(2)}) %collective-permute-start.31) | collective-permute-done | bytes 2080 | tf_op jit(solution)/shard_map/ppermute | solution.py:242
  (71 shorter events, 26.0 us)
Async XLA Ops:
  2.0 35.1 %collective-permute-start.13 = (bf16[48,2048]{1,0:T(8,128)(2,1)S(1)}, bf16[48,2048]{1,0:T(8,128)(2,1)S(1)}, u32[]{:S(2)}, u32[]{:S(2)}) collective-permute-start(bf16[48,2048]{1,0:T(8,128)(2,1)S(1)} %get-tuple-element.37), channel_id=1, source_target_pairs={{0,4},{4,0},{8,12},{12,8},{16,20},{20,16},{24,28},{28,24},{1,5},{5... | collective-permute-start | bytes 589832 | tf_op jit(solution)/shard_map/ppermute | solution.py:242
  2.5 23.2 %collective-permute-start.6 = (bf16[48,2048]{1,0:T(8,128)(2,1)S(1)}, bf16[48,2048]{1,0:T(8,128)(2,1)S(1)}, u32[]{:S(2)}, u32[]{:S(2)}) collective-permute-start(bf16[48,2048]{1,0:T(8,128)(2,1)S(1)} %get-tuple-element.29), channel_id=1, source_target_pairs={{0,24},{4,28},{8,16},{12,20},{16,8},{20,12},{24,0},{28,4},{1,25},{... | collective-permute-start | bytes 589832 | tf_op jit(solution)/shard_map/ppermute | solution.py:242
  7.2 20.3 %collective-permute-start.7 = (bf16[48,2048]{1,0:T(8,128)(2,1)S(1)}, bf16[48,2048]{1,0:T(8,128)(2,1)S(1)}, u32[]{:S(2)}, u32[]{:S(2)}) collective-permute-start(bf16[48,2048]{1,0:T(8,128)(2,1)S(1)} %get-tuple-element.30), channel_id=1, source_target_pairs={{0,28},{4,24},{8,20},{12,16},{16,12},{20,8},{24,4},{28,0},{1,29},{... | collective-permute-start | bytes 589832 | tf_op jit(solution)/shard_map/ppermute | solution.py:242
  11.9 13.7 %collective-permute-start = (bf16[128,512]{1,0:T(8,128)(2,1)S(1)}, bf16[128,512]{1,0:T(8,128)(2,1)S(1)}, u32[]{:S(2)}, u32[]{:S(2)}) collective-permute-start(bf16[128,512]{1,0:T(8,128)(2,1)S(1)} %shard_map.109.refs_0_), channel_id=1, source_target_pairs={{0,1},{1,0},{2,3},{3,2},{4,5},{5,4},{6,7},{7,6},{8,9},{9,8},{10,11... | collective-permute-start | bytes 393224 | tf_op jit(solution)/shard_map/ppermute | solution.py:242
  25.7 11.4 %collective-permute-start.14 = (bf16[48,2048]{1,0:T(8,128)(2,1)S(1)}, bf16[48,2048]{1,0:T(8,128)(2,1)S(1)}, u32[]{:S(2)}, u32[]{:S(2)}) collective-permute-start(bf16[48,2048]{1,0:T(8,128)(2,1)S(1)} %get-tuple-element.38), channel_id=1, source_target_pairs={{0,8},{4,12},{8,0},{12,4},{16,24},{20,28},{24,16},{28,20},{1,9},{5... | collective-permute-start | bytes 589832 | tf_op jit(solution)/shard_map/ppermute | solution.py:242
  25.7 16.1 %collective-permute-start.15 = (bf16[48,2048]{1,0:T(8,128)(2,1)S(1)}, bf16[48,2048]{1,0:T(8,128)(2,1)S(1)}, u32[]{:S(2)}, u32[]{:S(2)}) collective-permute-start(bf16[48,2048]{1,0:T(8,128)(2,1)S(1)} %get-tuple-element.39), channel_id=1, source_target_pairs={{0,12},{4,8},{8,4},{12,0},{16,28},{20,24},{24,20},{28,16},{1,13},{... | collective-permute-start | bytes 589832 | tf_op jit(solution)/shard_map/ppermute | solution.py:242
  27.5 9.0 %collective-permute-start.2 = (bf16[128,512]{1,0:T(8,128)(2,1)S(1)}, bf16[128,512]{1,0:T(8,128)(2,1)S(1)}, u32[]{:S(2)}, u32[]{:S(2)}) collective-permute-start(bf16[128,512]{1,0:T(8,128)(2,1)S(1)} %shard_map.109.refs_0_), channel_id=1, source_target_pairs={{0,3},{1,2},{2,1},{3,0},{4,7},{5,6},{6,5},{7,4},{8,11},{9,10},{10,... | collective-permute-start | bytes 393224 | tf_op jit(solution)/shard_map/ppermute | solution.py:242
  32.0 10.9 %collective-permute-start.10 = (bf16[96,512]{1,0:T(8,128)(2,1)S(1)}, bf16[96,512]{1,0:T(8,128)(2,1)S(1)}, u32[]{:S(2)}, u32[]{:S(2)}) collective-permute-start(bf16[96,512]{1,0:T(8,128)(2,1)S(1)} %shard_map.114.refs_0_), channel_id=1, source_target_pairs={{0,3},{1,2},{2,1},{3,0},{4,7},{5,6},{6,5},{7,4},{8,11},{9,10},{10,... | collective-permute-start | bytes 294920 | tf_op jit(solution)/shard_map/ppermute | solution.py:242
  36.5 8.1 %collective-permute-start.8 = (bf16[96,512]{1,0:T(8,128)(2,1)S(1)}, bf16[96,512]{1,0:T(8,128)(2,1)S(1)}, u32[]{:S(2)}, u32[]{:S(2)}) collective-permute-start(bf16[96,512]{1,0:T(8,128)(2,1)S(1)} %shard_map.114.refs_0_), channel_id=1, source_target_pairs={{0,1},{1,0},{2,3},{3,2},{4,5},{5,4},{6,7},{7,6},{8,9},{9,8},{10,11... | collective-permute-start | bytes 294920 | tf_op jit(solution)/shard_map/ppermute | solution.py:242
  37.0 9.1 %collective-permute-start.9 = (bf16[96,512]{1,0:T(8,128)(2,1)S(1)}, bf16[96,512]{1,0:T(8,128)(2,1)S(1)}, u32[]{:S(2)}, u32[]{:S(2)}) collective-permute-start(bf16[96,512]{1,0:T(8,128)(2,1)S(1)} %shard_map.114.refs_0_), channel_id=1, source_target_pairs={{0,2},{1,3},{2,0},{3,1},{4,6},{5,7},{6,4},{7,5},{8,10},{9,11},{10,... | collective-permute-start | bytes 294920 | tf_op jit(solution)/shard_map/ppermute | solution.py:242
  37.0 17.7 %collective-permute-start.22 = (bf16[48,2048]{1,0:T(8,128)(2,1)S(1)}, bf16[48,2048]{1,0:T(8,128)(2,1)S(1)}, u32[]{:S(2)}, u32[]{:S(2)}) collective-permute-start(bf16[48,2048]{1,0:T(8,128)(2,1)S(1)} %get-tuple-element.45), channel_id=1, source_target_pairs={{0,16},{4,20},{8,24},{12,28},{16,0},{20,4},{24,8},{28,12},{1,17},{... | collective-permute-start | bytes 589832 | tf_op jit(solution)/shard_map/ppermute | solution.py:242
  41.8 15.3 %collective-permute-start.23 = (bf16[48,2048]{1,0:T(8,128)(2,1)S(1)}, bf16[48,2048]{1,0:T(8,128)(2,1)S(1)}, u32[]{:S(2)}, u32[]{:S(2)}) collective-permute-start(bf16[48,2048]{1,0:T(8,128)(2,1)S(1)} %get-tuple-element.46), channel_id=1, source_target_pairs={{0,20},{4,16},{8,28},{12,24},{16,4},{20,0},{24,12},{28,8},{1,21},{... | collective-permute-start | bytes 589832 | tf_op jit(solution)/shard_map/ppermute | solution.py:242
  43.0 18.9 %collective-permute-start.16 = (bf16[192,512]{1,0:T(8,128)(2,1)S(1)}, bf16[192,512]{1,0:T(8,128)(2,1)S(1)}, u32[]{:S(2)}, u32[]{:S(2)}) collective-permute-start(bf16[192,512]{1,0:T(8,128)(2,1)S(1)} %shard_map.117.refs_0_), channel_id=1, source_target_pairs={{0,1},{1,0},{2,3},{3,2},{4,5},{5,4},{6,7},{7,6},{8,9},{9,8},{10,11... | collective-permute-start | bytes 589832 | tf_op jit(solution)/shard_map/ppermute | solution.py:242
  44.6 18.9 %collective-permute-start.17 = (bf16[192,512]{1,0:T(8,128)(2,1)S(1)}, bf16[192,512]{1,0:T(8,128)(2,1)S(1)}, u32[]{:S(2)}, u32[]{:S(2)}) collective-permute-start(bf16[192,512]{1,0:T(8,128)(2,1)S(1)} %shard_map.117.refs_0_), channel_id=1, source_target_pairs={{0,2},{1,3},{2,0},{3,1},{4,6},{5,7},{6,4},{7,5},{8,10},{9,11},{10,... | collective-permute-start | bytes 589832 | tf_op jit(solution)/shard_map/ppermute | solution.py:242
  46.1 19.0 %collective-permute-start.18 = (bf16[192,512]{1,0:T(8,128)(2,1)S(1)}, bf16[192,512]{1,0:T(8,128)(2,1)S(1)}, u32[]{:S(2)}, u32[]{:S(2)}) collective-permute-start(bf16[192,512]{1,0:T(8,128)(2,1)S(1)} %shard_map.117.refs_0_), channel_id=1, source_target_pairs={{0,3},{1,2},{2,1},{3,0},{4,7},{5,6},{6,5},{7,4},{8,11},{9,10},{10,... | collective-permute-start | bytes 589832 | tf_op jit(solution)/shard_map/ppermute | solution.py:242
  54.8 18.6 %collective-permute-start.11 = (bf16[4,48,512]{2,1,0:T(8,128)(2,1)S(1)}, bf16[4,48,512]{2,1,0:T(8,128)(2,1)S(1)}, u32[]{:S(2)}, u32[]{:S(2)}) collective-permute-start(bf16[4,48,512]{2,1,0:T(8,128)(2,1)S(1)} %get-tuple-element.34), channel_id=1, source_target_pairs={{0,24},{4,28},{8,16},{12,20},{16,8},{20,12},{24,0},{28,4},{1,25},{... | collective-permute-start | bytes 589832 | tf_op jit(solution)/shard_map/ppermute | solution.py:242
  57.1 19.6 %collective-permute-start.12 = (bf16[4,48,512]{2,1,0:T(8,128)(2,1)S(1)}, bf16[4,48,512]{2,1,0:T(8,128)(2,1)S(1)}, u32[]{:S(2)}, u32[]{:S(2)}) collective-permute-start(bf16[4,48,512]{2,1,0:T(8,128)(2,1)S(1)} %get-tuple-element.35), channel_id=1, source_target_pairs={{0,28},{4,24},{8,20},{12,16},{16,12},{20,8},{24,4},{28,0},{1,29},{... | collective-permute-start | bytes 589832 | tf_op jit(solution)/shard_map/ppermute | solution.py:242
  63.4 7.3 %collective-permute-start.25 = (bf16[96,512]{1,0:T(8,128)(2,1)S(1)}, bf16[96,512]{1,0:T(8,128)(2,1)S(1)}, u32[]{:S(2)}, u32[]{:S(2)}) collective-permute-start(bf16[96,512]{1,0:T(8,128)(2,1)S(1)} %shard_map.120.refs_0_), channel_id=1, source_target_pairs={{0,2},{1,3},{2,0},{3,1},{4,6},{5,7},{6,4},{7,5},{8,10},{9,11},{10,... | collective-permute-start | bytes 294920 | tf_op jit(solution)/shard_map/ppermute | solution.py:242
  65.1 6.4 %collective-permute-start.26 = (bf16[96,512]{1,0:T(8,128)(2,1)S(1)}, bf16[96,512]{1,0:T(8,128)(2,1)S(1)}, u32[]{:S(2)}, u32[]{:S(2)}) collective-permute-start(bf16[96,512]{1,0:T(8,128)(2,1)S(1)} %shard_map.120.refs_0_), channel_id=1, source_target_pairs={{0,3},{1,2},{2,1},{3,0},{4,7},{5,6},{6,5},{7,4},{8,11},{9,10},{10,... | collective-permute-start | bytes 294920 | tf_op jit(solution)/shard_map/ppermute | solution.py:242
  66.6 14.8 %collective-permute-start.19 = (bf16[4,48,512]{2,1,0:T(8,128)(2,1)S(1)}, bf16[4,48,512]{2,1,0:T(8,128)(2,1)S(1)}, u32[]{:S(2)}, u32[]{:S(2)}) collective-permute-start(bf16[4,48,512]{2,1,0:T(8,128)(2,1)S(1)} %get-tuple-element.41), channel_id=1, source_target_pairs={{0,4},{4,0},{8,12},{12,8},{16,20},{20,16},{24,28},{28,24},{1,5},{5... | collective-permute-start | bytes 589832 | tf_op jit(solution)/shard_map/ppermute | solution.py:242
  70.7 12.6 %collective-permute-start.20 = (bf16[4,48,512]{2,1,0:T(8,128)(2,1)S(1)}, bf16[4,48,512]{2,1,0:T(8,128)(2,1)S(1)}, u32[]{:S(2)}, u32[]{:S(2)}) collective-permute-start(bf16[4,48,512]{2,1,0:T(8,128)(2,1)S(1)} %get-tuple-element.42), channel_id=1, source_target_pairs={{0,8},{4,12},{8,0},{12,4},{16,24},{20,28},{24,16},{28,20},{1,9},{5... | collective-permute-start | bytes 589832 | tf_op jit(solution)/shard_map/ppermute | solution.py:242
  71.5 16.9 %collective-permute-start.21 = (bf16[4,48,512]{2,1,0:T(8,128)(2,1)S(1)}, bf16[4,48,512]{2,1,0:T(8,128)(2,1)S(1)}, u32[]{:S(2)}, u32[]{:S(2)}) collective-permute-start(bf16[4,48,512]{2,1,0:T(8,128)(2,1)S(1)} %get-tuple-element.43), channel_id=1, source_target_pairs={{0,12},{4,8},{8,4},{12,0},{16,28},{20,24},{24,20},{28,16},{1,13},{... | collective-permute-start | bytes 589832 | tf_op jit(solution)/shard_map/ppermute | solution.py:242
  73.4 15.6 %collective-permute-start.27 = (bf16[4,48,512]{2,1,0:T(8,128)(2,1)S(1)}, bf16[4,48,512]{2,1,0:T(8,128)(2,1)S(1)}, u32[]{:S(2)}, u32[]{:S(2)}) collective-permute-start(bf16[4,48,512]{2,1,0:T(8,128)(2,1)S(1)} %get-tuple-element.47), channel_id=1, source_target_pairs={{0,16},{4,20},{8,24},{12,28},{16,0},{20,4},{24,8},{28,12},{1,17},{... | collective-permute-start | bytes 589832 | tf_op jit(solution)/shard_map/ppermute | solution.py:242
  76.7 18.0 %collective-permute-start.28 = (bf16[4,48,512]{2,1,0:T(8,128)(2,1)S(1)}, bf16[4,48,512]{2,1,0:T(8,128)(2,1)S(1)}, u32[]{:S(2)}, u32[]{:S(2)}) collective-permute-start(bf16[4,48,512]{2,1,0:T(8,128)(2,1)S(1)} %get-tuple-element.48), channel_id=1, source_target_pairs={{0,20},{4,16},{8,28},{12,24},{16,4},{20,0},{24,12},{28,8},{1,21},{... | collective-permute-start | bytes 589832 | tf_op jit(solution)/shard_map/ppermute | solution.py:242
  (15 other events, 83.2 us)
